TPU v7x, 32 devices: a whole 2x2x4 slice. The times are simulated.
32 devices in a mesh: sp: 16 (over z, y, core), tp: 2 (over x).
Axes of the slice: x: 2, y: 2, z: 4, core: 2. Of those that a mesh axis runs over, the one named last changes fastest.
Arguments:
- tokens: bfloat16 [16384, 2048], P('sp'), may hold values from -6 to 6
- norm_gain: float32 [2048], replicated, may hold values from 0.1 to 1.9
- w_query: bfloat16 [2048, 512], P(None, 'tp'), may hold values from -0.79549513 to 0.79549513
- w_key: bfloat16 [2048, 128], P('sp'), may hold values from -0.79549513 to 0.79549513
- w_value: bfloat16 [2048, 128], P('sp'), may hold values from -0.125 to 0.125
- w_pool_in: bfloat16 [2048, 512], P(None, 'tp'), may hold values from -0.125 to 0.125
- sink_logit: float32 [8], P('tp'), may hold values from 3 to 7
- pool_scale: float32 [512], P('tp'), may hold values from 0.05 to 0.5
- w_out: bfloat16 [1024, 2048], P('tp', 'sp'), may hold values from -0.75 to 0.75
Outputs:
- mixed_out: bfloat16 [16384, 2048], P(('sp', 'tp'))
All inputs are finite; a program needn't handle non-finite values.
Results may differ from a plain program's by a relative error of at most 0.03.
The roundings to bfloat16 on the way count: a program that leaves them out, or rounds other values in their place, can miss the bound.
Values may be sent and summed in bfloat16 or wider, within the bound.
No kernel may reach another device: no remote copies, remote signals or barrier semaphores. Data moves between devices by JAX's collectives and lax.ppermute only.
A program may use at most 64 MiB of HBM per device.

v0:
```python
import jax
import jax.numpy as jnp
from jax import lax
from jax.sharding import PartitionSpec as P

HEAD = 64
QH = 8
KVH = 2
POOL_CH = 128
WINDOW = 128
QB = 128


NEG_BIG = -1e30
POOL_SPANS = (2, 4, 8, 16)


def extended(block, sides, width):
    for axis, dim in sides:
        count = lax.axis_size(axis)
        forward = [(i, i + 1) for i in range(count - 1)]
        backward = [(target, source) for source, target in forward]
        low = lax.ppermute(
            lax.slice_in_dim(block, block.shape[dim] - width, None, axis=dim), axis, forward
        )
        high = lax.ppermute(lax.slice_in_dim(block, 0, width, axis=dim), axis, backward)
        block = jnp.concatenate([low, block, high], axis=dim)
    return block


def layer_normed(tokens, norm_gain):
    values = tokens.astype(jnp.float32)
    center = jnp.mean(values, axis=-1, keepdims=True)
    spread = jnp.mean(jnp.square(values - center), axis=-1, keepdims=True)
    return ((values - center) * lax.rsqrt(spread + 1e-06) * norm_gain).astype(jnp.bfloat16)


def rotate(values, positions):
    half = HEAD // 2
    inverse = 10000.0 ** (-jnp.arange(half, dtype=jnp.float32) / half)
    angles = positions[:, None] * inverse[None, :]
    cosine = jnp.cos(angles)[:, None, :]
    sine = jnp.sin(angles)[:, None, :]
    first = values[..., :half]
    second = values[..., half:]
    return jnp.concatenate(
        [first * cosine - second * sine, first * sine + second * cosine], axis=-1
    )


def body(tokens, norm_gain, w_query, w_key, w_value, w_pool_in, sink_logit, pool_scale, w_out):
    local_rows = tokens.shape[0]
    seq_total = local_rows * lax.axis_size("sp")
    offset = lax.axis_index("sp") * local_rows
    tp_place = lax.axis_index("tp")
    local_heads = w_query.shape[1] // HEAD
    local_pool = w_pool_in.shape[1]
    reach = POOL_SPANS[-1] // 2
    normed = layer_normed(tokens, norm_gain)
    positions = (offset + jnp.arange(local_rows)).astype(jnp.float32)
    query = rotate(
        jnp.dot(normed, w_query, preferred_element_type=jnp.float32).reshape(
            local_rows, local_heads, HEAD
        ),
        positions,
    ).astype(jnp.bfloat16)
    key_head = tp_place * local_heads // (QH // KVH)
    key_cols = lax.dynamic_slice_in_dim(w_key, key_head * HEAD, HEAD, 1)
    value_cols = lax.dynamic_slice_in_dim(w_value, key_head * HEAD, HEAD, 1)
    key_sum = jnp.dot(
        normed,
        lax.all_gather(key_cols, "sp", axis=0, tiled=True),
        preferred_element_type=jnp.float32,
    )
    value_sum = jnp.dot(
        normed,
        lax.all_gather(value_cols, "sp", axis=0, tiled=True),
        preferred_element_type=jnp.float32,
    )
    key = rotate(key_sum[:, None, :], positions)[:, 0, :].astype(jnp.bfloat16)
    value = value_sum.astype(jnp.bfloat16)
    key_value = jnp.concatenate([key, value], axis=1)
    pool_in = jnp.dot(normed, w_pool_in, preferred_element_type=jnp.float32).astype(jnp.bfloat16)
    widened = extended(jnp.concatenate([key_value, pool_in], axis=1), (("sp", 0),), WINDOW)
    kv_wide = widened[:, : 2 * HEAD]
    pool_wide = widened[WINDOW - reach : WINDOW + local_rows + reach, 2 * HEAD :]
    span = QB + 2 * WINDOW
    sink_here = sink_logit[:, None, None]
    results = []
    for block in range(local_rows // QB):
        queries = query[block * QB : (block + 1) * QB]
        keys = kv_wide[block * QB : block * QB + span, :HEAD]
        values = kv_wide[block * QB : block * QB + span, HEAD:]
        scores = jnp.einsum(
            "ihd,jd->hij", queries, keys, preferred_element_type=jnp.float32
        ) * HEAD ** (-0.5)
        query_pos = offset + block * QB + jnp.arange(QB)
        key_pos = offset + block * QB - WINDOW + jnp.arange(span)
        valid = (
            (jnp.abs(query_pos[:, None] - key_pos[None, :]) <= WINDOW)
            & (key_pos[None, :] >= 0)
            & (key_pos[None, :] < seq_total)
        )
        scores = jnp.where(valid, scores, NEG_BIG)
        highest = jnp.maximum(jnp.max(scores, axis=-1, keepdims=True), sink_here)
        expo = jnp.where(valid, jnp.exp(scores - highest), 0.0)
        total = jnp.sum(expo, axis=-1, keepdims=True) + jnp.exp(sink_here - highest)
        weights = (expo / total).astype(jnp.bfloat16)
        result = jnp.einsum("hij,jd->ihd", weights, values, preferred_element_type=jnp.float32)
        results.append(result.reshape(QB, local_heads * HEAD).astype(jnp.bfloat16))
    attended = jnp.concatenate(results, axis=0)
    pool_vals = pool_wide.astype(jnp.float32)
    window_sum = pool_vals
    global_pos = offset + jnp.arange(local_rows)
    channel = tp_place * local_pool + jnp.arange(local_pool)
    window_group = channel // POOL_CH
    measured = jnp.zeros((local_rows, local_pool), jnp.float32)
    stride = 1
    for index, width in enumerate(POOL_SPANS):
        window_sum = window_sum[:-stride] + window_sum[stride:]
        stride = width
        sums = window_sum[reach - width // 2 : reach - width // 2 + local_rows]
        counted = (
            jnp.minimum(global_pos + width // 2, seq_total)
            - jnp.maximum(global_pos - width // 2, 0)
        ).astype(jnp.float32)
        measured = measured + jnp.where(
            window_group[None, :] == index, sums / counted[:, None], 0.0
        )
    pooled = ((measured - pool_vals[reach : reach + local_rows]) * pool_scale).astype(jnp.bfloat16)
    attended_rows, pooled_rows = (
        lax.all_to_all(attended, "tp", split_axis=0, concat_axis=1, tiled=True),
        lax.all_to_all(pooled, "tp", split_axis=0, concat_axis=1, tiled=True),
    )
    joined = jnp.concatenate([attended_rows, pooled_rows], axis=1)
    out_rows_all = lax.all_gather(w_out, "tp", axis=0, tiled=True)
    projected = jnp.dot(
        joined,
        lax.all_gather(out_rows_all, "sp", axis=1, tiled=True),
        preferred_element_type=jnp.float32,
    )
    return projected.astype(jnp.bfloat16)


def solution(mesh):
    in_specs = (
        P("sp", None),
        P(),
        P(None, "tp"),
        P("sp", None),
        P("sp", None),
        P(None, "tp"),
        P("tp"),
        P("tp"),
        P("tp", "sp"),
    )
    out_specs = P(("sp", "tp"), None)
    return jax.shard_map(body, mesh=mesh, in_specs=in_specs, out_specs=out_specs, check_vma=False)
```

profile of v0, /device:TPU:0, one launch (start us, length us, event | category | flops | bytes accessed | tf_op | source)
XLA Modules:
  0.0 166.7 jit_solution(2030448479956947112)
XLA Ops:
  6.6 0.9 constant_dynamic-slice_fusion.1
  7.5 24.6 %all_gather.12 = bf16[2048,64]{1,0:T(8,128)(2,1)S(1)} all-gather(bf16[128,64]{1,0:T(8,128)(2,1)S(1)} %constant_dynamic-slice_fusion.1), channel_id=1, replica_groups=mesh['sp'=16,'tp'=2] {'sp'}, dimensions={0}, use_global_device_ids=true | all-gather | bytes 278528 | tf_op jit(solution)/shard_map/all_gather | solution.py:72
  32.1 3.0 %convert_reduce_fusion = f32[1024]{0:T(1024)S(1)} fusion(bf16[1024,2048]{1,0:T(8,128)(2,1)} %param.9), kind=kLoop, calls=%fused_computation.1 | loop fusion | flops 4193280 | bytes 4198400 | tf_op jit(solution)/shard_map/reduce_sum | solution.py:33
  35.5 1.2 fusion.2
  36.9 18.9 %all_gather.13 = bf16[2048,64]{1,0:T(8,128)(2,1)S(1)} all-gather(bf16[128,64]{1,0:T(8,128)(2,1)S(1)} %constant_dynamic-slice_fusion), channel_id=1, replica_groups=mesh['sp'=16,'tp'=2] {'sp'}, dimensions={0}, use_global_device_ids=true | all-gather | bytes 278528 | tf_op jit(solution)/shard_map/all_gather | solution.py:77
  55.8 3.0 %fusion.4 = bf16[1024,2048]{1,0:T(8,128)(2,1)S(1)} fusion(bf16[1024,2048]{1,0:T(8,128)(2,1)} %param.9, f32[2048]{0:T(1024)S(1)} %copy-done.53, f32[1024]{0:T(1024)S(1)} %add_rsqrt_fusion, f32[1024]{0:T(1024)S(1)} %broadcast_multiply_fusion), kind=kLoop, calls=%fused_computation.6 | loop fusion | flops 10485760 | bytes 8404992 | tf_op jit(solution)/shard_map/convert_element_type | solution.py:35
  58.8 1.4 convolution_bitcast_fusion
  60.2 1.4 convolution_convert_fusion.2
  61.6 1.3 convolution_convert_fusion.1
  63.6 1.3 collective-permute-start.1
  64.9 3.7 %collective-permute-start = (bf16[128,384]{0,1:T(8,128)(2,1)S(1)}, bf16[128,384]{0,1:T(8,128)(2,1)}, u32[]{:S(2)}, u32[]{:S(2)}) collective-permute-start(bf16[128,384]{0,1:T(8,128)(2,1)S(1)} %get-tuple-element.9), channel_id=1, source_target_pairs={{0,2},{2,4},{4,6},{6,8},{8,10},{10,12},{12,14},{14,16},{16,18},{18... | collective-permute-start | bytes 294920 | tf_op jit(solution)/shard_map/ppermute | solution.py:23
  68.5 7.3 %all_gather.14 = bf16[1024,128]{1,0:T(8,128)(2,1)} all-gather(bf16[512,128]{1,0:T(8,128)(2,1)S(1)} %copy-done.28), channel_id=1, replica_groups=mesh['sp'=16,'tp'=2] {'tp'}, dimensions={0}, use_global_device_ids=true | all-gather | bytes 393216 | tf_op jit(solution)/shard_map/all_gather | solution.py:136
  77.9 3.8 %fusion.164 = f32[1024,256]{0,1:T(8,128)S(1)} fusion(bf16[1024,2048]{1,0:T(8,128)(2,1)} %copy-done.2, bf16[2048,256]{1,0:T(8,128)(2,1)} %param.11), kind=kOutput, calls=%fused_computation.317 | convolution fusion | flops 1073741824 | bytes 6291456 | tf_op jit(solution)/shard_map/dot_general | solution.py:62
  82.1 1.7 %fusion.163 = (f32[4,128]{1,0:T(4,128)}, f32[4,128,384]{1,2,0:T(8,128)}) fusion(bf16[1024,4,32]{0,2,1:T(8,128)(2,1)S(1)} %get-tuple-element.6, bf16[1024,4,32]{0,2,1:T(8,128)(2,1)S(1)} %get-tuple-element.5, bf16[1024,1,32]{0,2,1:T(8,128)(2,1)S(1)} %get-tuple-element.11, bf16[1024,1,32]{0,2,1:T(8,128)(2,1)S(1)} %get-tuple-element.12, ...), kind=kOutput, calls=%fused_computation.316 | convolution fusion | flops 25984512 | bytes 1492992 | tf_op jit(solution)/shard_map/ihd,jd->hij/dot_general | solution.py:94
  84.0 1.8 %fusion.162 = (f32[4,128]{1,0:T(4,128)}, f32[4,128,384]{1,2,0:T(8,128)}) fusion(bf16[1024,4,32]{0,2,1:T(8,128)(2,1)S(1)} %get-tuple-element.6, bf16[1024,4,32]{0,2,1:T(8,128)(2,1)S(1)} %get-tuple-element.5, bf16[1024,1,32]{0,2,1:T(8,128)(2,1)S(1)} %get-tuple-element.11, bf16[1024,1,32]{0,2,1:T(8,128)(2,1)S(1)} %get-tuple-element.12, ...), kind=kOutput, calls=%fused_computation.315 | convolution fusion | flops 25984512 | bytes 1492992 | tf_op jit(solution)/shard_map/ihd,jd->hij/dot_general | solution.py:94
  86.1 1.8 %fusion.161 = (f32[4,128]{1,0:T(4,128)}, f32[4,128,384]{1,2,0:T(8,128)}) fusion(bf16[1024,4,32]{0,2,1:T(8,128)(2,1)S(1)} %get-tuple-element.6, bf16[1024,4,32]{0,2,1:T(8,128)(2,1)S(1)} %get-tuple-element.5, bf16[1024,1,32]{0,2,1:T(8,128)(2,1)S(1)} %get-tuple-element.11, bf16[1024,1,32]{0,2,1:T(8,128)(2,1)S(1)} %get-tuple-element.12, ...), kind=kOutput, calls=%fused_computation.314 | convolution fusion | flops 25984512 | bytes 1492992 | tf_op jit(solution)/shard_map/ihd,jd->hij/dot_general | solution.py:94
  88.1 1.8 %fusion.160 = (f32[4,128]{1,0:T(4,128)}, f32[4,128,384]{1,2,0:T(8,128)}) fusion(bf16[1024,4,32]{0,2,1:T(8,128)(2,1)S(1)} %get-tuple-element.6, bf16[1024,4,32]{0,2,1:T(8,128)(2,1)S(1)} %get-tuple-element.5, bf16[1024,1,32]{0,2,1:T(8,128)(2,1)S(1)} %get-tuple-element.11, bf16[1024,1,32]{0,2,1:T(8,128)(2,1)S(1)} %get-tuple-element.12, ...), kind=kOutput, calls=%fused_computation.313 | convolution fusion | flops 25984512 | bytes 1492992 | tf_op jit(solution)/shard_map/ihd,jd->hij/dot_general | solution.py:94
  90.1 1.8 %fusion.159 = (f32[4,128]{1,0:T(4,128)}, f32[4,128,384]{1,2,0:T(8,128)}) fusion(bf16[1024,4,32]{0,2,1:T(8,128)(2,1)S(1)} %get-tuple-element.6, bf16[1024,4,32]{0,2,1:T(8,128)(2,1)S(1)} %get-tuple-element.5, bf16[1024,1,32]{0,2,1:T(8,128)(2,1)S(1)} %get-tuple-element.11, bf16[1024,1,32]{0,2,1:T(8,128)(2,1)S(1)} %get-tuple-element.12, ...), kind=kOutput, calls=%fused_computation.312 | convolution fusion | flops 25984512 | bytes 1492992 | tf_op jit(solution)/shard_map/ihd,jd->hij/dot_general | solution.py:94
  92.1 1.7 %fusion.158 = (f32[4,128]{1,0:T(4,128)}, f32[4,128,384]{1,2,0:T(8,128)}) fusion(bf16[1024,4,32]{0,2,1:T(8,128)(2,1)S(1)} %get-tuple-element.6, bf16[1024,4,32]{0,2,1:T(8,128)(2,1)S(1)} %get-tuple-element.5, bf16[1024,1,32]{0,2,1:T(8,128)(2,1)S(1)} %get-tuple-element.11, bf16[1024,1,32]{0,2,1:T(8,128)(2,1)S(1)} %get-tuple-element.12, ...), kind=kOutput, calls=%fused_computation.311 | convolution fusion | flops 25984512 | bytes 1492992 | tf_op jit(solution)/shard_map/ihd,jd->hij/dot_general | solution.py:94
  95.8 1.0 fusion.157
  97.8 0.7 exponential_add_fusion
  98.4 1.6 convolution_convert_fusion.3
  100.1 1.6 copy.42
  101.7 1.0 fusion.39
  102.8 1.3 fusion.38
  104.1 1.0 fusion.37
  105.7 0.7 exponential_add_fusion.1
  106.4 0.9 convolution_convert_fusion.4
  107.3 1.6 copy.41
  108.9 1.6 convolution_convert_fusion.5
  110.5 1.6 copy.40
  112.1 2.1 %convolution_convert_fusion.6 = bf16[64,4,128]{2,0,1:T(8,128)(2,1)} fusion(f32[4,128,384]{1,2,0:T(8,128)} %get-tuple-element.42, f32[4,128]{1,0:T(4,128)} %get-tuple-element.29, f32[4,128]{1,0:T(4,128)} %get-tuple-element.20, pred[128,384]{0,1:T(8,128)(4,1)S(1)} %fusion.52, bf16[1024,64]{0,1:T(8,128)(2,1)S(1)} %convolution_convert_fusion.2), kind=kOutput, calls=%fused_computation.41 | convolution fusion | flops 25985024 | bytes 954368 | tf_op jit(solution)/shard_map/hij,jd->ihd/dot_general | solution.py:109
  114.2 1.6 copy.39
  115.8 1.6 convolution_convert_fusion.7
  117.4 1.6 copy.38
  119.0 2.1 %convolution_convert_fusion.8 = bf16[64,4,128]{2,0,1:T(8,128)(2,1)} fusion(f32[4,128,384]{1,2,0:T(8,128)} %get-tuple-element.38, f32[4,128]{1,0:T(4,128)S(1)} %copy-done.58, f32[4,128]{1,0:T(4,128)S(1)} %copy-done.51, pred[128,384]{0,1:T(8,128)(4,1)S(1)} %copy-done.14, bf16[1024,64]{0,1:T(8,128)(2,1)S(1)} %convolution_convert_fusion.2), kind=kOutput, calls=%fused_computation.43 | convolution fusion | flops 25985024 | bytes 954368 | tf_op jit(solution)/shard_map/hij,jd->ihd/dot_general | solution.py:109
  121.1 1.6 copy.37
  122.7 0.9 convolution_convert_fusion.9
  123.6 1.0 copy.36
  124.7 1.1 convolution_convert_fusion.10
  130.9 3.7 %all-to-all-start = ((bf16[2,512,256]{2,1,0:T(8,128)(2,1)}), bf16[2,512,256]{2,1,0:T(8,128)(2,1)S(1)}, u32[]{:S(2)}, u32[]{:S(2)}) async-start(bf16[2,512,256]{2,1,0:T(8,128)(2,1)} %bitcast.49), calls=%async_computation | async-start | bytes 1048576 | tf_op jit(solution)/shard_map/all_to_all | solution.py:132
  134.6 1.1 fusion.42
  137.7 1.6 fusion.22
  139.3 0.8 copy.55
  140.2 2.7 %all-to-all-done = bf16[2,512,256]{2,1,0:T(8,128)(2,1)S(1)} async-done(((bf16[2,512,256]{2,1,0:T(8,128)(2,1)}), bf16[2,512,256]{2,1,0:T(8,128)(2,1)S(1)}, u32[]{:S(2)}, u32[]{:S(2)}) %all-to-all-start) | async-done | bytes 524320 | tf_op jit(solution)/shard_map/all_to_all | solution.py:132
  142.9 3.5 %all-to-all-start.1 = ((bf16[2,512,256]{1,2,0:T(8,128)(2,1)}), bf16[2,512,256]{1,2,0:T(8,128)(2,1)S(1)}, u32[]{:S(2)}, u32[]{:S(2)}) async-start(bf16[2,512,256]{1,2,0:T(8,128)(2,1)} %bitcast.149), calls=%async_computation.1 | async-start | bytes 1048576 | tf_op jit(solution)/shard_map/all_to_all | solution.py:133
  146.6 7.4 %all-to-all-done.1 = bf16[2,512,256]{1,2,0:T(8,128)(2,1)S(1)} async-done(((bf16[2,512,256]{1,2,0:T(8,128)(2,1)}), bf16[2,512,256]{1,2,0:T(8,128)(2,1)S(1)}, u32[]{:S(2)}, u32[]{:S(2)}) %all-to-all-start.1) | async-done | bytes 524320 | tf_op jit(solution)/shard_map/all_to_all | solution.py:133
  154.0 5.9 %convolution_convert_fusion = bf16[512,2048]{1,0:T(8,128)(2,1)} fusion(bf16[1024,2048]{1,0:T(8,128)(2,1)} %all-gather.2.cloned.1.call-done, bf16[512,512]{0,1:T(8,128)(2,1)S(1)} %bitcast.153, bf16[512,512]{0,1:T(8,128)(2,1)S(1)} %bitcast.154), kind=kOutput, calls=%fused_computation.7 | convolution fusion | flops 2150629376 | bytes 7340032 | tf_op jit(solution)/shard_map/dot_general | solution.py:137
  (200 shorter events, 15.1 us)
Async XLA Ops:
  6.5 55.1 %copy-start = (bf16[2048,256]{1,0:T(8,128)(2,1)S(1)}, bf16[2048,256]{1,0:T(8,128)(2,1)}, u32[]{:S(2)}) copy-start(bf16[2048,256]{1,0:T(8,128)(2,1)} %param.14) | copy-start | bytes 3145732
  6.5 147.5 %all-gather.2.cloned.1.call-start = ((), (), s32[]{:S(2)}) async-start(), calls=%async_computation.2 | async-start | bytes 4456448 | tf_op jit(solution)/shard_map/all_gather | solution.py:139
  32.1 3.4 %copy-start.1 = (bf16[1024,2048]{1,0:T(8,128)(2,1)S(1)}, bf16[1024,2048]{1,0:T(8,128)(2,1)}, u32[]{:S(2)}) copy-start(bf16[1024,2048]{1,0:T(8,128)(2,1)} %param.9) | copy-start | bytes 12582916
  35.5 20.2 %copy-start.53 = (f32[2048]{0:T(1024)S(1)}, f32[2048]{0:T(1024)}, u32[]{:S(2)}) copy-start(f32[2048]{0:T(1024)} %param.10) | copy-start | bytes 24580
  58.8 2.8 %copy-start.2 = (bf16[1024,2048]{1,0:T(8,128)(2,1)}, bf16[1024,2048]{1,0:T(8,128)(2,1)S(1)}, u32[]{:S(2)}) copy-start(bf16[1024,2048]{1,0:T(8,128)(2,1)S(1)} %fusion.4) | copy-start | bytes 12582916
  61.6 6.9 %copy-start.28 = (bf16[512,128]{1,0:T(8,128)(2,1)S(1)}, bf16[512,128]{1,0:T(8,128)(2,1)}, u32[]{:S(2)}) copy-start(bf16[512,128]{1,0:T(8,128)(2,1)} %param.17) | copy-start | bytes 393220
  63.6 31.9 %collective-permute-start.1 = (bf16[128,384]{0,1:T(8,128)(2,1)S(1)}, bf16[128,384]{0,1:T(8,128)(2,1)S(1)}, u32[]{:S(2)}, u32[]{:S(2)}) collective-permute-start(bf16[128,384]{0,1:T(8,128)(2,1)S(1)} %get-tuple-element.10), channel_id=1, source_target_pairs={{2,0},{4,2},{6,4},{8,6},{10,8},{12,10},{14,12},{16,14},{18,16},{20... | collective-permute-start | bytes 294920 | tf_op jit(solution)/shard_map/ppermute | solution.py:26
  64.9 31.0 %collective-permute-start = (bf16[128,384]{0,1:T(8,128)(2,1)S(1)}, bf16[128,384]{0,1:T(8,128)(2,1)}, u32[]{:S(2)}, u32[]{:S(2)}) collective-permute-start(bf16[128,384]{0,1:T(8,128)(2,1)S(1)} %get-tuple-element.9), channel_id=1, source_target_pairs={{0,2},{2,4},{4,6},{6,8},{8,10},{10,12},{12,14},{14,16},{16,18},{18... | collective-permute-start | bytes 294920 | tf_op jit(solution)/shard_map/ppermute | solution.py:23
  88.1 5.7 %copy-start.10 = (pred[128,384]{0,1:T(8,128)(4,1)}, pred[128,384]{0,1:T(8,128)(4,1)S(1)}, u32[]{:S(2)}) copy-start(pred[128,384]{0,1:T(8,128)(4,1)S(1)} %fusion.50) | copy-start | bytes 147460
  90.1 5.7 %copy-start.12 = (pred[128,384]{0,1:T(8,128)(4,1)}, pred[128,384]{0,1:T(8,128)(4,1)S(1)}, u32[]{:S(2)}) copy-start(pred[128,384]{0,1:T(8,128)(4,1)S(1)} %fusion.48) | copy-start | bytes 147460
  92.1 4.8 %copy-start.15 = (pred[128,384]{0,1:T(8,128)(4,1)}, pred[128,384]{0,1:T(8,128)(4,1)S(1)}, u32[]{:S(2)}) copy-start(pred[128,384]{0,1:T(8,128)(4,1)S(1)} %fusion.46) | copy-start | bytes 147460
  97.7 4.0 %copy-start.4 = (f32[4,128,384]{1,2,0:T(8,128)S(1)}, f32[4,128,384]{1,2,0:T(8,128)}, u32[]{:S(2)}) copy-start(f32[4,128,384]{1,2,0:T(8,128)} %get-tuple-element.44) | copy-start | bytes 2359300
  101.6 3.4 %copy-start.7 = (f32[4,128,384]{1,2,0:T(8,128)S(1)}, f32[4,128,384]{1,2,0:T(8,128)}, u32[]{:S(2)}) copy-start(f32[4,128,384]{1,2,0:T(8,128)} %get-tuple-element.38) | copy-start | bytes 2359300
  101.6 3.4 %copy-start.13 = (pred[128,384]{0,1:T(8,128)(4,1)S(1)}, pred[128,384]{0,1:T(8,128)(4,1)}, u32[]{:S(2)}) copy-start(pred[128,384]{0,1:T(8,128)(4,1)} %copy-done.12) | copy-start | bytes 147460
  101.7 3.4 %copy-start.50 = (f32[4,128]{1,0:T(4,128)S(1)}, f32[4,128]{1,0:T(4,128)}, u32[]{:S(2)}) copy-start(f32[4,128]{1,0:T(4,128)} %get-tuple-element.18) | copy-start | bytes 6148
  101.7 3.6 %copy-start.8 = (f32[4,128,384]{1,2,0:T(8,128)S(1)}, f32[4,128,384]{1,2,0:T(8,128)}, u32[]{:S(2)}) copy-start(f32[4,128,384]{1,2,0:T(8,128)} %get-tuple-element.36) | copy-start | bytes 2359300
  101.7 3.6 %copy-start.16 = (pred[128,384]{0,1:T(8,128)(4,1)S(1)}, pred[128,384]{0,1:T(8,128)(4,1)}, u32[]{:S(2)}) copy-start(pred[128,384]{0,1:T(8,128)(4,1)} %copy-done.15) | copy-start | bytes 147460
  101.7 3.6 %copy-start.48 = (f32[4,128]{1,0:T(4,128)S(1)}, f32[4,128]{1,0:T(4,128)}, u32[]{:S(2)}) copy-start(f32[4,128]{1,0:T(4,128)} %get-tuple-element.17) | copy-start | bytes 6148
  101.7 3.8 %copy-start.3 = (f32[4,128,384]{1,2,0:T(8,128)S(1)}, f32[4,128,384]{1,2,0:T(8,128)}, u32[]{:S(2)}) copy-start(f32[4,128,384]{1,2,0:T(8,128)} %get-tuple-element.46) | copy-start | bytes 2359300
  101.7 3.8 %copy-start.52 = (f32[4,128]{1,0:T(4,128)S(1)}, f32[4,128]{1,0:T(4,128)}, u32[]{:S(2)}) copy-start(f32[4,128]{1,0:T(4,128)} %get-tuple-element.22) | copy-start | bytes 6148
  102.7 2.9 %copy-start.31 = (f32[4,128]{1,0:T(4,128)S(1)}, f32[4,128]{1,0:T(4,128)}, u32[]{:S(2)}) copy-start(f32[4,128]{1,0:T(4,128)} %get-tuple-element.45) | copy-start | bytes 6148
  102.7 2.9 %copy-start.33 = (f32[4,128]{1,0:T(4,128)S(1)}, f32[4,128]{1,0:T(4,128)}, u32[]{:S(2)}) copy-start(f32[4,128]{1,0:T(4,128)} %get-tuple-element.43) | copy-start | bytes 6148
  102.7 2.9 %copy-start.35 = (f32[4,128]{1,0:T(4,128)S(1)}, f32[4,128]{1,0:T(4,128)}, u32[]{:S(2)}) copy-start(f32[4,128]{1,0:T(4,128)} %get-tuple-element.41) | copy-start | bytes 6148
  102.7 2.9 %copy-start.37 = (f32[4,128]{1,0:T(4,128)S(1)}, f32[4,128]{1,0:T(4,128)}, u32[]{:S(2)}) copy-start(f32[4,128]{1,0:T(4,128)} %get-tuple-element.39) | copy-start | bytes 6148
  102.7 2.9 %copy-start.39 = (f32[4,128]{1,0:T(4,128)S(1)}, f32[4,128]{1,0:T(4,128)}, u32[]{:S(2)}) copy-start(f32[4,128]{1,0:T(4,128)} %get-tuple-element.37) | copy-start | bytes 6148
  102.8 2.9 %copy-start.41 = (f32[4,128]{1,0:T(4,128)S(1)}, f32[4,128]{1,0:T(4,128)}, u32[]{:S(2)}) copy-start(f32[4,128]{1,0:T(4,128)} %get-tuple-element.35) | copy-start | bytes 6148
  102.8 2.9 %copy-start.55 = (f32[4]{0:T(128)S(1)}, f32[4]{0:T(128)}, u32[]{:S(2)}) copy-start(f32[4]{0:T(128)} %param.15) | copy-start | bytes 52
  110.5 5.3 %copy-start.6 = (f32[4,128,384]{1,2,0:T(8,128)S(1)}, f32[4,128,384]{1,2,0:T(8,128)}, u32[]{:S(2)}) copy-start(f32[4,128,384]{1,2,0:T(8,128)} %get-tuple-element.40) | copy-start | bytes 2359300
  110.5 5.3 %copy-start.11 = (pred[128,384]{0,1:T(8,128)(4,1)S(1)}, pred[128,384]{0,1:T(8,128)(4,1)}, u32[]{:S(2)}) copy-start(pred[128,384]{0,1:T(8,128)(4,1)} %copy-done.10) | copy-start | bytes 147460
  114.2 4.8 %copy-start.14 = (pred[128,384]{0,1:T(8,128)(4,1)S(1)}, pred[128,384]{0,1:T(8,128)(4,1)}, u32[]{:S(2)}) copy-start(pred[128,384]{0,1:T(8,128)(4,1)} %copy-done.12) | copy-start | bytes 147460
  114.2 4.8 %copy-start.51 = (f32[4,128]{1,0:T(4,128)S(1)}, f32[4,128]{1,0:T(4,128)}, u32[]{:S(2)}) copy-start(f32[4,128]{1,0:T(4,128)} %get-tuple-element.18) | copy-start | bytes 6148
  114.2 4.8 %copy-start.58 = (f32[4,128]{1,0:T(4,128)S(1)}, f32[4,128]{1,0:T(4,128)}, u32[]{:S(2)}) copy-start(f32[4,128]{1,0:T(4,128)} %get-tuple-element.27) | copy-start | bytes 6148
  117.4 5.3 %copy-start.9 = (f32[4,128,384]{1,2,0:T(8,128)S(1)}, f32[4,128,384]{1,2,0:T(8,128)}, u32[]{:S(2)}) copy-start(f32[4,128,384]{1,2,0:T(8,128)} %get-tuple-element.36) | copy-start | bytes 2359300
  117.4 5.3 %copy-start.17 = (pred[128,384]{0,1:T(8,128)(4,1)S(1)}, pred[128,384]{0,1:T(8,128)(4,1)}, u32[]{:S(2)}) copy-start(pred[128,384]{0,1:T(8,128)(4,1)} %copy-done.15) | copy-start | bytes 147460
  117.4 5.3 %copy-start.49 = (f32[4,128]{1,0:T(4,128)S(1)}, f32[4,128]{1,0:T(4,128)}, u32[]{:S(2)}) copy-start(f32[4,128]{1,0:T(4,128)} %get-tuple-element.17) | copy-start | bytes 6148
  117.4 5.3 %copy-start.57 = (f32[4,128]{1,0:T(4,128)S(1)}, f32[4,128]{1,0:T(4,128)}, u32[]{:S(2)}) copy-start(f32[4,128]{1,0:T(4,128)} %get-tuple-element.26) | copy-start | bytes 6148
  121.1 3.5 %copy-start.19 = (pred[128,384]{0,1:T(8,128)(4,1)S(1)}, pred[128,384]{0,1:T(8,128)(4,1)}, u32[]{:S(2)}) copy-start(pred[128,384]{0,1:T(8,128)(4,1)} %copy-done.18) | copy-start | bytes 147460
  121.1 3.5 %copy-start.47 = (f32[4,128]{1,0:T(4,128)S(1)}, f32[4,128]{1,0:T(4,128)}, u32[]{:S(2)}) copy-start(f32[4,128]{1,0:T(4,128)} %copy-done.46) | copy-start | bytes 6148
  121.1 3.5 %copy-start.56 = (f32[4,128]{1,0:T(4,128)S(1)}, f32[4,128]{1,0:T(4,128)}, u32[]{:S(2)}) copy-start(f32[4,128]{1,0:T(4,128)} %get-tuple-element.16) | copy-start | bytes 6148
  123.6 3.5 %copy-start.27 = (bf16[128,256]{1,0:T(8,128)(2,1)S(1)}, bf16[128,256]{1,0:T(8,128)(2,1)}, u32[]{:S(2)}) copy-start(bf16[128,256]{1,0:T(8,128)(2,1)} %copy.37) | copy-start | bytes 196612
  124.6 3.2 %copy-start.26 = (bf16[128,256]{1,0:T(8,128)(2,1)S(1)}, bf16[128,256]{1,0:T(8,128)(2,1)}, u32[]{:S(2)}) copy-start(bf16[128,256]{1,0:T(8,128)(2,1)} %copy.38) | copy-start | bytes 196612
  124.6 3.8 %copy-start.25 = (bf16[128,256]{1,0:T(8,128)(2,1)S(1)}, bf16[128,256]{1,0:T(8,128)(2,1)}, u32[]{:S(2)}) copy-start(bf16[128,256]{1,0:T(8,128)(2,1)} %copy.39) | copy-start | bytes 196612
  124.6 4.4 %copy-start.24 = (bf16[128,256]{1,0:T(8,128)(2,1)S(1)}, bf16[128,256]{1,0:T(8,128)(2,1)}, u32[]{:S(2)}) copy-start(bf16[128,256]{1,0:T(8,128)(2,1)} %copy.40) | copy-start | bytes 196612
  124.7 5.0 %copy-start.23 = (bf16[128,256]{1,0:T(8,128)(2,1)S(1)}, bf16[128,256]{1,0:T(8,128)(2,1)}, u32[]{:S(2)}) copy-start(bf16[128,256]{1,0:T(8,128)(2,1)} %copy.41) | copy-start | bytes 196612
  124.7 5.6 %copy-start.22 = (bf16[128,256]{1,0:T(8,128)(2,1)S(1)}, bf16[128,256]{1,0:T(8,128)(2,1)}, u32[]{:S(2)}) copy-start(bf16[128,256]{1,0:T(8,128)(2,1)} %copy.42) | copy-start | bytes 196612
  124.7 9.9 %copy-start.21 = (bf16[128,384]{0,1:T(8,128)(2,1)S(1)}, bf16[128,384]{0,1:T(8,128)(2,1)}, u32[]{:S(2)}) copy-start(bf16[128,384]{0,1:T(8,128)(2,1)} %copy-done.20) | copy-start | bytes 294916
  130.9 12.0 %all-to-all-start = ((bf16[2,512,256]{2,1,0:T(8,128)(2,1)}), bf16[2,512,256]{2,1,0:T(8,128)(2,1)S(1)}, u32[]{:S(2)}, u32[]{:S(2)}) async-start(bf16[2,512,256]{2,1,0:T(8,128)(2,1)} %bitcast.49), calls=%async_computation | async-start | bytes 1048576 | tf_op jit(solution)/shard_map/all_to_all | solution.py:132
  142.9 11.1 %all-to-all-start.1 = ((bf16[2,512,256]{1,2,0:T(8,128)(2,1)}), bf16[2,512,256]{1,2,0:T(8,128)(2,1)S(1)}, u32[]{:S(2)}, u32[]{:S(2)}) async-start(bf16[2,512,256]{1,2,0:T(8,128)(2,1)} %bitcast.149), calls=%async_computation.1 | async-start | bytes 1048576 | tf_op jit(solution)/shard_map/all_to_all | solution.py:133
  (21 other events, 26.9 us)
Sparse Core Ops, SparseCore 0:
  76.0 49.8 all-gather.1
where the time goes:
time: 168 us; the launch traced here: 167 us
  blocking collectives  50.8 us (30%)
  matrix products  37.6 us (22%)
  other arithmetic  22.2 us (13%)
  local copies, waits for them, and re-layouts  19.4 us (12%)
  between operations  14.5 us (9%)
  starting transfers between devices  12.2 us (7%)
  waiting for transfers between devices  10.2 us (6%)
    all_gather x1, blocking collectives, body(): lax.all_gather(key_cols, 'sp', axis=0, tiled=True)  24.6 us
    all_gather x1, blocking collectives, body(): lax.all_gather(value_cols, 'sp', axis=0, tiled=True)  18.9 us
    dot_general x8, matrix products, body(): jnp.einsum('hij,jd->ihd', weights, values, preferred_element_type=jnp.flo...  11.9 us
    dot_general x8, matrix products, body(): jnp.einsum('ihd,jd->hij', queries, keys, preferred_element_type=jnp.float32)  11.9 us
    convert_element_type x8, local copies, waits for them, and re-layouts, body(): results.append(result.reshape(QB, local_heads * HEAD).astype(jnp.bfloat16))  10.6 us
    all_to_all x1, waiting for transfers between devices, body(): lax.all_to_all(pooled, 'tp', split_axis=0, concat_axis=1, tiled=True)  7.42 us
    all_gather x1, blocking collectives, body(): out_rows_all = lax.all_gather(w_out, 'tp', axis=0, tiled=True)  7.31 us
    dot_general x1, matrix products, body(): jnp.dot(joined, lax.all_gather(out_rows_all, 'sp', axis=1, tiled=True), p...  5.88 us
  transfers between devices with their start and end apart: 5, of which 2 were waited for; matrix products, arithmetic and copies ran while one was open for 35% of the time, Pallas kernels for 0%

commit v1 on v0

--- a/solution.py
+++ b/solution.py
@@ -1,6 +1,11 @@
+import functools
+
 import jax
 import jax.numpy as jnp
+import numpy as np
 from jax import lax
+from jax.experimental import pallas as pl
+from jax.experimental.pallas import tpu as pltpu
 from jax.sharding import PartitionSpec as P
 
 HEAD = 64
@@ -48,7 +53,7 @@
     )
 
 
-def body(tokens, norm_gain, w_query, w_key, w_value, w_pool_in, sink_logit, pool_scale, w_out):
+def plain_body(tokens, norm_gain, w_query, w_key, w_value, w_pool_in, sink_logit, pool_scale, w_out):
     local_rows = tokens.shape[0]
     seq_total = local_rows * lax.axis_size("sp")
     offset = lax.axis_index("sp") * local_rows
@@ -142,6 +147,456 @@
     return projected.astype(jnp.bfloat16)
 
 
+LANES = 128
+ROW_TILE = 256
+BF16 = jnp.bfloat16
+F32 = jnp.float32
+
+
+def whole():
+    return pl.BlockSpec(memory_space=pltpu.VMEM)
+
+
+def scalars():
+    return pl.BlockSpec(memory_space=pltpu.SMEM)
+
+
+def aligned(start, size=QB):
+    return pl.ds(pl.multiple_of(start, QB), size)
+
+
+def cost(flops, moved=0):
+    return pl.CostEstimate(flops=flops, bytes_accessed=moved, transcendentals=0)
+
+
+def rope_lanes(values, cosine, sine):
+    lane = lax.broadcasted_iota(jnp.int32, values.shape, 1)
+    swapped = jnp.where(
+        lane % HEAD < HEAD // 2,
+        pltpu.roll(values, LANES - HEAD // 2, 1),
+        pltpu.roll(values, HEAD // 2, 1),
+    )
+    return values * cosine + swapped * sine
+
+
+def project_kernel(tokens, gain, w_query, w_pool, cosine, sine, normed, query, pool):
+    for row in range(0, tokens.shape[0], 16):
+        rows = slice(row, row + 16)
+        values = tokens[rows, :].astype(F32)
+        centred = values - jnp.mean(values, axis=-1, keepdims=True)
+        spread = jnp.mean(centred * centred, axis=-1, keepdims=True)
+        normed[rows, :] = (centred * lax.rsqrt(spread + 1e-06) * gain[...]).astype(BF16)
+    left = normed[...]
+    pool[...] = jnp.dot(left, w_pool[...], preferred_element_type=F32).astype(BF16)
+    products = jnp.dot(left, w_query[...], preferred_element_type=F32)
+    for lane in range(0, products.shape[1], LANES):
+        turned = rope_lanes(products[:, lane : lane + LANES], cosine[...], sine[...])
+        query[:, lane : lane + LANES] = turned.astype(BF16) * HEAD ** (-0.5)
+
+
+def key_value_kernel(places, normed, *refs):
+    pieces, (cosine, sine, pool_head, pool_tail, key_value, head, tail, weight) = refs[:4], refs[4:]
+    step, last = pl.program_id(0), pl.num_programs(0) - 1
+    depth = pieces[0].shape[1]
+
+    @pl.when(step == 0)
+    def _():
+        for index, piece in enumerate(pieces):
+            for slot in range(piece.shape[0]):
+                place = places[index * piece.shape[0] + slot]
+                weight[pl.ds(pl.multiple_of(place * depth, depth), depth), :] = piece[slot]
+
+    products = jnp.dot(normed[...], weight[...], preferred_element_type=F32)
+    lane = lax.broadcasted_iota(jnp.int32, products.shape, 1)
+    turned = rope_lanes(products, cosine[...], sine[...])
+    result = jnp.where(lane < HEAD, turned, products).astype(BF16)
+    key_value[...] = result
+    edge = pool_head.shape[0]
+    for when, out, rows, pool in (
+        (step == 0, head, result[:WINDOW], pool_head),
+        (step == last, tail, result[-WINDOW:], pool_tail),
+    ):
+
+        @pl.when(when)
+        def _(out=out, rows=rows, pool=pool):
+            out[:WINDOW, :] = rows
+            for group in range(pool.shape[1] // LANES):
+                start = WINDOW + group * edge
+                out[start : start + edge, :] = pool[:, group * LANES : (group + 1) * LANES]
+
+
+def pool_kernel(info, pool, low, high, scale, out, wide):
+    rows, channels = pool.shape
+    edge = (wide.shape[0] - rows) // 2
+    chunks, chunk = out.shape[0], out.shape[1]
+    place, total = info[0], info[2] * rows
+    tp = info[1]
+    groups = channels // LANES
+    for group in range(groups):
+        start = WINDOW + group * edge
+        lanes = slice(group * LANES, (group + 1) * LANES)
+        wide[:edge, lanes] = low[start : start + edge, :]
+        wide[edge + rows :, lanes] = high[start : start + edge, :]
+    wide[edge : edge + rows, :] = pool[...]
+    span = QB + 2 * edge
+    row = lax.broadcasted_iota(jnp.int32, (QB, span), 0) + edge
+    column = lax.broadcasted_iota(jnp.int32, (QB, span), 1)
+    bands, reaches = [], []
+    for group in range(groups):
+        reach = lax.shift_left(jnp.int32(1), tp * groups + group)
+        inside = (column >= row - reach) & (column < row + reach)
+        bands.append(jnp.where(inside, 1.0, 0.0).astype(BF16))
+        reaches.append(reach)
+    for step in range(chunks):
+        target = lax.bitwise_xor(tp, step)
+        for block in range(0, chunk, QB):
+            start = target * chunk + block
+            position = place * rows + start + lax.broadcasted_iota(jnp.int32, (QB, 1), 0)
+            for group in range(groups):
+                lanes = slice(group * LANES, (group + 1) * LANES)
+                sums = jnp.dot(
+                    bands[group],
+                    wide[aligned(start, span), lanes],
+                    preferred_element_type=F32,
+                )
+                counted = jnp.minimum(position + reaches[group], total) - jnp.maximum(
+                    position - reaches[group], 0
+                )
+                mean = sums * (1.0 / counted.astype(F32))
+                own = pool[aligned(start), lanes].astype(F32)
+                out[step, block : block + QB, lanes] = ((mean - own) * scale[:, lanes]).astype(BF16)
+
+
+def attend_kernel(step, info, sink, query, key_value, low, high, out, keys, values):
+    chunk = out.shape[0]
+    place, tp, count = info[0], info[1], info[2]
+    target = lax.bitwise_xor(tp, step)
+    chunks = query.shape[0] // chunk
+    begin = pl.multiple_of(target * chunk, chunk)
+
+    def put(start, rows):
+        wide = rows.astype(F32)
+        lane = lax.broadcasted_iota(jnp.int32, wide.shape, 1)
+        turned = pltpu.roll(wide, HEAD, 1)
+        for side, (key, value) in enumerate(((wide, turned), (turned, wide))):
+            first = lane < HEAD if side == 0 else lane >= HEAD
+            keys[side, start : start + rows.shape[0], :] = jnp.where(first, key, 0.0).astype(BF16)
+            values[side, start : start + rows.shape[0], :] = jnp.where(first, value, 0.0).astype(
+                BF16
+            )
+
+    for block in range(0, chunk, QB):
+        put(WINDOW + block, key_value[aligned(begin + block), :])
+    before = key_value[aligned(jnp.maximum(begin - WINDOW, 0)), :]
+    put(0, jnp.where(target == 0, low[:WINDOW, :], before))
+    after_start = jnp.minimum(begin + chunk, query.shape[0] - WINDOW)
+    after = key_value[aligned(after_start), :]
+    put(WINDOW + chunk, jnp.where(target == chunks - 1, high[:WINDOW, :], after))
+
+    row = lax.broadcasted_iota(jnp.int32, (QB, WINDOW), 0)
+    column = lax.broadcasted_iota(jnp.int32, (QB, WINDOW), 1)
+    at_start = (place == 0) & (target == 0)
+    at_end = (place == count - 1) & (target == chunks - 1)
+    for block in range(0, chunk, QB):
+        low_ok, high_ok = column >= row, column <= row
+        if block == 0:
+            low_ok = low_ok & jnp.logical_not(at_start)
+        if block == chunk - QB:
+            high_ok = high_ok & jnp.logical_not(at_end)
+        for pair in range(query.shape[1] // LANES):
+            lanes = slice(pair * LANES, (pair + 1) * LANES)
+            queries = query[aligned(begin + block), lanes]
+            result = None
+            for side in range(2):
+                scores = lax.dot_general(
+                    queries,
+                    keys[side, block : block + QB + 2 * WINDOW, :],
+                    (((1,), (1,)), ((), ())),
+                    preferred_element_type=F32,
+                )
+                parts = (
+                    jnp.where(low_ok, scores[:, :WINDOW], NEG_BIG),
+                    scores[:, WINDOW : WINDOW + QB],
+                    jnp.where(high_ok, scores[:, WINDOW + QB :], NEG_BIG),
+                )
+                logit = sink[2 * pair + side]
+                top = jnp.maximum(jnp.maximum(parts[0], parts[1]), parts[2])
+                top = jnp.maximum(jnp.max(top, axis=-1, keepdims=True), logit)
+                expo = [jnp.exp(part - top) for part in parts]
+                total = jnp.sum(expo[0] + expo[1] + expo[2], axis=-1, keepdims=True)
+                inverse = 1.0 / (total + jnp.exp(logit - top))
+                weights = jnp.concatenate([(part * inverse).astype(BF16) for part in expo], axis=1)
+                part = jnp.dot(
+                    weights,
+                    values[side, block : block + QB + 2 * WINDOW, :],
+                    preferred_element_type=F32,
+                )
+                result = part if result is None else result + part
+            out[block : block + QB, lanes] = result.astype(BF16)
+
+
+def output_kernel(parts, table, info, *refs):
+    attended, pooled = refs[:parts], refs[parts : 2 * parts]
+    sources, out = refs[2 * parts : 2 * parts + 4], refs[2 * parts + 4]
+    weight, joined, staged, in_sem, out_sem = refs[2 * parts + 5 :]
+    loads = [
+        pltpu.make_async_copy(source, weight.at[index], in_sem.at[index])
+        for index, source in enumerate(sources)
+    ]
+    order = (0, 2, 1, 3)
+    for index in order:
+        loads[index].start()
+    tp = info[1]
+    width = attended[0].shape[1]
+    for step in range(parts):
+        owner = lax.bitwise_xor(tp, step)
+        for half, part in enumerate((attended[step], pooled[step])):
+            start = pl.multiple_of((half * parts + owner) * width, LANES)
+            joined[:, pl.ds(start, width)] = part[...]
+    depth, lanes = weight.shape[2], weight.shape[3]
+    blocks = weight.shape[1] // parts
+    stores = []
+    for index in order:
+        loads[index].wait()
+        for block in range(0, blocks, 2):
+            total = None
+            entries = [(index * blocks + block + side) * (parts + 1) for side in range(2)]
+            for step in range(parts):
+                start = pl.multiple_of(lax.bitwise_xor(tp, step) * depth, LANES)
+                right = jnp.concatenate(
+                    [weight[index, table[entry + 1 + step]] for entry in entries], axis=1
+                )
+                product = jnp.dot(
+                    joined[:, pl.ds(start, depth)], right, preferred_element_type=F32
+                )
+                total = product if total is None else total + product
+            for side in range(2):
+                number = index * blocks + block + side
+                staged[number] = total[:, side * lanes : (side + 1) * lanes].astype(BF16)
+                start = pl.multiple_of(table[entries[side]] * lanes, LANES)
+                store = pltpu.make_async_copy(
+                    staged.at[number], out.at[:, pl.ds(start, lanes)], out_sem.at[number]
+                )
+                store.start()
+                stores.append(store)
+    for store in stores:
+        store.wait()
+
+
+def exchange_orders(sp_count, tp_count):
+    sp_bits = [tp_count << bit for bit in range(1, sp_count.bit_length() - 1)][::-1]
+    tp_bits = [1 << bit for bit in range(tp_count.bit_length() - 1)]
+    for bits in (sp_bits, sp_bits[:1] + tp_bits + sp_bits[1:]):
+        yield bits, bits[-1:] + bits[:-1]
+
+
+def slot_masks(bits):
+    masks = [0]
+    for bit in bits:
+        masks = masks + [mask ^ bit for mask in masks]
+    return masks
+
+
+def doubled(block, orders, sp_count, tp_count):
+    even, odd = orders
+    devices = range(sp_count * tp_count)
+
+    def send(array, masks):
+        pairs = [(i, i ^ masks[(i // tp_count) & 1]) for i in devices]
+        return lax.ppermute(array, ("sp", "tp"), pairs)
+
+    held = block[None]
+    for masks in zip(even[:-1], odd[:-1]):
+        held = jnp.concatenate([held, send(held, masks)], axis=0)
+    core = (tp_count, tp_count)
+    other = send(held, core)
+    came = send(held, (even[-1], odd[-1]))
+    return held, came, other, send(came, core)
+
+
+def fast_body(tokens, norm_gain, w_query, w_key, w_value, w_pool_in, sink_logit, pool_scale, w_out):
+    sp_count, tp_count = lax.axis_size("sp"), lax.axis_size("tp")
+    local_rows, width = tokens.shape
+    sp_place, tp_place = lax.axis_index("sp"), lax.axis_index("tp")
+    local_heads = w_query.shape[1] // HEAD
+    heads_width, local_pool = w_query.shape[1], w_pool_in.shape[1]
+    chunk = local_rows // tp_count
+    kv_orders, out_orders = exchange_orders(sp_count, tp_count)
+
+    key_head = tp_place * local_heads // (QH // KVH)
+    kv_block = jnp.concatenate(
+        [lax.dynamic_slice_in_dim(w, key_head * HEAD, HEAD, 1) for w in (w_key, w_value)], axis=1
+    )
+    kv_pieces = doubled(kv_block, kv_orders, sp_count, tp_count)
+    out_pieces = doubled(w_out, out_orders, sp_count, tp_count)
+
+    odd = sp_place % 2
+    info = jnp.stack([sp_place, tp_place, jnp.int32(sp_count)]).astype(jnp.int32)
+
+    def by_class(pairs):
+        return jnp.where(odd == 0, jnp.array(pairs[0], jnp.int32), jnp.array(pairs[1], jnp.int32))
+
+    kv_tables, out_tables = [], []
+    for flip in range(2):
+        for late in range(2):
+            rows = []
+            for order in (kv_orders if flip == 0 else kv_orders[::-1]):
+                extra = order[-1] if late else 0
+                rows.append([((mask ^ extra) // tp_count) ^ flip for mask in slot_masks(order[:-1])])
+            kv_tables.append(by_class(rows) ^ sp_place)
+            rows = []
+            for order in (out_orders if flip == 0 else out_orders[::-1]):
+                extra = order[-1] if late else 0
+                masks = [mask ^ extra for mask in slot_masks(order[:-1])]
+                found = {}
+                for slot, mask in enumerate(masks):
+                    found.setdefault(mask // tp_count, {})[mask % tp_count] = slot
+                rows.append(
+                    [[delta ^ flip] + [slots[t] for t in range(tp_count)] for delta, slots in found.items()]
+                )
+            picked = by_class(rows)
+            out_tables.append(picked ^ jnp.pad(sp_place[None], (0, tp_count))[None, :])
+    kv_table = jnp.concatenate(kv_tables)
+    out_table = jnp.concatenate(out_tables).reshape(-1)
+
+    half = HEAD // 2
+    inverse = 10000.0 ** (-jnp.arange(half, dtype=F32) / half)
+    inverse = jnp.tile(inverse, LANES // half)
+    positions = (sp_place * local_rows + jnp.arange(local_rows)).astype(F32)
+    angles = positions[:, None] * inverse[None, :]
+    cosine = jnp.cos(angles)
+    sign = jnp.where(jnp.arange(LANES) % HEAD < half, -1.0, 1.0).astype(F32)
+    sine = jnp.sin(angles) * sign[None, :]
+
+    def rows_of(columns, size=ROW_TILE):
+        return pl.BlockSpec((size, columns), lambda i: (i, 0))
+
+    def fixed(shape, index=0):
+        return pl.BlockSpec(shape, lambda i: (index,) + (0,) * (len(shape) - 1))
+
+    tiles = local_rows // ROW_TILE
+    normed, query, pool_in = pl.pallas_call(
+        project_kernel,
+        grid=(tiles,),
+        in_specs=[
+            rows_of(width),
+            fixed((1, width)),
+            fixed(w_query.shape),
+            fixed(w_pool_in.shape),
+            rows_of(LANES),
+            rows_of(LANES),
+        ],
+        out_specs=[rows_of(width), rows_of(heads_width), rows_of(local_pool)],
+        out_shape=[
+            jax.ShapeDtypeStruct(tokens.shape, BF16),
+            jax.ShapeDtypeStruct((local_rows, heads_width), BF16),
+            jax.ShapeDtypeStruct((local_rows, local_pool), BF16),
+        ],
+        cost_estimate=cost(2 * local_rows * width * (heads_width + local_pool)),
+        name="project",
+    )(tokens, norm_gain[None, :], w_query, w_pool_in, cosine, sine)
+
+    edge = 2 * (POOL_SPANS[-1] // 2)
+    payload = (WINDOW + edge * (local_pool // LANES), LANES)
+    key_value, head, tail = pl.pallas_call(
+        key_value_kernel,
+        grid=(tiles,),
+        in_specs=[scalars(), rows_of(width)]
+        + [fixed(piece.shape) for piece in kv_pieces]
+        + [
+            rows_of(LANES),
+            rows_of(LANES),
+            fixed((edge, local_pool)),
+            fixed((edge, local_pool), local_rows // edge - 1),
+        ],
+        out_specs=[rows_of(LANES), fixed(payload), fixed(payload)],
+        out_shape=[
+            jax.ShapeDtypeStruct((local_rows, LANES), BF16),
+            jax.ShapeDtypeStruct(payload, BF16),
+            jax.ShapeDtypeStruct(payload, BF16),
+        ],
+        scratch_shapes=[pltpu.VMEM((width, LANES), BF16)],
+        cost_estimate=cost(2 * local_rows * width * LANES),
+        name="key_value",
+    )(kv_table, normed, *kv_pieces, cosine, sine, pool_in, pool_in)
+
+    forward = [(i, i + 1) for i in range(sp_count - 1)]
+    low = lax.ppermute(tail, "sp", forward)
+    high = lax.ppermute(head, "sp", [(target, source) for source, target in forward])
+
+    pooled = pl.pallas_call(
+        pool_kernel,
+        in_specs=[scalars()] + [whole()] * 4,
+        out_specs=whole(),
+        out_shape=jax.ShapeDtypeStruct((tp_count, chunk, local_pool), BF16),
+        scratch_shapes=[pltpu.VMEM((local_rows + 2 * edge, local_pool), BF16)],
+        cost_estimate=cost(2 * local_rows * local_pool * 160),
+        name="pool",
+    )(info, pool_in, low, high, pool_scale[None, :])
+
+    devices = range(tp_count)
+
+    def hand_over(part, step):
+        if step == 0:
+            return part
+        return lax.ppermute(part, "tp", [(i, i ^ step) for i in devices])
+
+    pooled_parts = [hand_over(pooled[step], step) for step in devices]
+
+    attended_parts = [None] * tp_count
+    for step in list(devices)[1:] + [0]:
+        attended = pl.pallas_call(
+            functools.partial(attend_kernel, step),
+            in_specs=[scalars(), scalars()] + [whole()] * 4,
+            out_specs=whole(),
+            out_shape=jax.ShapeDtypeStruct((chunk, heads_width), BF16),
+            scratch_shapes=[pltpu.VMEM((2, chunk + 2 * WINDOW, LANES), BF16)] * 2,
+            cost_estimate=cost(4 * chunk * 3 * WINDOW * LANES * local_heads),
+            name=f"attend{step}",
+        )(info, sink_logit, query, key_value, low, high)
+        attended_parts[step] = hand_over(attended, step)
+
+    columns = w_out.shape[1] * sp_count
+    return pl.pallas_call(
+        functools.partial(output_kernel, tp_count),
+        in_specs=[scalars(), scalars()]
+        + [whole()] * (2 * tp_count)
+        + [pl.BlockSpec(memory_space=pltpu.HBM)] * 4,
+        out_specs=pl.BlockSpec(memory_space=pltpu.HBM),
+        out_shape=jax.ShapeDtypeStruct((chunk, columns), BF16),
+        scratch_shapes=[
+            pltpu.VMEM((4,) + out_pieces[0].shape, BF16),
+            pltpu.VMEM((chunk, w_out.shape[0] * tp_count), BF16),
+            pltpu.VMEM((sp_count, chunk, w_out.shape[1]), BF16),
+            pltpu.SemaphoreType.DMA((4,)),
+            pltpu.SemaphoreType.DMA((sp_count,)),
+        ],
+        cost_estimate=cost(2 * chunk * columns * w_out.shape[0] * tp_count),
+        name="output",
+    )(out_table, info, *attended_parts, *pooled_parts, *out_pieces)
+
+
+def tiled(rows, w_query, w_pool_in, w_out):
+    counts = lax.axis_size("sp"), lax.axis_size("tp")
+    return (
+        all(count & (count - 1) == 0 for count in counts)
+        and counts[0] >= 8
+        and rows % (counts[1] * QB) == 0
+        and rows % ROW_TILE == 0
+        and w_query.shape[1] % LANES == 0
+        and w_pool_in.shape[1] % LANES == 0
+        and w_out.shape[1] % LANES == 0
+        and counts[1] * w_query.shape[1] == QH * HEAD
+    )
+
+
+def body(*args):
+    tokens, w_query, w_pool_in, w_out = args[0], args[2], args[5], args[8]
+    if tiled(tokens.shape[0], w_query, w_pool_in, w_out):
+        return fast_body(*args)
+    return plain_body(*args)
+
+
 def solution(mesh):
     in_specs = (
         P("sp", None),

time: 168 us -> 96.6 us (0.57)
  the two profiles are of different devices: /device:TPU:0 before, /device:TPU:8 now
where the time goes in v1:
time: 96.6 us; the launch traced here: 96.1 us
  Pallas kernels  33.6 us (35%)
  starting transfers between devices  27.6 us (29%)
  waiting for transfers between devices  21.4 us (22%)
  other arithmetic  7.54 us (8%)
  local copies, waits for them, and re-layouts  5.58 us (6%)
    ppermute x11, starting transfers between devices, send(): return lax.ppermute(array, ('sp', 'tp'), pairs)  18.9 us
    ppermute x11, waiting for transfers between devices, send(): return lax.ppermute(array, ('sp', 'tp'), pairs)  18.5 us
    pallas_call x2, Pallas kernels, fast_body(): pl.pallas_call(functools.partial(attend_kernel, step), in_specs=[scalars(...  11 us
    pallas_call x1, Pallas kernels, fast_body(): pl.pallas_call(project_kernel, grid=(tiles,), in_specs=[rows_of(width), f...  8.45 us
    pallas_call x1, Pallas kernels, fast_body(): pl.pallas_call(functools.partial(output_kernel, tp_count), in_specs=[scal...  6.35 us
    pallas_call x1, Pallas kernels, fast_body(): pl.pallas_call(key_value_kernel, grid=(tiles,), in_specs=[scalars(), rows...  5.29 us
    ppermute x1, starting transfers between devices, fast_body(): lax.ppermute(head, 'sp', [(target, source) for source, target in forward])  4.36 us
    mul x1, other arithmetic, fast_body(): sine = jnp.sin(angles) * sign[None, :]  3.06 us
  transfers between devices with their start and end apart: 15, of which 7 were waited for; matrix products, arithmetic and copies ran while one was open for 10% of the time, Pallas kernels for 28%

profile of v1, /device:TPU:8, one launch (start us, length us, event | category | flops | bytes accessed | tf_op | source)
XLA Modules:
  0.0 96.1 jit_solution(8978780086876371552)
XLA Ops:
  0.0 0.0 copy-start.22
  0.0 0.0 copy-start.15
  0.0 0.0 copy-start.16
  0.1 2.7 %collective-permute-start.9 = (bf16[1,512,128]{2,1,0:T(8,128)(2,1)}, bf16[1,512,128]{2,1,0:T(8,128)(2,1)S(1)}, u32[]{:S(2)}, u32[]{:S(2)}) collective-permute-start(bf16[1,512,128]{2,1,0:T(8,128)(2,1)} %bitcast.11), channel_id=1, source_target_pairs={{0,16},{1,17},{2,6},{3,7},{4,20},{5,21},{6,2},{7,3},{8,24},{9,25},... | collective-permute-start | bytes 393224 | tf_op jit(solution)/shard_map/ppermute | solution.py:406
  2.7 4.1 %collective-permute-done.9 = bf16[1,512,128]{2,1,0:T(8,128)(2,1)S(1)} collective-permute-done((bf16[1,512,128]{2,1,0:T(8,128)(2,1)}, bf16[1,512,128]{2,1,0:T(8,128)(2,1)S(1)}, u32[]{:S(2)}, u32[]{:S(2)}) %collective-permute-start.9) | collective-permute-done | bytes 131104 | tf_op jit(solution)/shard_map/ppermute | solution.py:406
  6.8 0.9 pad_maximum_fusion.2
  7.8 1.6 %collective-permute-start.10 = (bf16[2,512,128]{2,1,0:T(8,128)(2,1)S(1)}, bf16[2,512,128]{2,1,0:T(8,128)(2,1)S(1)}, u32[]{:S(2)}, u32[]{:S(2)}) collective-permute-start(bf16[2,512,128]{2,1,0:T(8,128)(2,1)S(1)} %pad_maximum_fusion.2), channel_id=1, source_target_pairs={{0,1},{1,0},{2,18},{3,19},{4,5},{5,4},{6,22},{7,23},{8,9},{9,8},{1... | collective-permute-start | bytes 786440 | tf_op jit(solution)/shard_map/ppermute | solution.py:406
  9.3 4.9 %collective-permute-done.10 = bf16[2,512,128]{2,1,0:T(8,128)(2,1)S(1)} collective-permute-done((bf16[2,512,128]{2,1,0:T(8,128)(2,1)S(1)}, bf16[2,512,128]{2,1,0:T(8,128)(2,1)S(1)}, u32[]{:S(2)}, u32[]{:S(2)}) %collective-permute-start.10) | collective-permute-done | bytes 262176 | tf_op jit(solution)/shard_map/ppermute | solution.py:406
  14.2 1.0 pad_maximum_fusion.1
  15.2 0.8 collective-permute-start.11
  15.9 0.9 constant_dynamic-slice_fusion
  16.8 0.1 maximum_bitcast_fusion
  16.9 2.7 %collective-permute-start = (bf16[1,128,128]{2,1,0:T(8,128)(2,1)S(1)}, bf16[1,128,128]{2,1,0:T(8,128)(2,1)S(1)}, u32[]{:S(2)}, u32[]{:S(2)}) collective-permute-start(bf16[1,128,128]{2,1,0:T(8,128)(2,1)S(1)} %maximum_bitcast_fusion), channel_id=1, source_target_pairs={{0,16},{1,17},{2,6},{3,7},{4,20},{5,21},{6,2},{7,3},{8,24},{9,25},... | collective-permute-start | bytes 98312 | tf_op jit(solution)/shard_map/ppermute | solution.py:406
  19.6 4.8 %collective-permute-done.11 = bf16[4,512,128]{2,1,0:T(8,128)(2,1)S(1)} collective-permute-done((bf16[4,512,128]{2,1,0:T(8,128)(2,1)S(1)}, bf16[4,512,128]{2,1,0:T(8,128)(2,1)S(1)}, u32[]{:S(2)}, u32[]{:S(2)}) %collective-permute-start.11) | collective-permute-done | bytes 524320 | tf_op jit(solution)/shard_map/ppermute | solution.py:406
  24.4 1.0 %pad_maximum_fusion.refs_4_ = bf16[8,512,128]{2,1,0:T(8,128)(2,1)S(1)} fusion(bf16[4,512,128]{2,1,0:T(8,128)(2,1)S(1)} %collective-permute-done.11, bf16[2,512,128]{2,1,0:T(8,128)(2,1)S(1)} %collective-permute-done.10, bf16[1,512,128]{2,1,0:T(8,128)(2,1)S(1)} %collective-permute-done.9, bf16[1,512,128]{2,1,0:T(8,128)(2,1)} %bitcast.14), kind=kLoop, calls=%fused_computation | loop fusion | flops 1572864 | bytes 2097152 | tf_op jit(solution)/shard_map/concatenate | solution.py:410
  25.4 1.6 %collective-permute-start.12 = (bf16[8,512,128]{2,1,0:T(8,128)(2,1)S(1)}, bf16[8,512,128]{2,1,0:T(8,128)(2,1)S(1)}, u32[]{:S(2)}, u32[]{:S(2)}) collective-permute-start(bf16[8,512,128]{2,1,0:T(8,128)(2,1)S(1)} %pad_maximum_fusion.refs_4_), channel_id=1, source_target_pairs={{0,4},{1,5},{2,10},{3,11},{4,0},{5,1},{6,14},{7,15},{8,12},{9,13},... | collective-permute-start | bytes 3145736 | tf_op jit(solution)/shard_map/ppermute | solution.py:406
  27.0 0.1 mul.35
  27.1 3.1 %fusion = (f32[1024,128]{1,0:T(8,128)}, f32[1024,128]{1,0:T(8,128)}) fusion(f32[128]{0:T(128)S(1)} %compare_select_fusion, f32[128]{0:T(128)S(1)} %mul.35, f32[1024]{0:T(1024)S(1)} %add_convert_fusion), kind=kLoop, calls=%fused_computation.3 | loop fusion | flops 262144 | bytes 1053696 | tf_op jit(solution)/shard_map/mul | solution.py:469
  30.2 1.7 %collective-permute-start.1 = (bf16[2,128,128]{2,1,0:T(8,128)(2,1)S(1)}, bf16[2,128,128]{2,1,0:T(8,128)(2,1)S(1)}, u32[]{:S(2)}, u32[]{:S(2)}) collective-permute-start(bf16[2,128,128]{2,1,0:T(8,128)(2,1)S(1)} %pad_maximum_fusion.4), channel_id=1, source_target_pairs={{0,8},{1,9},{2,18},{3,19},{4,12},{5,13},{6,22},{7,23},{8,0},{9,1},... | collective-permute-start | bytes 196616 | tf_op jit(solution)/shard_map/ppermute | solution.py:406
  31.9 3.3 %collective-permute-done.1 = bf16[2,128,128]{2,1,0:T(8,128)(2,1)S(1)} collective-permute-done((bf16[2,128,128]{2,1,0:T(8,128)(2,1)S(1)}, bf16[2,128,128]{2,1,0:T(8,128)(2,1)S(1)}, u32[]{:S(2)}, u32[]{:S(2)}) %collective-permute-start.1) | collective-permute-done | bytes 65568 | tf_op jit(solution)/shard_map/ppermute | solution.py:406
  35.2 0.6 collective-permute-start.2
  35.8 4.6 %collective-permute-start.3 = (bf16[4,128,128]{2,1,0:T(8,128)(2,1)S(1)}, bf16[4,128,128]{2,1,0:T(8,128)(2,1)S(1)}, u32[]{:S(2)}, u32[]{:S(2)}) collective-permute-start(bf16[4,128,128]{2,1,0:T(8,128)(2,1)S(1)} %pad_maximum_fusion.3.refs_0_), channel_id=1, source_target_pairs={{0,2},{1,3},{2,0},{3,1},{4,6},{5,7},{6,4},{7,5},{8,10},{9,11},{10,... | collective-permute-start | bytes 393224 | tf_op jit(solution)/shard_map/ppermute | solution.py:406
  40.4 1.3 %collective-permute-done.2.refs_1_ = bf16[4,128,128]{2,1,0:T(8,128)(2,1)S(1)} collective-permute-done((bf16[4,128,128]{2,1,0:T(8,128)(2,1)S(1)}, bf16[4,128,128]{2,1,0:T(8,128)(2,1)S(1)}, u32[]{:S(2)}, u32[]{:S(2)}) %collective-permute-start.2) | collective-permute-done | bytes 131104 | tf_op jit(solution)/shard_map/ppermute | solution.py:406
  41.7 2.4 %collective-permute-start.4 = (bf16[4,128,128]{2,1,0:T(8,128)(2,1)S(1)}, bf16[4,128,128]{2,1,0:T(8,128)(2,1)S(1)}, u32[]{:S(2)}, u32[]{:S(2)}) collective-permute-start(bf16[4,128,128]{2,1,0:T(8,128)(2,1)S(1)} %collective-permute-done.2.refs_1_), channel_id=1, source_target_pairs={{0,2},{1,3},{2,0},{3,1},{4,6},{5,7},{6,4},{7,5},{8,10},{9,11},{10,... | collective-permute-start | bytes 393224 | tf_op jit(solution)/shard_map/ppermute | solution.py:406
  44.1 0.5 collective-permute-start.14
  44.6 8.4 %project.1 = (bf16[1024,2048]{1,0:T(8,128)(2,1)}, bf16[1024,256]{1,0:T(8,128)(2,1)}, bf16[1024,256]{1,0:T(8,128)(2,1)}) custom-call(bf16[1024,2048]{1,0:T(8,128)(2,1)} %tokens.1, f32[1,2048]{1,0:T(1,128)} %bitcast.16, bf16[2048,256]{1,0:T(8,128)(2,1)} %w_query.1, bf16[2048,256]{1,0:T(8,128)(2,1)} %w_pool.1, f32[1024,128]{1,0:T(8,128)} %get-tuple-element.20.cosine.refs_4_, ...), custom_call_target="tpu_custom_call" | custom-call | flops 2147483648 | tf_op jit(solution)/shard_map/project/pallas_call | solution.py:478
  53.0 0.7 pad_add_fusion.2.places
  53.8 0.6 copy-done.3
  54.4 0.1 copy-done.4
  54.5 5.3 %key_value.1 = (bf16[1024,128]{1,0:T(8,128)(2,1)}, bf16[160,128]{1,0:T(8,128)(2,1)}, bf16[160,128]{1,0:T(8,128)(2,1)}) custom-call(s32[16]{0:T(128)} %pad_add_fusion.2.places, bf16[1024,2048]{1,0:T(8,128)(2,1)} %get-tuple-element.12.normed, bf16[4,128,128]{2,1,0:T(8,128)(2,1)} %copy-done.1, bf16[4,128,128]{2,1,0:T(8,128)(2,1)} %copy-done.2, ...), custom_call_target="tpu_custom_call" | custom-call | flops 536870912 | tf_op jit(solution)/shard_map/key_value/pallas_call | solution.py:501
  59.8 2.3 %collective-permute-start.5 = (bf16[160,128]{1,0:T(8,128)(2,1)}, bf16[160,128]{1,0:T(8,128)(2,1)S(1)}, u32[]{:S(2)}, u32[]{:S(2)}) collective-permute-start(bf16[160,128]{1,0:T(8,128)(2,1)} %get-tuple-element.15), channel_id=1, source_target_pairs={{0,2},{2,4},{4,6},{6,8},{8,10},{10,12},{12,14},{14,16},{16,18},{18... | collective-permute-start | bytes 122888 | tf_op jit(solution)/shard_map/ppermute | solution.py:524
  62.1 4.4 %collective-permute-start.6 = (bf16[160,128]{1,0:T(8,128)(2,1)}, bf16[160,128]{1,0:T(8,128)(2,1)S(1)}, u32[]{:S(2)}, u32[]{:S(2)}) collective-permute-start(bf16[160,128]{1,0:T(8,128)(2,1)} %get-tuple-element.16), channel_id=1, source_target_pairs={{2,0},{4,2},{6,4},{8,6},{10,8},{12,10},{14,12},{16,14},{18,16},{20... | collective-permute-start | bytes 122888 | tf_op jit(solution)/shard_map/ppermute | solution.py:525
  66.4 0.6 pad_add_fusion.1.info
  67.1 1.2 %collective-permute-done.6.high = bf16[160,128]{1,0:T(8,128)(2,1)S(1)} collective-permute-done((bf16[160,128]{1,0:T(8,128)(2,1)}, bf16[160,128]{1,0:T(8,128)(2,1)S(1)}, u32[]{:S(2)}, u32[]{:S(2)}) %collective-permute-start.6) | collective-permute-done | bytes 40992 | tf_op jit(solution)/shard_map/ppermute | solution.py:525
  68.2 0.6 copy-done.6
  68.8 2.5 %pool.1 = bf16[2,512,256]{2,1,0:T(8,128)(2,1)} custom-call(s32[3]{0:T(128)} %pad_add_fusion.1.info, bf16[1024,256]{1,0:T(8,128)(2,1)} %get-tuple-element.13.refs_6_.refs_7_.pool, bf16[160,128]{1,0:T(8,128)(2,1)} %copy-done.5, bf16[160,128]{1,0:T(8,128)(2,1)} %copy-done.6, f32[1,256]{1,0:T(1,128)} %bitcast.15), custom_call_target="tpu_custom_call" | custom-call | flops 83886080 | tf_op jit(solution)/shard_map/pool/pallas_call | solution.py:527
  71.4 1.8 %slice_bitcast_fusion = (bf16[512,256]{1,0:T(8,128)(2,1)S(1)}, bf16[512,256]{1,0:T(8,128)(2,1)}) fusion(bf16[2,512,256]{2,1,0:T(8,128)(2,1)} %pool.1), kind=kLoop, calls=%fused_computation.5 | loop fusion | bytes 1048576 | tf_op jit(solution)/shard_map/squeeze | solution.py:544
  73.1 1.5 %collective-permute-start.8 = (bf16[512,256]{1,0:T(8,128)(2,1)S(1)}, bf16[512,256]{1,0:T(8,128)(2,1)S(1)}, u32[]{:S(2)}, u32[]{:S(2)}) collective-permute-start(bf16[512,256]{1,0:T(8,128)(2,1)S(1)} %get-tuple-element.17), channel_id=1, source_target_pairs={{0,1},{1,0},{2,3},{3,2},{4,5},{5,4},{6,7},{7,6},{8,9},{9,8},{10,11... | collective-permute-start | bytes 786440 | tf_op jit(solution)/shard_map/ppermute | solution.py:542
  74.6 5.5 %attend1.1 = bf16[512,256]{1,0:T(8,128)(2,1)} custom-call(s32[3]{0:T(128)} %pad_add_fusion.1.info, f32[4]{0:T(128)} %sink.3, bf16[1024,256]{1,0:T(8,128)(2,1)} %get-tuple-element.11.query, bf16[1024,128]{1,0:T(8,128)(2,1)} %get-tuple-element.14.key_value, bf16[160,128]{1,0:T(8,128)(2,1)} %copy-done.5, bf16[160,128]{1,0:T(8,128)(2,1)} %copy-done.6), custom_call_target="tpu_custom_call" | custom-call | flops 402653184 | tf_op jit(solution)/shard_map/attend1/pallas_call | solution.py:548
  80.1 0.5 collective-permute-start.7
  80.7 0.1 select_xor_fusion.3
  80.8 0.1 pad_add_fusion
  80.9 0.1 copy.26
  80.9 0.7 reshape.27.table
  81.6 5.5 %attend0.1.refs_0_ = bf16[512,256]{1,0:T(8,128)(2,1)} custom-call(s32[3]{0:T(128)} %pad_add_fusion.1.info, f32[4]{0:T(128)} %sink.3, bf16[1024,256]{1,0:T(8,128)(2,1)} %get-tuple-element.11.query, bf16[1024,128]{1,0:T(8,128)(2,1)} %get-tuple-element.14.key_value, bf16[160,128]{1,0:T(8,128)(2,1)} %copy-done.5, bf16[160,128]{1,0:T(8,128)(2,1)} %copy-done.6), custom_call_target="tpu_custom_call" | custom-call | flops 402653184 | tf_op jit(solution)/shard_map/attend0/pallas_call | solution.py:548
  87.1 1.8 %collective-permute-done.7.refs_1_ = bf16[512,256]{1,0:T(8,128)(2,1)S(1)} collective-permute-done((bf16[512,256]{1,0:T(8,128)(2,1)}, bf16[512,256]{1,0:T(8,128)(2,1)S(1)}, u32[]{:S(2)}, u32[]{:S(2)}) %collective-permute-start.7) | collective-permute-done | bytes 262176 | tf_op jit(solution)/shard_map/ppermute | solution.py:542
  88.9 0.7 copy-done.25
  89.6 6.3 %output.1 = bf16[512,2048]{1,0:T(8,128)(2,1)} custom-call(s32[48]{0:T(128)} %reshape.27.table, s32[3]{0:T(128)} %pad_add_fusion.1.info, bf16[512,256]{1,0:T(8,128)(2,1)} %attend0.1.refs_0_, bf16[512,256]{1,0:T(8,128)(2,1)} %copy-done.25, bf16[512,256]{1,0:T(8,128)(2,1)} %get-tuple-element.18.refs_2_, bf16[512,256]{1,0:T(8,128)(2,1)} %copy-done.24, ...), custom_call_target="tpu_custom_call" | custom-call | flops 2147483648 | tf_op jit(solution)/shard_map/output/pallas_call | solution.py:560
  (63 shorter events, 0.2 us)
Async XLA Ops:
  0.0 31.8 %copy-start.19 = (s32[4]{0:T(128)S(1)}, s32[4]{0:T(128)}, u32[]{:S(2)}) copy-start(s32[4]{0:T(128)} %constant.100.clone) | copy-start | bytes 52
  0.0 31.8 %copy-start.20 = (s32[4]{0:T(128)S(1)}, s32[4]{0:T(128)}, u32[]{:S(2)}) copy-start(s32[4]{0:T(128)} %constant.101.clone) | copy-start | bytes 52
  0.0 31.8 %copy-start.21 = (s32[4]{0:T(128)S(1)}, s32[4]{0:T(128)}, u32[]{:S(2)}) copy-start(s32[4]{0:T(128)} %constant.104.clone) | copy-start | bytes 52
  0.0 31.8 %copy-start.22 = (s32[4]{0:T(128)S(1)}, s32[4]{0:T(128)}, u32[]{:S(2)}) copy-start(s32[4]{0:T(128)} %constant.105.clone) | copy-start | bytes 52
  0.0 35.8 %copy-start.15 = (s32[4]{0:T(128)S(1)}, s32[4]{0:T(128)}, u32[]{:S(2)}) copy-start(s32[4]{0:T(128)} %constant.108.clone) | copy-start | bytes 52
  0.0 35.8 %copy-start.16 = (s32[4]{0:T(128)S(1)}, s32[4]{0:T(128)}, u32[]{:S(2)}) copy-start(s32[4]{0:T(128)} %constant.109.clone) | copy-start | bytes 52
  0.0 35.8 %copy-start.17 = (s32[4]{0:T(128)S(1)}, s32[4]{0:T(128)}, u32[]{:S(2)}) copy-start(s32[4]{0:T(128)} %constant.112.clone) | copy-start | bytes 52
  0.1 35.8 %copy-start.18 = (s32[4]{0:T(128)S(1)}, s32[4]{0:T(128)}, u32[]{:S(2)}) copy-start(s32[4]{0:T(128)} %constant.113.clone) | copy-start | bytes 52
  0.1 6.7 %collective-permute-start.9 = (bf16[1,512,128]{2,1,0:T(8,128)(2,1)}, bf16[1,512,128]{2,1,0:T(8,128)(2,1)S(1)}, u32[]{:S(2)}, u32[]{:S(2)}) collective-permute-start(bf16[1,512,128]{2,1,0:T(8,128)(2,1)} %bitcast.11), channel_id=1, source_target_pairs={{0,16},{1,17},{2,6},{3,7},{4,20},{5,21},{6,2},{7,3},{8,24},{9,25},... | collective-permute-start | bytes 393224 | tf_op jit(solution)/shard_map/ppermute | solution.py:406
  7.8 6.4 %collective-permute-start.10 = (bf16[2,512,128]{2,1,0:T(8,128)(2,1)S(1)}, bf16[2,512,128]{2,1,0:T(8,128)(2,1)S(1)}, u32[]{:S(2)}, u32[]{:S(2)}) collective-permute-start(bf16[2,512,128]{2,1,0:T(8,128)(2,1)S(1)} %pad_maximum_fusion.2), channel_id=1, source_target_pairs={{0,1},{1,0},{2,18},{3,19},{4,5},{5,4},{6,22},{7,23},{8,9},{9,8},{1... | collective-permute-start | bytes 786440 | tf_op jit(solution)/shard_map/ppermute | solution.py:406
  15.2 9.2 %collective-permute-start.11 = (bf16[4,512,128]{2,1,0:T(8,128)(2,1)S(1)}, bf16[4,512,128]{2,1,0:T(8,128)(2,1)S(1)}, u32[]{:S(2)}, u32[]{:S(2)}) collective-permute-start(bf16[4,512,128]{2,1,0:T(8,128)(2,1)S(1)} %pad_maximum_fusion.1), channel_id=1, source_target_pairs={{0,8},{1,9},{2,3},{3,2},{4,12},{5,13},{6,7},{7,6},{8,0},{9,1},{10,... | collective-permute-start | bytes 1572872 | tf_op jit(solution)/shard_map/ppermute | solution.py:406
  16.9 13.3 %collective-permute-start = (bf16[1,128,128]{2,1,0:T(8,128)(2,1)S(1)}, bf16[1,128,128]{2,1,0:T(8,128)(2,1)S(1)}, u32[]{:S(2)}, u32[]{:S(2)}) collective-permute-start(bf16[1,128,128]{2,1,0:T(8,128)(2,1)S(1)} %maximum_bitcast_fusion), channel_id=1, source_target_pairs={{0,16},{1,17},{2,6},{3,7},{4,20},{5,21},{6,2},{7,3},{8,24},{9,25},... | collective-permute-start | bytes 98312 | tf_op jit(solution)/shard_map/ppermute | solution.py:406
  25.4 27.6 %copy-start = (bf16[8,512,128]{2,1,0:T(8,128)(2,1)}, bf16[8,512,128]{2,1,0:T(8,128)(2,1)S(1)}, u32[]{:S(2)}) copy-start(bf16[8,512,128]{2,1,0:T(8,128)(2,1)S(1)} %pad_maximum_fusion.refs_4_) | copy-start | bytes 3145732
  25.4 18.7 %collective-permute-start.12 = (bf16[8,512,128]{2,1,0:T(8,128)(2,1)S(1)}, bf16[8,512,128]{2,1,0:T(8,128)(2,1)S(1)}, u32[]{:S(2)}, u32[]{:S(2)}) collective-permute-start(bf16[8,512,128]{2,1,0:T(8,128)(2,1)S(1)} %pad_maximum_fusion.refs_4_), channel_id=1, source_target_pairs={{0,4},{1,5},{2,10},{3,11},{4,0},{5,1},{6,14},{7,15},{8,12},{9,13},... | collective-permute-start | bytes 3145736 | tf_op jit(solution)/shard_map/ppermute | solution.py:406
  30.2 5.0 %collective-permute-start.1 = (bf16[2,128,128]{2,1,0:T(8,128)(2,1)S(1)}, bf16[2,128,128]{2,1,0:T(8,128)(2,1)S(1)}, u32[]{:S(2)}, u32[]{:S(2)}) collective-permute-start(bf16[2,128,128]{2,1,0:T(8,128)(2,1)S(1)} %pad_maximum_fusion.4), channel_id=1, source_target_pairs={{0,8},{1,9},{2,18},{3,19},{4,12},{5,13},{6,22},{7,23},{8,0},{9,1},... | collective-permute-start | bytes 196616 | tf_op jit(solution)/shard_map/ppermute | solution.py:406
  35.2 18.5 %copy-start.1 = (bf16[4,128,128]{2,1,0:T(8,128)(2,1)}, bf16[4,128,128]{2,1,0:T(8,128)(2,1)S(1)}, u32[]{:S(2)}) copy-start(bf16[4,128,128]{2,1,0:T(8,128)(2,1)S(1)} %pad_maximum_fusion.3.refs_0_) | copy-start | bytes 393220
  35.2 6.4 %collective-permute-start.2 = (bf16[4,128,128]{2,1,0:T(8,128)(2,1)S(1)}, bf16[4,128,128]{2,1,0:T(8,128)(2,1)S(1)}, u32[]{:S(2)}, u32[]{:S(2)}) collective-permute-start(bf16[4,128,128]{2,1,0:T(8,128)(2,1)S(1)} %pad_maximum_fusion.3.refs_0_), channel_id=1, source_target_pairs={{0,4},{1,5},{2,10},{3,11},{4,0},{5,1},{6,14},{7,15},{8,12},{9,13},... | collective-permute-start | bytes 393224 | tf_op jit(solution)/shard_map/ppermute | solution.py:406
  35.8 17.9 %collective-permute-start.3 = (bf16[4,128,128]{2,1,0:T(8,128)(2,1)S(1)}, bf16[4,128,128]{2,1,0:T(8,128)(2,1)S(1)}, u32[]{:S(2)}, u32[]{:S(2)}) collective-permute-start(bf16[4,128,128]{2,1,0:T(8,128)(2,1)S(1)} %pad_maximum_fusion.3.refs_0_), channel_id=1, source_target_pairs={{0,2},{1,3},{2,0},{3,1},{4,6},{5,7},{6,4},{7,5},{8,10},{9,11},{10,... | collective-permute-start | bytes 393224 | tf_op jit(solution)/shard_map/ppermute | solution.py:406
  41.7 12.1 %copy-start.2 = (bf16[4,128,128]{2,1,0:T(8,128)(2,1)}, bf16[4,128,128]{2,1,0:T(8,128)(2,1)S(1)}, u32[]{:S(2)}) copy-start(bf16[4,128,128]{2,1,0:T(8,128)(2,1)S(1)} %collective-permute-done.2.refs_1_) | copy-start | bytes 393220
  41.7 12.0 %collective-permute-start.4 = (bf16[4,128,128]{2,1,0:T(8,128)(2,1)S(1)}, bf16[4,128,128]{2,1,0:T(8,128)(2,1)S(1)}, u32[]{:S(2)}, u32[]{:S(2)}) collective-permute-start(bf16[4,128,128]{2,1,0:T(8,128)(2,1)S(1)} %collective-permute-done.2.refs_1_), channel_id=1, source_target_pairs={{0,2},{1,3},{2,0},{3,1},{4,6},{5,7},{6,4},{7,5},{8,10},{9,11},{10,... | collective-permute-start | bytes 393224 | tf_op jit(solution)/shard_map/ppermute | solution.py:406
  44.1 44.8 %collective-permute-start.13 = (bf16[8,512,128]{2,1,0:T(8,128)(2,1)S(1)}, bf16[8,512,128]{2,1,0:T(8,128)(2,1)}, u32[]{:S(2)}, u32[]{:S(2)}) collective-permute-start(bf16[8,512,128]{2,1,0:T(8,128)(2,1)S(1)} %pad_maximum_fusion.refs_4_), channel_id=1, source_target_pairs={{0,2},{1,3},{2,0},{3,1},{4,6},{5,7},{6,4},{7,5},{8,10},{9,11},{10,... | collective-permute-start | bytes 3145736 | tf_op jit(solution)/shard_map/ppermute | solution.py:406
  44.1 15.7 %copy-start.23 = (bf16[8,512,128]{2,1,0:T(8,128)(2,1)}, bf16[8,512,128]{2,1,0:T(8,128)(2,1)S(1)}, u32[]{:S(2)}) copy-start(bf16[8,512,128]{2,1,0:T(8,128)(2,1)S(1)} %collective-permute-done.12.refs_5_) | copy-start | bytes 3145732
  44.1 44.8 %collective-permute-start.14 = (bf16[8,512,128]{2,1,0:T(8,128)(2,1)S(1)}, bf16[8,512,128]{2,1,0:T(8,128)(2,1)}, u32[]{:S(2)}, u32[]{:S(2)}) collective-permute-start(bf16[8,512,128]{2,1,0:T(8,128)(2,1)S(1)} %collective-permute-done.12.refs_5_), channel_id=1, source_target_pairs={{0,2},{1,3},{2,0},{3,1},{4,6},{5,7},{6,4},{7,5},{8,10},{9,11},{10,... | collective-permute-start | bytes 3145736 | tf_op jit(solution)/shard_map/ppermute | solution.py:406
  53.7 0.6 copy-start.3
  53.7 0.7 copy-start.4
  54.4 26.2 %copy-start.7 = (s32[4,3]{0,1:T(4,128)S(1)}, s32[4,3]{0,1:T(4,128)}, u32[]{:S(2)}) copy-start(s32[4,3]{0,1:T(4,128)} %constant.102.clone) | copy-start | bytes 148
  54.4 26.2 %copy-start.8 = (s32[4,3]{0,1:T(4,128)S(1)}, s32[4,3]{0,1:T(4,128)}, u32[]{:S(2)}) copy-start(s32[4,3]{0,1:T(4,128)} %constant.103.clone) | copy-start | bytes 148
  54.4 26.2 %copy-start.9 = (s32[4,3]{0,1:T(4,128)S(1)}, s32[4,3]{0,1:T(4,128)}, u32[]{:S(2)}) copy-start(s32[4,3]{0,1:T(4,128)} %constant.106.clone) | copy-start | bytes 148
  54.4 26.2 %copy-start.10 = (s32[4,3]{0,1:T(4,128)S(1)}, s32[4,3]{0,1:T(4,128)}, u32[]{:S(2)}) copy-start(s32[4,3]{0,1:T(4,128)} %constant.107.clone) | copy-start | bytes 148
  54.4 26.2 %copy-start.11 = (s32[4,3]{0,1:T(4,128)S(1)}, s32[4,3]{0,1:T(4,128)}, u32[]{:S(2)}) copy-start(s32[4,3]{0,1:T(4,128)} %constant.110.clone) | copy-start | bytes 148
  54.4 26.2 %copy-start.12 = (s32[4,3]{0,1:T(4,128)S(1)}, s32[4,3]{0,1:T(4,128)}, u32[]{:S(2)}) copy-start(s32[4,3]{0,1:T(4,128)} %constant.111.clone) | copy-start | bytes 148
  54.4 26.2 %copy-start.13 = (s32[4,3]{0,1:T(4,128)S(1)}, s32[4,3]{0,1:T(4,128)}, u32[]{:S(2)}) copy-start(s32[4,3]{0,1:T(4,128)} %constant.114.clone) | copy-start | bytes 148
  54.5 26.2 %copy-start.14 = (s32[4,3]{0,1:T(4,128)S(1)}, s32[4,3]{0,1:T(4,128)}, u32[]{:S(2)}) copy-start(s32[4,3]{0,1:T(4,128)} %constant.115.clone) | copy-start | bytes 148
  59.8 7.3 %collective-permute-start.5 = (bf16[160,128]{1,0:T(8,128)(2,1)}, bf16[160,128]{1,0:T(8,128)(2,1)S(1)}, u32[]{:S(2)}, u32[]{:S(2)}) collective-permute-start(bf16[160,128]{1,0:T(8,128)(2,1)} %get-tuple-element.15), channel_id=1, source_target_pairs={{0,2},{2,4},{4,6},{6,8},{8,10},{10,12},{12,14},{14,16},{16,18},{18... | collective-permute-start | bytes 122888 | tf_op jit(solution)/shard_map/ppermute | solution.py:524
  62.1 6.2 %collective-permute-start.6 = (bf16[160,128]{1,0:T(8,128)(2,1)}, bf16[160,128]{1,0:T(8,128)(2,1)S(1)}, u32[]{:S(2)}, u32[]{:S(2)}) collective-permute-start(bf16[160,128]{1,0:T(8,128)(2,1)} %get-tuple-element.16), channel_id=1, source_target_pairs={{2,0},{4,2},{6,4},{8,6},{10,8},{12,10},{14,12},{16,14},{18,16},{20... | collective-permute-start | bytes 122888 | tf_op jit(solution)/shard_map/ppermute | solution.py:525
  67.1 1.2 %copy-start.5 = (bf16[160,128]{1,0:T(8,128)(2,1)}, bf16[160,128]{1,0:T(8,128)(2,1)S(1)}, u32[]{:S(2)}) copy-start(bf16[160,128]{1,0:T(8,128)(2,1)S(1)} %collective-permute-done.5.low) | copy-start | bytes 122884
  68.2 0.6 copy-start.6
  73.1 14.0 %collective-permute-start.8 = (bf16[512,256]{1,0:T(8,128)(2,1)S(1)}, bf16[512,256]{1,0:T(8,128)(2,1)S(1)}, u32[]{:S(2)}, u32[]{:S(2)}) collective-permute-start(bf16[512,256]{1,0:T(8,128)(2,1)S(1)} %get-tuple-element.17), channel_id=1, source_target_pairs={{0,1},{1,0},{2,3},{3,2},{4,5},{5,4},{6,7},{7,6},{8,9},{9,8},{10,11... | collective-permute-start | bytes 786440 | tf_op jit(solution)/shard_map/ppermute | solution.py:542
  80.1 8.8 %collective-permute-start.7 = (bf16[512,256]{1,0:T(8,128)(2,1)}, bf16[512,256]{1,0:T(8,128)(2,1)S(1)}, u32[]{:S(2)}, u32[]{:S(2)}) collective-permute-start(bf16[512,256]{1,0:T(8,128)(2,1)} %attend1.1), channel_id=1, source_target_pairs={{0,1},{1,0},{2,3},{3,2},{4,5},{5,4},{6,7},{7,6},{8,9},{9,8},{10,11... | collective-permute-start | bytes 786440 | tf_op jit(solution)/shard_map/ppermute | solution.py:542
  87.1 1.8 %copy-start.24 = (bf16[512,256]{1,0:T(8,128)(2,1)}, bf16[512,256]{1,0:T(8,128)(2,1)S(1)}, u32[]{:S(2)}) copy-start(bf16[512,256]{1,0:T(8,128)(2,1)S(1)} %collective-permute-done.8.refs_3_) | copy-start | bytes 786436
  88.9 0.7 copy-start.25

commit v2 on v1

--- a/solution.py
+++ b/solution.py
@@ -151,6 +151,8 @@
 ROW_TILE = 256
 BF16 = jnp.bfloat16
 F32 = jnp.float32
+INFO = 3
+GRANT = 16 * 1024 * 1024
 
 
 def whole():
@@ -169,66 +171,102 @@
     return pl.CostEstimate(flops=flops, bytes_accessed=moved, transcendentals=0)
 
 
-def rope_lanes(values, cosine, sine):
+def rope_angles(block, base, blocks):
+    (cosine, sine), row = (base[0], base[1]), pl.ds(block, 1)
+    turn, lift = blocks[0, row, :], blocks[1, row, :]
+    return cosine * turn - sine * lift, sine * turn + cosine * lift
+
+
+def rope_lanes(values, angles):
     lane = lax.broadcasted_iota(jnp.int32, values.shape, 1)
     swapped = jnp.where(
         lane % HEAD < HEAD // 2,
-        pltpu.roll(values, LANES - HEAD // 2, 1),
+        -pltpu.roll(values, LANES - HEAD // 2, 1),
         pltpu.roll(values, HEAD // 2, 1),
     )
-    return values * cosine + swapped * sine
-
-
-def project_kernel(tokens, gain, w_query, w_pool, cosine, sine, normed, query, pool):
-    for row in range(0, tokens.shape[0], 16):
-        rows = slice(row, row + 16)
-        values = tokens[rows, :].astype(F32)
+    return values * angles[0] + swapped * angles[1]
+
+
+def load_project_kernel(info, *refs):
+    (tokens, *shared), (normed, query, pool), (rows, *kept) = refs[:6], refs[6:9], refs[9:15]
+    sems = refs[15]
+    size = normed.shape[0]
+    tiles = tokens.shape[0] // size
+
+    def tile(ref, index):
+        return ref.at[index * size : (index + 1) * size, :]
+
+    pairs = [(tile(tokens, 0), tile(rows, 0))] + list(zip(shared, kept))
+    pairs += [(tile(tokens, index), tile(rows, index)) for index in range(1, tiles)]
+    copies = [pltpu.make_async_copy(*pair, sems.at[index]) for index, pair in enumerate(pairs)]
+    for copy in copies:
+        copy.start()
+    copies[0].wait()
+    copies[1].wait()
+    project_kernel(0, info, rows, *kept, normed, query, pool, ready=copies[2:6])
+    for copy in copies[6:]:
+        copy.wait()
+
+
+def project_kernel(
+    offset, info, tokens, gain, w_query, w_pool, base, blocks, normed, query, pool, ready=()
+):
+    size = normed.shape[0]
+    for row in range(0, size, 16):
+        values = tokens[offset + row : offset + row + 16, :].astype(F32)
         centred = values - jnp.mean(values, axis=-1, keepdims=True)
         spread = jnp.mean(centred * centred, axis=-1, keepdims=True)
-        normed[rows, :] = (centred * lax.rsqrt(spread + 1e-06) * gain[...]).astype(BF16)
+        normed[row : row + 16, :] = (centred * lax.rsqrt(spread + 1e-06) * gain[...]).astype(BF16)
+    for copy in ready:
+        copy.wait()
     left = normed[...]
     pool[...] = jnp.dot(left, w_pool[...], preferred_element_type=F32).astype(BF16)
     products = jnp.dot(left, w_query[...], preferred_element_type=F32)
-    for lane in range(0, products.shape[1], LANES):
-        turned = rope_lanes(products[:, lane : lane + LANES], cosine[...], sine[...])
-        query[:, lane : lane + LANES] = turned.astype(BF16) * HEAD ** (-0.5)
-
-
-def key_value_kernel(places, normed, *refs):
-    pieces, (cosine, sine, pool_head, pool_tail, key_value, head, tail, weight) = refs[:4], refs[4:]
-    step, last = pl.program_id(0), pl.num_programs(0) - 1
+    first = info[0] * (tokens.shape[0] // QB) + offset // QB
+    for row in range(0, size, QB):
+        angles = rope_angles(first + row // QB, base, blocks)
+        for lane in range(0, products.shape[1], LANES):
+            turned = rope_lanes(products[row : row + QB, lane : lane + LANES], angles)
+            query[row : row + QB, lane : lane + LANES] = turned.astype(BF16) * HEAD ** (-0.5)
+
+
+def key_value_kernel(tiles, info, *refs):
+    pieces, normed, pools = refs[:4], refs[4 : 4 + tiles], refs[4 + tiles : 6 + tiles]
+    base, blocks, key_value, head, tail, weight = refs[6 + tiles :]
     depth = pieces[0].shape[1]
-
-    @pl.when(step == 0)
-    def _():
-        for index, piece in enumerate(pieces):
-            for slot in range(piece.shape[0]):
-                place = places[index * piece.shape[0] + slot]
-                weight[pl.ds(pl.multiple_of(place * depth, depth), depth), :] = piece[slot]
-
-    products = jnp.dot(normed[...], weight[...], preferred_element_type=F32)
-    lane = lax.broadcasted_iota(jnp.int32, products.shape, 1)
-    turned = rope_lanes(products, cosine[...], sine[...])
-    result = jnp.where(lane < HEAD, turned, products).astype(BF16)
-    key_value[...] = result
-    edge = pool_head.shape[0]
-    for when, out, rows, pool in (
-        (step == 0, head, result[:WINDOW], pool_head),
-        (step == last, tail, result[-WINDOW:], pool_tail),
-    ):
-
-        @pl.when(when)
-        def _(out=out, rows=rows, pool=pool):
-            out[:WINDOW, :] = rows
-            for group in range(pool.shape[1] // LANES):
-                start = WINDOW + group * edge
-                out[start : start + edge, :] = pool[:, group * LANES : (group + 1) * LANES]
-
-
-def pool_kernel(info, pool, low, high, scale, out, wide):
-    rows, channels = pool.shape
+    for index, piece in enumerate(pieces):
+        for slot in range(piece.shape[0]):
+            place = info[INFO + index * piece.shape[0] + slot]
+            weight[pl.ds(pl.multiple_of(place * depth, depth), depth), :] = piece[slot]
+    size = normed[0].shape[0]
+    first = info[0] * (key_value.shape[0] // QB)
+    for tile in range(tiles):
+        products = jnp.dot(normed[tile][...], weight[...], preferred_element_type=F32)
+        lane = lax.broadcasted_iota(jnp.int32, (QB, LANES), 1)
+        for row in range(0, size, QB):
+            angles = rope_angles(first + (tile * size + row) // QB, base, blocks)
+            plain = products[row : row + QB, :]
+            result = jnp.where(lane < HEAD, rope_lanes(plain, angles), plain).astype(BF16)
+            key_value[tile * size + row : tile * size + row + QB, :] = result
+            if tile == 0 and row == 0:
+                head[:WINDOW, :] = result
+            if tile == tiles - 1 and row == size - QB:
+                tail[:WINDOW, :] = result
+    edge = (head.shape[0] - WINDOW) // (pools[0].shape[1] // LANES)
+    for group in range(pools[0].shape[1] // LANES):
+        lanes = slice(group * LANES, (group + 1) * LANES)
+        rows = slice(WINDOW + group * edge, WINDOW + (group + 1) * edge)
+        head[rows, :] = pools[0][:edge, lanes]
+        tail[rows, :] = pools[1][size - edge :, lanes]
+
+
+def pool_kernel(tiles, chunks, info, *refs):
+    pools, (low, high, scale), outs = refs[:tiles], refs[tiles : tiles + 3], refs[tiles + 3 : -1]
+    wide = refs[-1]
+    size, channels = pools[0].shape
+    rows = size * tiles
     edge = (wide.shape[0] - rows) // 2
-    chunks, chunk = out.shape[0], out.shape[1]
+    chunk = rows // chunks
     place, total = info[0], info[2] * rows
     tp = info[1]
     groups = channels // LANES
@@ -237,7 +275,8 @@
         lanes = slice(group * LANES, (group + 1) * LANES)
         wide[:edge, lanes] = low[start : start + edge, :]
         wide[edge + rows :, lanes] = high[start : start + edge, :]
-    wide[edge : edge + rows, :] = pool[...]
+    for tile in range(tiles):
+        wide[edge + tile * size : edge + (tile + 1) * size, :] = pools[tile][...]
     span = QB + 2 * edge
     row = lax.broadcasted_iota(jnp.int32, (QB, span), 0) + edge
     column = lax.broadcasted_iota(jnp.int32, (QB, span), 1)
@@ -263,15 +302,27 @@
                     position - reaches[group], 0
                 )
                 mean = sums * (1.0 / counted.astype(F32))
-                own = pool[aligned(start), lanes].astype(F32)
-                out[step, block : block + QB, lanes] = ((mean - own) * scale[:, lanes]).astype(BF16)
-
-
-def attend_kernel(step, info, sink, query, key_value, low, high, out, keys, values):
+                own = wide[pl.ds(pl.multiple_of(start + edge, edge), QB), lanes].astype(F32)
+                outs[step][block : block + QB, lanes] = ((mean - own) * scale[:, lanes]).astype(BF16)
+
+
+def attend_kernel(step, tiles, info, sink, *refs):
+    pieces = refs[:tiles]
+    key_value, low, high, out, keys, values, query = refs[tiles:]
     chunk = out.shape[0]
+    size = pieces[0].shape[0]
     place, tp, count = info[0], info[1], info[2]
     target = lax.bitwise_xor(tp, step)
-    chunks = query.shape[0] // chunk
+    total_rows = key_value.shape[0]
+    chunks = total_rows // chunk
+    for option in range(chunks):
+
+        @pl.when(target == option)
+        def _(option=option):
+            for row in range(0, chunk, size):
+                part = pieces[(option * chunk + row) // size]
+                query[row : row + size, :] = part[...]
+
     begin = pl.multiple_of(target * chunk, chunk)
 
     def put(start, rows):
@@ -289,7 +340,7 @@
         put(WINDOW + block, key_value[aligned(begin + block), :])
     before = key_value[aligned(jnp.maximum(begin - WINDOW, 0)), :]
     put(0, jnp.where(target == 0, low[:WINDOW, :], before))
-    after_start = jnp.minimum(begin + chunk, query.shape[0] - WINDOW)
+    after_start = jnp.minimum(begin + chunk, total_rows - WINDOW)
     after = key_value[aligned(after_start), :]
     put(WINDOW + chunk, jnp.where(target == chunks - 1, high[:WINDOW, :], after))
 
@@ -305,7 +356,7 @@
             high_ok = high_ok & jnp.logical_not(at_end)
         for pair in range(query.shape[1] // LANES):
             lanes = slice(pair * LANES, (pair + 1) * LANES)
-            queries = query[aligned(begin + block), lanes]
+            queries = query[block : block + QB, lanes]
             result = None
             for side in range(2):
                 scores = lax.dot_general(
@@ -335,17 +386,10 @@
             out[block : block + QB, lanes] = result.astype(BF16)
 
 
-def output_kernel(parts, table, info, *refs):
+def output_kernel(parts, offset, info, *refs):
     attended, pooled = refs[:parts], refs[parts : 2 * parts]
-    sources, out = refs[2 * parts : 2 * parts + 4], refs[2 * parts + 4]
-    weight, joined, staged, in_sem, out_sem = refs[2 * parts + 5 :]
-    loads = [
-        pltpu.make_async_copy(source, weight.at[index], in_sem.at[index])
-        for index, source in enumerate(sources)
-    ]
+    sources, (out, joined, staged, out_sem) = refs[2 * parts : 2 * parts + 4], refs[2 * parts + 4 :]
     order = (0, 2, 1, 3)
-    for index in order:
-        loads[index].start()
     tp = info[1]
     width = attended[0].shape[1]
     for step in range(parts):
@@ -353,18 +397,17 @@
         for half, part in enumerate((attended[step], pooled[step])):
             start = pl.multiple_of((half * parts + owner) * width, LANES)
             joined[:, pl.ds(start, width)] = part[...]
-    depth, lanes = weight.shape[2], weight.shape[3]
-    blocks = weight.shape[1] // parts
+    depth, lanes = sources[0].shape[1], sources[0].shape[2]
+    blocks = sources[0].shape[0] // parts
     stores = []
     for index in order:
-        loads[index].wait()
         for block in range(0, blocks, 2):
             total = None
             entries = [(index * blocks + block + side) * (parts + 1) for side in range(2)]
             for step in range(parts):
                 start = pl.multiple_of(lax.bitwise_xor(tp, step) * depth, LANES)
                 right = jnp.concatenate(
-                    [weight[index, table[entry + 1 + step]] for entry in entries], axis=1
+                    [sources[index][info[offset + entry + 1 + step]] for entry in entries], axis=1
                 )
                 product = jnp.dot(
                     joined[:, pl.ds(start, depth)], right, preferred_element_type=F32
@@ -373,7 +416,7 @@
             for side in range(2):
                 number = index * blocks + block + side
                 staged[number] = total[:, side * lanes : (side + 1) * lanes].astype(BF16)
-                start = pl.multiple_of(table[entries[side]] * lanes, LANES)
+                start = pl.multiple_of(info[offset + entries[side]] * lanes, LANES)
                 store = pltpu.make_async_copy(
                     staged.at[number], out.at[:, pl.ds(start, lanes)], out_sem.at[number]
                 )
@@ -409,9 +452,44 @@
     for masks in zip(even[:-1], odd[:-1]):
         held = jnp.concatenate([held, send(held, masks)], axis=0)
     core = (tp_count, tp_count)
-    other = send(held, core)
     came = send(held, (even[-1], odd[-1]))
-    return held, came, other, send(came, core)
+    return held, came, send(held, core), send(came, core)
+
+
+def device_table(sp_count, tp_count, kv_orders, out_orders):
+    rows = []
+    for sp_place in range(sp_count):
+        for tp_place in range(tp_count):
+            kinds = [sp_place % 2, 1 - sp_place % 2]
+            kv_part, out_part = [], []
+            for flip, kind in enumerate(kinds):
+                for late in range(2):
+                    order = kv_orders[kind]
+                    extra = order[-1] * late
+                    for mask in slot_masks(order[:-1]):
+                        kv_part.append(sp_place ^ flip ^ ((mask ^ extra) // tp_count))
+                    order = out_orders[kind]
+                    extra = order[-1] * late
+                    found = {}
+                    for slot, mask in enumerate(slot_masks(order[:-1])):
+                        delta, step = divmod(mask ^ extra, tp_count)
+                        found.setdefault(delta, {})[step] = slot
+                    for delta, slots in found.items():
+                        out_part.append(sp_place ^ flip ^ delta)
+                        out_part += [slots[step] for step in range(tp_count)]
+            rows.append([sp_place, tp_place, sp_count] + kv_part + out_part)
+    return np.array(rows, np.int32)
+
+
+def rope_tables(length):
+    half = HEAD // 2
+    inverse = np.float32(10000.0) ** (-np.arange(half, dtype=np.float32) / np.float32(half))
+    inverse = np.tile(inverse.astype(np.float64), LANES // half)
+    tables = []
+    for positions in (np.arange(QB), np.arange(0, length, QB)):
+        angles = positions[:, None] * inverse[None, :]
+        tables.append(np.stack([np.cos(angles), np.sin(angles)]).astype(np.float32))
+    return tables
 
 
 def fast_body(tokens, norm_gain, w_query, w_key, w_value, w_pool_in, sink_logit, pool_scale, w_out):
@@ -430,111 +508,85 @@
     kv_pieces = doubled(kv_block, kv_orders, sp_count, tp_count)
     out_pieces = doubled(w_out, out_orders, sp_count, tp_count)
 
-    odd = sp_place % 2
-    info = jnp.stack([sp_place, tp_place, jnp.int32(sp_count)]).astype(jnp.int32)
-
-    def by_class(pairs):
-        return jnp.where(odd == 0, jnp.array(pairs[0], jnp.int32), jnp.array(pairs[1], jnp.int32))
-
-    kv_tables, out_tables = [], []
-    for flip in range(2):
-        for late in range(2):
-            rows = []
-            for order in (kv_orders if flip == 0 else kv_orders[::-1]):
-                extra = order[-1] if late else 0
-                rows.append([((mask ^ extra) // tp_count) ^ flip for mask in slot_masks(order[:-1])])
-            kv_tables.append(by_class(rows) ^ sp_place)
-            rows = []
-            for order in (out_orders if flip == 0 else out_orders[::-1]):
-                extra = order[-1] if late else 0
-                masks = [mask ^ extra for mask in slot_masks(order[:-1])]
-                found = {}
-                for slot, mask in enumerate(masks):
-                    found.setdefault(mask // tp_count, {})[mask % tp_count] = slot
-                rows.append(
-                    [[delta ^ flip] + [slots[t] for t in range(tp_count)] for delta, slots in found.items()]
-                )
-            picked = by_class(rows)
-            out_tables.append(picked ^ jnp.pad(sp_place[None], (0, tp_count))[None, :])
-    kv_table = jnp.concatenate(kv_tables)
-    out_table = jnp.concatenate(out_tables).reshape(-1)
-
-    half = HEAD // 2
-    inverse = 10000.0 ** (-jnp.arange(half, dtype=F32) / half)
-    inverse = jnp.tile(inverse, LANES // half)
-    positions = (sp_place * local_rows + jnp.arange(local_rows)).astype(F32)
-    angles = positions[:, None] * inverse[None, :]
-    cosine = jnp.cos(angles)
-    sign = jnp.where(jnp.arange(LANES) % HEAD < half, -1.0, 1.0).astype(F32)
-    sine = jnp.sin(angles) * sign[None, :]
-
-    def rows_of(columns, size=ROW_TILE):
-        return pl.BlockSpec((size, columns), lambda i: (i, 0))
-
-    def fixed(shape, index=0):
-        return pl.BlockSpec(shape, lambda i: (index,) + (0,) * (len(shape) - 1))
+    table = device_table(sp_count, tp_count, kv_orders, out_orders)
+    info = lax.dynamic_index_in_dim(jnp.array(table), sp_place * tp_count + tp_place, 0, False)
+    base, blocks = (jnp.array(t) for t in rope_tables(local_rows * sp_count))
+
+    def call(name, kernel, operands, specs, out_shape, scratch, flops):
+        single = not isinstance(out_shape, list)
+        shapes = [
+            jax.ShapeDtypeStruct(*(shape if isinstance(shape[0], tuple) else (shape, BF16)))
+            for shape in ([out_shape] if single else out_shape)
+        ]
+        spec = pltpu.HBM if name == "output" else pltpu.VMEM
+        outs = [pl.BlockSpec(memory_space=spec)] * len(shapes)
+        return pl.pallas_call(
+            kernel,
+            in_specs=specs,
+            out_specs=outs[0] if single else outs,
+            out_shape=shapes[0] if single else shapes,
+            scratch_shapes=scratch,
+            compiler_params=pltpu.CompilerParams(vmem_limit_bytes=GRANT),
+            cost_estimate=cost(flops),
+        )(*operands)
 
     tiles = local_rows // ROW_TILE
-    normed, query, pool_in = pl.pallas_call(
-        project_kernel,
-        grid=(tiles,),
-        in_specs=[
-            rows_of(width),
-            fixed((1, width)),
-            fixed(w_query.shape),
-            fixed(w_pool_in.shape),
-            rows_of(LANES),
-            rows_of(LANES),
-        ],
-        out_specs=[rows_of(width), rows_of(heads_width), rows_of(local_pool)],
-        out_shape=[
-            jax.ShapeDtypeStruct(tokens.shape, BF16),
-            jax.ShapeDtypeStruct((local_rows, heads_width), BF16),
-            jax.ShapeDtypeStruct((local_rows, local_pool), BF16),
-        ],
-        cost_estimate=cost(2 * local_rows * width * (heads_width + local_pool)),
-        name="project",
-    )(tokens, norm_gain[None, :], w_query, w_pool_in, cosine, sine)
+    normed, queries, pools = [], [], []
+    results = [(ROW_TILE, width), (ROW_TILE, heads_width), (ROW_TILE, local_pool)]
+    held = (tokens, norm_gain[None, :], w_query, w_pool_in, base, blocks)
+    held = tuple(pltpu.with_memory_space_constraint(part, pltpu.HBM) for part in held)
+    for tile in range(tiles):
+        flops = 2 * ROW_TILE * width * (heads_width + local_pool)
+        if tile == 0:
+            outs = call(
+                "project0",
+                load_project_kernel,
+                (info, *held),
+                [scalars()] + [pl.BlockSpec(memory_space=pltpu.HBM)] * 6,
+                results + [(part.shape, part.dtype) for part in held],
+                [pltpu.SemaphoreType.DMA((5 + tiles,))],
+                flops,
+            )
+            held = outs[3:]
+        else:
+            outs = call(
+                f"project{tile}",
+                functools.partial(project_kernel, tile * ROW_TILE),
+                (info, *held),
+                [scalars()] + [whole()] * 6,
+                results,
+                [],
+                flops,
+            )
+        for found, out in zip((normed, queries, pools), outs):
+            found.append(out)
 
     edge = 2 * (POOL_SPANS[-1] // 2)
     payload = (WINDOW + edge * (local_pool // LANES), LANES)
-    key_value, head, tail = pl.pallas_call(
-        key_value_kernel,
-        grid=(tiles,),
-        in_specs=[scalars(), rows_of(width)]
-        + [fixed(piece.shape) for piece in kv_pieces]
-        + [
-            rows_of(LANES),
-            rows_of(LANES),
-            fixed((edge, local_pool)),
-            fixed((edge, local_pool), local_rows // edge - 1),
-        ],
-        out_specs=[rows_of(LANES), fixed(payload), fixed(payload)],
-        out_shape=[
-            jax.ShapeDtypeStruct((local_rows, LANES), BF16),
-            jax.ShapeDtypeStruct(payload, BF16),
-            jax.ShapeDtypeStruct(payload, BF16),
-        ],
-        scratch_shapes=[pltpu.VMEM((width, LANES), BF16)],
-        cost_estimate=cost(2 * local_rows * width * LANES),
-        name="key_value",
-    )(kv_table, normed, *kv_pieces, cosine, sine, pool_in, pool_in)
+    key_value, head, tail = call(
+        "key_value",
+        functools.partial(key_value_kernel, tiles),
+        (info, *kv_pieces, *normed, pools[0], pools[-1], *held[4:]),
+        [scalars()] + [whole()] * (8 + tiles),
+        [(local_rows, LANES), payload, payload],
+        [pltpu.VMEM((width, LANES), BF16)],
+        2 * local_rows * width * LANES,
+    )
 
     forward = [(i, i + 1) for i in range(sp_count - 1)]
     low = lax.ppermute(tail, "sp", forward)
     high = lax.ppermute(head, "sp", [(target, source) for source, target in forward])
 
-    pooled = pl.pallas_call(
-        pool_kernel,
-        in_specs=[scalars()] + [whole()] * 4,
-        out_specs=whole(),
-        out_shape=jax.ShapeDtypeStruct((tp_count, chunk, local_pool), BF16),
-        scratch_shapes=[pltpu.VMEM((local_rows + 2 * edge, local_pool), BF16)],
-        cost_estimate=cost(2 * local_rows * local_pool * 160),
-        name="pool",
-    )(info, pool_in, low, high, pool_scale[None, :])
-
     devices = range(tp_count)
+    pooled = call(
+        "pool",
+        functools.partial(pool_kernel, tiles, tp_count),
+        (info, *pools, low, high, pool_scale[None, :]),
+        [scalars()] + [whole()] * (tiles + 3),
+        [(chunk, local_pool)] * tp_count,
+        [pltpu.VMEM((local_rows + 2 * edge, local_pool), BF16)],
+        2 * local_rows * local_pool * 160,
+    )
 
     def hand_over(part, step):
         if step == 0:
@@ -545,35 +597,32 @@
 
     attended_parts = [None] * tp_count
     for step in list(devices)[1:] + [0]:
-        attended = pl.pallas_call(
-            functools.partial(attend_kernel, step),
-            in_specs=[scalars(), scalars()] + [whole()] * 4,
-            out_specs=whole(),
-            out_shape=jax.ShapeDtypeStruct((chunk, heads_width), BF16),
-            scratch_shapes=[pltpu.VMEM((2, chunk + 2 * WINDOW, LANES), BF16)] * 2,
-            cost_estimate=cost(4 * chunk * 3 * WINDOW * LANES * local_heads),
-            name=f"attend{step}",
-        )(info, sink_logit, query, key_value, low, high)
+        attended = call(
+            f"attend{step}",
+            functools.partial(attend_kernel, step, tiles),
+            (info, sink_logit, *queries, key_value, low, high),
+            [scalars(), scalars()] + [whole()] * (tiles + 3),
+            (chunk, heads_width),
+            [pltpu.VMEM((2, chunk + 2 * WINDOW, LANES), BF16)] * 2
+            + [pltpu.VMEM((chunk, heads_width), BF16)],
+            4 * chunk * 3 * WINDOW * LANES * local_heads,
+        )
         attended_parts[step] = hand_over(attended, step)
 
     columns = w_out.shape[1] * sp_count
-    return pl.pallas_call(
-        functools.partial(output_kernel, tp_count),
-        in_specs=[scalars(), scalars()]
-        + [whole()] * (2 * tp_count)
-        + [pl.BlockSpec(memory_space=pltpu.HBM)] * 4,
-        out_specs=pl.BlockSpec(memory_space=pltpu.HBM),
-        out_shape=jax.ShapeDtypeStruct((chunk, columns), BF16),
-        scratch_shapes=[
-            pltpu.VMEM((4,) + out_pieces[0].shape, BF16),
+    return call(
+        "output",
+        functools.partial(output_kernel, tp_count, INFO + sp_count),
+        (info, *attended_parts, *pooled_parts, *out_pieces),
+        [scalars()] + [whole()] * (2 * tp_count) + [whole()] * 4,
+        (chunk, columns),
+        [
             pltpu.VMEM((chunk, w_out.shape[0] * tp_count), BF16),
             pltpu.VMEM((sp_count, chunk, w_out.shape[1]), BF16),
-            pltpu.SemaphoreType.DMA((4,)),
             pltpu.SemaphoreType.DMA((sp_count,)),
         ],
-        cost_estimate=cost(2 * chunk * columns * w_out.shape[0] * tp_count),
-        name="output",
-    )(out_table, info, *attended_parts, *pooled_parts, *out_pieces)
+        2 * chunk * columns * w_out.shape[0] * tp_count,
+    )
 
 
 def tiled(rows, w_query, w_pool_in, w_out):

time: 96.6 us -> 92.7 us (0.960)
  the two profiles are of different devices: /device:TPU:8 before, /device:TPU:0 now
where the time goes in v2:
time: 92.7 us; the launch traced here: 90.9 us
  waiting for transfers between devices  36.8 us (40%)
  Pallas kernels  25.9 us (28%)
  starting transfers between devices  23.3 us (25%)
  other arithmetic  3 us (3%)
  local copies, waits for them, and re-layouts  1.56 us (2%)
    ppermute x11, waiting for transfers between devices, send(): return lax.ppermute(array, ('sp', 'tp'), pairs)  32.2 us
    pallas_call x9, Pallas kernels, call(): pl.pallas_call(kernel, in_specs=specs, out_specs=outs[0] if single else o...  25.9 us
    ppermute x11, starting transfers between devices, send(): return lax.ppermute(array, ('sp', 'tp'), pairs)  17.8 us
    concatenate x5, other arithmetic, doubled(): held = jnp.concatenate([held, send(held, masks)], axis=0)  2.92 us
    ppermute x2, waiting for transfers between devices, hand_over(): return lax.ppermute(part, 'tp', [(i, i ^ step) for i in devices])  2.81 us
    ppermute x2, starting transfers between devices, hand_over(): return lax.ppermute(part, 'tp', [(i, i ^ step) for i in devices])  2.16 us
    ppermute x1, starting transfers between devices, fast_body(): low = lax.ppermute(tail, 'sp', forward)  2.02 us
  transfers between devices with their start and end apart: 15, of which 8 were waited for; matrix products, arithmetic and copies ran while one was open for 2% of the time, Pallas kernels for 23%

profile of v2, /device:TPU:0, one launch (start us, length us, event | category | flops | bytes accessed | tf_op | source)
XLA Modules:
  0.0 90.9 jit_solution(12496799956887920458)
XLA Ops:
  0.0 4.1 %collective-permute-start.9 = (bf16[1,512,128]{2,1,0:T(8,128)(2,1)}, bf16[1,512,128]{2,1,0:T(8,128)(2,1)S(1)}, u32[]{:S(2)}, u32[]{:S(2)}) collective-permute-start(bf16[1,512,128]{2,1,0:T(8,128)(2,1)} %bitcast.8), channel_id=1, source_target_pairs={{0,16},{1,17},{2,6},{3,7},{4,20},{5,21},{6,2},{7,3},{8,24},{9,25},... | collective-permute-start | bytes 393224 | tf_op jit(solution)/shard_map/ppermute | solution.py:449
  4.1 3.2 %collective-permute-done.9 = bf16[1,512,128]{2,1,0:T(8,128)(2,1)S(1)} collective-permute-done((bf16[1,512,128]{2,1,0:T(8,128)(2,1)}, bf16[1,512,128]{2,1,0:T(8,128)(2,1)S(1)}, u32[]{:S(2)}, u32[]{:S(2)}) %collective-permute-start.9) | collective-permute-done | bytes 131104 | tf_op jit(solution)/shard_map/ppermute | solution.py:449
  7.2 0.9 %pad_maximum_fusion.2 = bf16[2,512,128]{2,1,0:T(8,128)(2,1)S(1)} fusion(bf16[1,512,128]{2,1,0:T(8,128)(2,1)S(1)} %collective-permute-done.9, bf16[1,512,128]{2,1,0:T(8,128)(2,1)} %bitcast.9), kind=kLoop, calls=%fused_computation.2 | loop fusion | flops 131072 | bytes 524288 | tf_op jit(solution)/shard_map/concatenate | solution.py:453
  8.2 3.3 %collective-permute-start.10 = (bf16[2,512,128]{2,1,0:T(8,128)(2,1)S(1)}, bf16[2,512,128]{2,1,0:T(8,128)(2,1)S(1)}, u32[]{:S(2)}, u32[]{:S(2)}) collective-permute-start(bf16[2,512,128]{2,1,0:T(8,128)(2,1)S(1)} %pad_maximum_fusion.2), channel_id=1, source_target_pairs={{0,1},{1,0},{2,18},{3,19},{4,5},{5,4},{6,22},{7,23},{8,9},{9,8},{1... | collective-permute-start | bytes 786440 | tf_op jit(solution)/shard_map/ppermute | solution.py:449
  11.4 4.4 %collective-permute-done.10 = bf16[2,512,128]{2,1,0:T(8,128)(2,1)S(1)} collective-permute-done((bf16[2,512,128]{2,1,0:T(8,128)(2,1)S(1)}, bf16[2,512,128]{2,1,0:T(8,128)(2,1)S(1)}, u32[]{:S(2)}, u32[]{:S(2)}) %collective-permute-start.10) | collective-permute-done | bytes 262176 | tf_op jit(solution)/shard_map/ppermute | solution.py:449
  15.8 1.0 %pad_maximum_fusion.1 = bf16[4,512,128]{2,1,0:T(8,128)(2,1)S(1)} fusion(bf16[2,512,128]{2,1,0:T(8,128)(2,1)S(1)} %collective-permute-done.10, bf16[1,512,128]{2,1,0:T(8,128)(2,1)S(1)} %collective-permute-done.9, bf16[1,512,128]{2,1,0:T(8,128)(2,1)} %bitcast.10), kind=kLoop, calls=%fused_computation.1 | loop fusion | flops 524288 | bytes 1048576 | tf_op jit(solution)/shard_map/concatenate | solution.py:453
  16.8 1.4 %collective-permute-start.11 = (bf16[4,512,128]{2,1,0:T(8,128)(2,1)S(1)}, bf16[4,512,128]{2,1,0:T(8,128)(2,1)S(1)}, u32[]{:S(2)}, u32[]{:S(2)}) collective-permute-start(bf16[4,512,128]{2,1,0:T(8,128)(2,1)S(1)} %pad_maximum_fusion.1), channel_id=1, source_target_pairs={{0,8},{1,9},{2,3},{3,2},{4,12},{5,13},{6,7},{7,6},{8,0},{9,1},{10,... | collective-permute-start | bytes 1572872 | tf_op jit(solution)/shard_map/ppermute | solution.py:449
  18.1 7.9 %collective-permute-done.11 = bf16[4,512,128]{2,1,0:T(8,128)(2,1)S(1)} collective-permute-done((bf16[4,512,128]{2,1,0:T(8,128)(2,1)S(1)}, bf16[4,512,128]{2,1,0:T(8,128)(2,1)S(1)}, u32[]{:S(2)}, u32[]{:S(2)}) %collective-permute-start.11) | collective-permute-done | bytes 524320 | tf_op jit(solution)/shard_map/ppermute | solution.py:449
  26.0 1.0 %pad_maximum_fusion.refs_4_ = bf16[8,512,128]{2,1,0:T(8,128)(2,1)S(1)} fusion(bf16[4,512,128]{2,1,0:T(8,128)(2,1)S(1)} %collective-permute-done.11, bf16[2,512,128]{2,1,0:T(8,128)(2,1)S(1)} %collective-permute-done.10, bf16[1,512,128]{2,1,0:T(8,128)(2,1)S(1)} %collective-permute-done.9, bf16[1,512,128]{2,1,0:T(8,128)(2,1)} %bitcast.11), kind=kLoop, calls=%fused_computation | loop fusion | flops 1572864 | bytes 2097152 | tf_op jit(solution)/shard_map/concatenate | solution.py:453
  27.0 2.1 %collective-permute-start.12 = (bf16[8,512,128]{2,1,0:T(8,128)(2,1)S(1)}, bf16[8,512,128]{2,1,0:T(8,128)(2,1)S(1)}, u32[]{:S(2)}, u32[]{:S(2)}) collective-permute-start(bf16[8,512,128]{2,1,0:T(8,128)(2,1)S(1)} %pad_maximum_fusion.refs_4_), channel_id=1, source_target_pairs={{0,4},{1,5},{2,10},{3,11},{4,0},{5,1},{6,14},{7,15},{8,12},{9,13},... | collective-permute-start | bytes 3145736 | tf_op jit(solution)/shard_map/ppermute | solution.py:449
  29.1 0.9 constant_dynamic-slice_fusion
  30.0 0.1 collective-permute-start.13
  30.1 11.8 %collective-permute-done.12.refs_5_ = bf16[8,512,128]{2,1,0:T(8,128)(2,1)S(1)} collective-permute-done((bf16[8,512,128]{2,1,0:T(8,128)(2,1)S(1)}, bf16[8,512,128]{2,1,0:T(8,128)(2,1)S(1)}, u32[]{:S(2)}, u32[]{:S(2)}) %collective-permute-start.12) | collective-permute-done | bytes 1048608 | tf_op jit(solution)/shard_map/ppermute | solution.py:449
  41.9 0.0 collective-permute-start.14
  41.9 0.1 maximum_bitcast_fusion
  42.0 2.6 %collective-permute-start = (bf16[1,128,128]{2,1,0:T(8,128)(2,1)S(1)}, bf16[1,128,128]{2,1,0:T(8,128)(2,1)S(1)}, u32[]{:S(2)}, u32[]{:S(2)}) collective-permute-start(bf16[1,128,128]{2,1,0:T(8,128)(2,1)S(1)} %maximum_bitcast_fusion), channel_id=1, source_target_pairs={{0,16},{1,17},{2,6},{3,7},{4,20},{5,21},{6,2},{7,3},{8,24},{9,25},... | collective-permute-start | bytes 98312 | tf_op jit(solution)/shard_map/ppermute | solution.py:449
  44.6 2.3 %collective-permute-done = bf16[1,128,128]{2,1,0:T(8,128)(2,1)S(1)} collective-permute-done((bf16[1,128,128]{2,1,0:T(8,128)(2,1)S(1)}, bf16[1,128,128]{2,1,0:T(8,128)(2,1)S(1)}, u32[]{:S(2)}, u32[]{:S(2)}) %collective-permute-start) | collective-permute-done | bytes 32800 | tf_op jit(solution)/shard_map/ppermute | solution.py:449
  46.9 1.7 %collective-permute-start.1 = (bf16[2,128,128]{2,1,0:T(8,128)(2,1)S(1)}, bf16[2,128,128]{2,1,0:T(8,128)(2,1)S(1)}, u32[]{:S(2)}, u32[]{:S(2)}) collective-permute-start(bf16[2,128,128]{2,1,0:T(8,128)(2,1)S(1)} %pad_maximum_fusion.4), channel_id=1, source_target_pairs={{0,8},{1,9},{2,18},{3,19},{4,12},{5,13},{6,22},{7,23},{8,0},{9,1},... | collective-permute-start | bytes 196616 | tf_op jit(solution)/shard_map/ppermute | solution.py:449
  48.6 2.6 %collective-permute-done.1 = bf16[2,128,128]{2,1,0:T(8,128)(2,1)S(1)} collective-permute-done((bf16[2,128,128]{2,1,0:T(8,128)(2,1)S(1)}, bf16[2,128,128]{2,1,0:T(8,128)(2,1)S(1)}, u32[]{:S(2)}, u32[]{:S(2)}) %collective-permute-start.1) | collective-permute-done | bytes 65568 | tf_op jit(solution)/shard_map/ppermute | solution.py:449
  51.2 2.1 %collective-permute-start.2 = (bf16[4,128,128]{2,1,0:T(8,128)(2,1)S(1)}, bf16[4,128,128]{2,1,0:T(8,128)(2,1)S(1)}, u32[]{:S(2)}, u32[]{:S(2)}) collective-permute-start(bf16[4,128,128]{2,1,0:T(8,128)(2,1)S(1)} %pad_maximum_fusion.3.refs_0_), channel_id=1, source_target_pairs={{0,4},{1,5},{2,10},{3,11},{4,0},{5,1},{6,14},{7,15},{8,12},{9,13},... | collective-permute-start | bytes 393224 | tf_op jit(solution)/shard_map/ppermute | solution.py:449
  53.3 0.7 fusion.info
  54.0 3.5 %shard_map.118 = (bf16[256,2048]{1,0:T(8,128)(2,1)S(1)}, bf16[256,256]{1,0:T(8,128)(2,1)S(1)}, bf16[256,256]{1,0:T(8,128)(2,1)S(1)}, bf16[1024,2048]{1,0:T(8,128...) custom-call(s32[67]{0:T(128)S(1)} %fusion.info, ...), custom_call_target="tpu_custom_call" | custom-call | flops 536870912 | tf_op jit(solution)/shard_map/pallas_call | solution.py:523
  57.5 0.1 collective-permute-start.3
  57.6 0.0 collective-permute-done.2.refs_1_
  57.6 0.5 collective-permute-start.4
  58.1 2.0 %shard_map.121 = (bf16[256,2048]{1,0:T(8,128)(2,1)S(1)}, bf16[256,256]{1,0:T(8,128)(2,1)S(1)}, bf16[256,256]{1,0:T(8,128)(2,1)S(1)}) custom-call(s32[67]{0:T(128)S(1)} %fusion.info, bf16[1024,2048]{1,0:T(8,128)(2,1)S(1)} %get-tuple-element.29.tokens, f32[1,2048]{1,0:T(1,128)S(1)} %get-tuple-element.30.gain, bf16[2048,256]{1,0:T(8,128)(2,1)S(1)} %get-tuple-element.31.w_query, ...), custom_call_target="tpu_custom_call" | custom-call | flops 536870912 | tf_op jit(solution)/shard_map/pallas_call | solution.py:523
  60.1 2.0 %shard_map.120 = (bf16[256,2048]{1,0:T(8,128)(2,1)S(1)}, bf16[256,256]{1,0:T(8,128)(2,1)S(1)}, bf16[256,256]{1,0:T(8,128)(2,1)S(1)}) custom-call(s32[67]{0:T(128)S(1)} %fusion.info, bf16[1024,2048]{1,0:T(8,128)(2,1)S(1)} %get-tuple-element.29.tokens, f32[1,2048]{1,0:T(1,128)S(1)} %get-tuple-element.30.gain, bf16[2048,256]{1,0:T(8,128)(2,1)S(1)} %get-tuple-element.31.w_query, ...), custom_call_target="tpu_custom_call" | custom-call | flops 536870912 | tf_op jit(solution)/shard_map/pallas_call | solution.py:523
  62.1 2.0 %shard_map.119 = (bf16[256,2048]{1,0:T(8,128)(2,1)S(1)}, bf16[256,256]{1,0:T(8,128)(2,1)S(1)}, bf16[256,256]{1,0:T(8,128)(2,1)S(1)}) custom-call(s32[67]{0:T(128)S(1)} %fusion.info, bf16[1024,2048]{1,0:T(8,128)(2,1)S(1)} %get-tuple-element.29.tokens, f32[1,2048]{1,0:T(1,128)S(1)} %get-tuple-element.30.gain, bf16[2048,256]{1,0:T(8,128)(2,1)S(1)} %get-tuple-element.31.w_query, ...), custom_call_target="tpu_custom_call" | custom-call | flops 536870912 | tf_op jit(solution)/shard_map/pallas_call | solution.py:523
  64.1 0.0 copy-start
  64.1 0.0 copy-start.1
  64.1 0.0 collective-permute-done.3.refs_2_
  64.1 0.0 collective-permute-done.4.refs_3_
  64.1 2.0 %shard_map.122 = (bf16[1024,128]{1,0:T(8,128)(2,1)S(1)}, bf16[160,128]{1,0:T(8,128)(2,1)S(1)}, bf16[160,128]{1,0:T(8,128)(2,1)S(1)}) custom-call(s32[67]{0:T(128)S(1)} %fusion.info, bf16[4,128,128]{2,1,0:T(8,128)(2,1)S(1)} %pad_maximum_fusion.3.refs_0_, bf16[4,128,128]{2,1,0:T(8,128)(2,1)S(1)} %collective-permute-done.2.refs_1_, ...), custom_call_target="tpu_custom_call" | custom-call | flops 536870912 | tf_op jit(solution)/shard_map/pallas_call | solution.py:523
  66.1 2.0 %collective-permute-start.5 = (bf16[160,128]{1,0:T(8,128)(2,1)S(1)}, bf16[160,128]{1,0:T(8,128)(2,1)S(1)}, u32[]{:S(2)}, u32[]{:S(2)}) collective-permute-start(bf16[160,128]{1,0:T(8,128)(2,1)S(1)} %get-tuple-element.45), channel_id=1, source_target_pairs={{0,2},{2,4},{4,6},{6,8},{8,10},{10,12},{12,14},{14,16},{16,18},{18... | collective-permute-start | bytes 122888 | tf_op jit(solution)/shard_map/ppermute | solution.py:577
  68.1 1.3 %collective-permute-start.6 = (bf16[160,128]{1,0:T(8,128)(2,1)S(1)}, bf16[160,128]{1,0:T(8,128)(2,1)S(1)}, u32[]{:S(2)}, u32[]{:S(2)}) collective-permute-start(bf16[160,128]{1,0:T(8,128)(2,1)S(1)} %get-tuple-element.46), channel_id=1, source_target_pairs={{2,0},{4,2},{6,4},{8,6},{10,8},{12,10},{14,12},{16,14},{18,16},{20... | collective-permute-start | bytes 122888 | tf_op jit(solution)/shard_map/ppermute | solution.py:578
  69.4 0.0 collective-permute-done.5.refs_5_.refs_4_
  69.4 1.8 %collective-permute-done.6.refs_6_.refs_5_ = bf16[160,128]{1,0:T(8,128)(2,1)S(1)} collective-permute-done((bf16[160,128]{1,0:T(8,128)(2,1)S(1)}, bf16[160,128]{1,0:T(8,128)(2,1)S(1)}, u32[]{:S(2)}, u32[]{:S(2)}) %collective-permute-start.6) | collective-permute-done | bytes 40992 | tf_op jit(solution)/shard_map/ppermute | solution.py:578
  71.2 0.0 copy-done
  71.2 1.2 %shard_map.125 = (bf16[512,256]{1,0:T(8,128)(2,1)S(1)}, bf16[512,256]{1,0:T(8,128)(2,1)S(1)}) custom-call(s32[67]{0:T(128)S(1)} %fusion.info, bf16[256,256]{1,0:T(8,128)(2,1)S(1)} %get-tuple-element.42.refs_8_.refs_0_, bf16[256,256]{1,0:T(8,128)(2,1)S(1)} %get-tuple-element.47.refs_1_, bf16[256,256]{1,0:T(8,128)(2,1)S(1)} %get-tuple-element.48.refs_2_, ...), custom_call_target="tpu_custom_call" | custom-call | flops 83886080 | tf_op jit(solution)/shard_map/pallas_call | solution.py:523
  72.4 1.6 %collective-permute-start.8 = (bf16[512,256]{1,0:T(8,128)(2,1)S(1)}, bf16[512,256]{1,0:T(8,128)(2,1)S(1)}, u32[]{:S(2)}, u32[]{:S(2)}) collective-permute-start(bf16[512,256]{1,0:T(8,128)(2,1)S(1)} %get-tuple-element.50), channel_id=1, source_target_pairs={{0,1},{1,0},{2,3},{3,2},{4,5},{5,4},{6,7},{7,6},{8,9},{9,8},{10,11... | collective-permute-start | bytes 786440 | tf_op jit(solution)/shard_map/ppermute | solution.py:594
  74.0 4.2 %shard_map.124 = bf16[512,256]{1,0:T(8,128)(2,1)S(1)} custom-call(s32[67]{0:T(128)S(1)} %fusion.info, f32[4]{0:T(128)S(1)} %copy-done.1, bf16[256,256]{1,0:T(8,128)(2,1)S(1)} %get-tuple-element.28.refs_0_, bf16[256,256]{1,0:T(8,128)(2,1)S(1)} %get-tuple-element.35.refs_1_, bf16[256,256]{1,0:T(8,128)(2,1)S(1)} %get-tuple-element.36.refs_2_, ...), custom_call_target="tpu_custom_call" | custom-call | flops 402653184 | tf_op jit(solution)/shard_map/pallas_call | solution.py:523
  78.2 0.6 collective-permute-start.7
  78.8 4.4 %shard_map.123.refs_0_ = bf16[512,256]{1,0:T(8,128)(2,1)S(1)} custom-call(s32[67]{0:T(128)S(1)} %fusion.info, f32[4]{0:T(128)S(1)} %copy-done.1, bf16[256,256]{1,0:T(8,128)(2,1)S(1)} %get-tuple-element.28.refs_0_, bf16[256,256]{1,0:T(8,128)(2,1)S(1)} %get-tuple-element.35.refs_1_, bf16[256,256]{1,0:T(8,128)(2,1)S(1)} %get-tuple-element.36.refs_2_, ...), custom_call_target="tpu_custom_call" | custom-call | flops 402653184 | tf_op jit(solution)/shard_map/pallas_call | solution.py:523
  83.2 0.0 collective-permute-done.8.refs_3_
  83.2 2.8 %collective-permute-done.7.refs_1_ = bf16[512,256]{1,0:T(8,128)(2,1)S(1)} collective-permute-done((bf16[512,256]{1,0:T(8,128)(2,1)S(1)}, bf16[512,256]{1,0:T(8,128)(2,1)S(1)}, u32[]{:S(2)}, u32[]{:S(2)}) %collective-permute-start.7) | collective-permute-done | bytes 262176 | tf_op jit(solution)/shard_map/ppermute | solution.py:594
  86.0 0.0 collective-permute-done.13.refs_6_
  86.0 0.0 collective-permute-done.14.refs_7_
  86.0 4.7 %shard_map.126 = bf16[512,2048]{1,0:T(8,128)(2,1)} custom-call(s32[67]{0:T(128)S(1)} %fusion.info, bf16[512,256]{1,0:T(8,128)(2,1)S(1)} %shard_map.123.refs_0_, bf16[512,256]{1,0:T(8,128)(2,1)S(1)} %collective-permute-done.7.refs_1_, bf16[512,256]{1,0:T(8,128)(2,1)S(1)} %get-tuple-element.49.refs_2_, bf16[512,256]{1,0:T(8,128)(2,1)S(1)} %collective-permute-done.8.refs_3_, ...), custom_call_target="tpu_custom_call" | custom-call | flops 2147483648 | tf_op jit(solution)/shard_map/pallas_call | solution.py:523
  (3 shorter events, 0.0 us)
Async XLA Ops:
  0.0 7.2 %collective-permute-start.9 = (bf16[1,512,128]{2,1,0:T(8,128)(2,1)}, bf16[1,512,128]{2,1,0:T(8,128)(2,1)S(1)}, u32[]{:S(2)}, u32[]{:S(2)}) collective-permute-start(bf16[1,512,128]{2,1,0:T(8,128)(2,1)} %bitcast.8), channel_id=1, source_target_pairs={{0,16},{1,17},{2,6},{3,7},{4,20},{5,21},{6,2},{7,3},{8,24},{9,25},... | collective-permute-start | bytes 393224 | tf_op jit(solution)/shard_map/ppermute | solution.py:449
  8.2 7.6 %collective-permute-start.10 = (bf16[2,512,128]{2,1,0:T(8,128)(2,1)S(1)}, bf16[2,512,128]{2,1,0:T(8,128)(2,1)S(1)}, u32[]{:S(2)}, u32[]{:S(2)}) collective-permute-start(bf16[2,512,128]{2,1,0:T(8,128)(2,1)S(1)} %pad_maximum_fusion.2), channel_id=1, source_target_pairs={{0,1},{1,0},{2,18},{3,19},{4,5},{5,4},{6,22},{7,23},{8,9},{9,8},{1... | collective-permute-start | bytes 786440 | tf_op jit(solution)/shard_map/ppermute | solution.py:449
  16.8 9.2 %collective-permute-start.11 = (bf16[4,512,128]{2,1,0:T(8,128)(2,1)S(1)}, bf16[4,512,128]{2,1,0:T(8,128)(2,1)S(1)}, u32[]{:S(2)}, u32[]{:S(2)}) collective-permute-start(bf16[4,512,128]{2,1,0:T(8,128)(2,1)S(1)} %pad_maximum_fusion.1), channel_id=1, source_target_pairs={{0,8},{1,9},{2,3},{3,2},{4,12},{5,13},{6,7},{7,6},{8,0},{9,1},{10,... | collective-permute-start | bytes 1572872 | tf_op jit(solution)/shard_map/ppermute | solution.py:449
  27.0 14.9 %collective-permute-start.12 = (bf16[8,512,128]{2,1,0:T(8,128)(2,1)S(1)}, bf16[8,512,128]{2,1,0:T(8,128)(2,1)S(1)}, u32[]{:S(2)}, u32[]{:S(2)}) collective-permute-start(bf16[8,512,128]{2,1,0:T(8,128)(2,1)S(1)} %pad_maximum_fusion.refs_4_), channel_id=1, source_target_pairs={{0,4},{1,5},{2,10},{3,11},{4,0},{5,1},{6,14},{7,15},{8,12},{9,13},... | collective-permute-start | bytes 3145736 | tf_op jit(solution)/shard_map/ppermute | solution.py:449
  30.0 56.0 %collective-permute-start.13 = (bf16[8,512,128]{2,1,0:T(8,128)(2,1)S(1)}, bf16[8,512,128]{2,1,0:T(8,128)(2,1)S(1)}, u32[]{:S(2)}, u32[]{:S(2)}) collective-permute-start(bf16[8,512,128]{2,1,0:T(8,128)(2,1)S(1)} %pad_maximum_fusion.refs_4_), channel_id=1, source_target_pairs={{0,2},{1,3},{2,0},{3,1},{4,6},{5,7},{6,4},{7,5},{8,10},{9,11},{10,... | collective-permute-start | bytes 3145736 | tf_op jit(solution)/shard_map/ppermute | solution.py:449
  41.9 44.1 %collective-permute-start.14 = (bf16[8,512,128]{2,1,0:T(8,128)(2,1)S(1)}, bf16[8,512,128]{2,1,0:T(8,128)(2,1)}, u32[]{:S(2)}, u32[]{:S(2)}) collective-permute-start(bf16[8,512,128]{2,1,0:T(8,128)(2,1)S(1)} %collective-permute-done.12.refs_5_), channel_id=1, source_target_pairs={{0,2},{1,3},{2,0},{3,1},{4,6},{5,7},{6,4},{7,5},{8,10},{9,11},{10,... | collective-permute-start | bytes 3145736 | tf_op jit(solution)/shard_map/ppermute | solution.py:449
  42.0 4.9 %collective-permute-start = (bf16[1,128,128]{2,1,0:T(8,128)(2,1)S(1)}, bf16[1,128,128]{2,1,0:T(8,128)(2,1)S(1)}, u32[]{:S(2)}, u32[]{:S(2)}) collective-permute-start(bf16[1,128,128]{2,1,0:T(8,128)(2,1)S(1)} %maximum_bitcast_fusion), channel_id=1, source_target_pairs={{0,16},{1,17},{2,6},{3,7},{4,20},{5,21},{6,2},{7,3},{8,24},{9,25},... | collective-permute-start | bytes 98312 | tf_op jit(solution)/shard_map/ppermute | solution.py:449
  46.9 4.3 %collective-permute-start.1 = (bf16[2,128,128]{2,1,0:T(8,128)(2,1)S(1)}, bf16[2,128,128]{2,1,0:T(8,128)(2,1)S(1)}, u32[]{:S(2)}, u32[]{:S(2)}) collective-permute-start(bf16[2,128,128]{2,1,0:T(8,128)(2,1)S(1)} %pad_maximum_fusion.4), channel_id=1, source_target_pairs={{0,8},{1,9},{2,18},{3,19},{4,12},{5,13},{6,22},{7,23},{8,0},{9,1},... | collective-permute-start | bytes 196616 | tf_op jit(solution)/shard_map/ppermute | solution.py:449
  51.2 6.4 %collective-permute-start.2 = (bf16[4,128,128]{2,1,0:T(8,128)(2,1)S(1)}, bf16[4,128,128]{2,1,0:T(8,128)(2,1)S(1)}, u32[]{:S(2)}, u32[]{:S(2)}) collective-permute-start(bf16[4,128,128]{2,1,0:T(8,128)(2,1)S(1)} %pad_maximum_fusion.3.refs_0_), channel_id=1, source_target_pairs={{0,4},{1,5},{2,10},{3,11},{4,0},{5,1},{6,14},{7,15},{8,12},{9,13},... | collective-permute-start | bytes 393224 | tf_op jit(solution)/shard_map/ppermute | solution.py:449
  57.5 6.6 %collective-permute-start.3 = (bf16[4,128,128]{2,1,0:T(8,128)(2,1)S(1)}, bf16[4,128,128]{2,1,0:T(8,128)(2,1)S(1)}, u32[]{:S(2)}, u32[]{:S(2)}) collective-permute-start(bf16[4,128,128]{2,1,0:T(8,128)(2,1)S(1)} %pad_maximum_fusion.3.refs_0_), channel_id=1, source_target_pairs={{0,2},{1,3},{2,0},{3,1},{4,6},{5,7},{6,4},{7,5},{8,10},{9,11},{10,... | collective-permute-start | bytes 393224 | tf_op jit(solution)/shard_map/ppermute | solution.py:449
  57.6 6.5 %collective-permute-start.4 = (bf16[4,128,128]{2,1,0:T(8,128)(2,1)S(1)}, bf16[4,128,128]{2,1,0:T(8,128)(2,1)S(1)}, u32[]{:S(2)}, u32[]{:S(2)}) collective-permute-start(bf16[4,128,128]{2,1,0:T(8,128)(2,1)S(1)} %collective-permute-done.2.refs_1_), channel_id=1, source_target_pairs={{0,2},{1,3},{2,0},{3,1},{4,6},{5,7},{6,4},{7,5},{8,10},{9,11},{10,... | collective-permute-start | bytes 393224 | tf_op jit(solution)/shard_map/ppermute | solution.py:449
  64.1 7.2 %copy-start = (f32[256]{0:T(256)S(1)}, f32[256]{0:T(256)}, u32[]{:S(2)}) copy-start(f32[256]{0:T(256)} %param.19) | copy-start | bytes 3076
  64.1 9.9 %copy-start.1 = (f32[4]{0:T(128)S(1)}, f32[4]{0:T(128)}, u32[]{:S(2)}) copy-start(f32[4]{0:T(128)} %sink.3) | copy-start | bytes 52
  66.1 3.3 %collective-permute-start.5 = (bf16[160,128]{1,0:T(8,128)(2,1)S(1)}, bf16[160,128]{1,0:T(8,128)(2,1)S(1)}, u32[]{:S(2)}, u32[]{:S(2)}) collective-permute-start(bf16[160,128]{1,0:T(8,128)(2,1)S(1)} %get-tuple-element.45), channel_id=1, source_target_pairs={{0,2},{2,4},{4,6},{6,8},{8,10},{10,12},{12,14},{14,16},{16,18},{18... | collective-permute-start | bytes 122888 | tf_op jit(solution)/shard_map/ppermute | solution.py:577
  68.1 3.1 %collective-permute-start.6 = (bf16[160,128]{1,0:T(8,128)(2,1)S(1)}, bf16[160,128]{1,0:T(8,128)(2,1)S(1)}, u32[]{:S(2)}, u32[]{:S(2)}) collective-permute-start(bf16[160,128]{1,0:T(8,128)(2,1)S(1)} %get-tuple-element.46), channel_id=1, source_target_pairs={{2,0},{4,2},{6,4},{8,6},{10,8},{12,10},{14,12},{16,14},{18,16},{20... | collective-permute-start | bytes 122888 | tf_op jit(solution)/shard_map/ppermute | solution.py:578
  72.4 10.8 %collective-permute-start.8 = (bf16[512,256]{1,0:T(8,128)(2,1)S(1)}, bf16[512,256]{1,0:T(8,128)(2,1)S(1)}, u32[]{:S(2)}, u32[]{:S(2)}) collective-permute-start(bf16[512,256]{1,0:T(8,128)(2,1)S(1)} %get-tuple-element.50), channel_id=1, source_target_pairs={{0,1},{1,0},{2,3},{3,2},{4,5},{5,4},{6,7},{7,6},{8,9},{9,8},{10,11... | collective-permute-start | bytes 786440 | tf_op jit(solution)/shard_map/ppermute | solution.py:594
  78.2 7.8 %collective-permute-start.7 = (bf16[512,256]{1,0:T(8,128)(2,1)S(1)}, bf16[512,256]{1,0:T(8,128)(2,1)S(1)}, u32[]{:S(2)}, u32[]{:S(2)}) collective-permute-start(bf16[512,256]{1,0:T(8,128)(2,1)S(1)} %shard_map.124), channel_id=1, source_target_pairs={{0,1},{1,0},{2,3},{3,2},{4,5},{5,4},{6,7},{7,6},{8,9},{9,8},{10,11... | collective-permute-start | bytes 786440 | tf_op jit(solution)/shard_map/ppermute | solution.py:594

commit v3 on v0

--- a/solution.py
+++ b/solution.py
@@ -1,6 +1,11 @@
+import functools
+
 import jax
 import jax.numpy as jnp
+import numpy as np
 from jax import lax
+from jax.experimental import pallas as pl
+from jax.experimental.pallas import tpu as pltpu
 from jax.sharding import PartitionSpec as P
 
 HEAD = 64
@@ -48,7 +53,7 @@
     )
 
 
-def body(tokens, norm_gain, w_query, w_key, w_value, w_pool_in, sink_logit, pool_scale, w_out):
+def plain_body(tokens, norm_gain, w_query, w_key, w_value, w_pool_in, sink_logit, pool_scale, w_out):
     local_rows = tokens.shape[0]
     seq_total = local_rows * lax.axis_size("sp")
     offset = lax.axis_index("sp") * local_rows
@@ -142,6 +147,559 @@
     return projected.astype(jnp.bfloat16)
 
 
+LANES = 128
+ROW_TILE = 256
+GRANT = 16 * 1024 * 1024
+BF16 = jnp.bfloat16
+F32 = jnp.float32
+
+
+def whole():
+    return pl.BlockSpec(memory_space=pltpu.VMEM)
+
+
+def aligned(start, size=QB, multiple=QB):
+    return pl.ds(pl.multiple_of(start, multiple), size)
+
+
+def here():
+    return lax.axis_index("sp"), lax.axis_index("tp")
+
+
+def rope_angles(block, base, blocks):
+    (cosine, sine), row = (base[0], base[1]), pl.ds(block, 1)
+    turn, lift = blocks[0, row, :], blocks[1, row, :]
+    return cosine * turn - sine * lift, sine * turn + cosine * lift
+
+
+def rope_lanes(values, angles):
+    lane = lax.broadcasted_iota(jnp.int32, values.shape, 1)
+    swapped = jnp.where(
+        lane % HEAD < HEAD // 2,
+        -pltpu.roll(values, LANES - HEAD // 2, 1),
+        pltpu.roll(values, HEAD // 2, 1),
+    )
+    return values * angles[0] + swapped * angles[1]
+
+
+def norm_kernel(*refs):
+    (tokens, gain, *shared), (normed, *kept), (rows, scale, sems) = refs[:6], refs[6:11], refs[11:]
+    tiles = tokens.shape[0] // ROW_TILE
+
+    def tile(ref, index):
+        return ref.at[index * ROW_TILE : (index + 1) * ROW_TILE, :]
+
+    pairs = [(gain, scale)] + [(tile(tokens, index), tile(rows, index)) for index in range(tiles)]
+    pairs += list(zip(shared, kept))
+    copies = [pltpu.make_async_copy(*pair, sems.at[index]) for index, pair in enumerate(pairs)]
+    for copy in copies:
+        copy.start()
+    copies[0].wait()
+    for index in range(tiles):
+        copies[1 + index].wait()
+
+        for row in range(index * ROW_TILE, (index + 1) * ROW_TILE, 16):
+            place = slice(row, row + 16)
+            values = rows[place, :].astype(F32)
+            centred = values - jnp.mean(values, axis=-1, keepdims=True)
+            spread = jnp.mean(centred * centred, axis=-1, keepdims=True)
+            normed[place, :] = (centred * lax.rsqrt(spread + 1e-06) * scale[...]).astype(BF16)
+
+    for copy in copies[1 + tiles :]:
+        copy.wait()
+
+
+def band(group, groups, edge):
+    row = lax.broadcasted_iota(jnp.int32, (QB, QB + 2 * edge), 0) + edge
+    column = lax.broadcasted_iota(jnp.int32, (QB, QB + 2 * edge), 1)
+    reach = lax.shift_left(jnp.int32(1), here()[1] * groups + group)
+    inside = (column >= row - reach) & (column < row + reach)
+    return reach, jnp.where(inside, 1.0, 0.0).astype(BF16)
+
+
+def inner_blocks(blocks):
+    half = blocks // 2
+    tp = here()[1]
+    return half - 1, (jnp.where(tp == 1, 1, half), jnp.where(tp == 0, 1, half))
+
+
+def pool_kernel(edge, normed, w_pool, scale, pool, *outs):
+    rows, channels = pool.shape
+    weight = w_pool[...]
+
+    @pl.loop(0, rows // ROW_TILE)
+    def _(tile):
+        place = aligned(tile * ROW_TILE, ROW_TILE)
+        pool[place, :] = jnp.dot(normed[place, :], weight, preferred_element_type=F32).astype(BF16)
+
+    groups = channels // LANES
+    bands = [band(group, groups, edge) for group in range(groups)]
+    count, firsts = inner_blocks(rows // QB)
+    for first, out in zip(firsts, outs):
+
+        @pl.loop(0, count)
+        def _(step, first=first, out=out):
+            start = (first + step) * QB
+            for group, (reach, inside) in enumerate(bands):
+                lanes = slice(group * LANES, (group + 1) * LANES)
+                wide = pool[aligned(start - edge, QB + 2 * edge, edge), lanes]
+                sums = jnp.dot(inside, wide, preferred_element_type=F32)
+                own = pool[aligned(start), lanes].astype(F32)
+                mean = sums * (0.5 / lax.convert_element_type(reach, F32))
+                out[aligned(step * QB), lanes] = ((mean - own) * scale[:, lanes]).astype(BF16)
+
+
+def query_kernel(normed, w_query, base, blocks, query):
+    weight = w_query[...]
+    first = here()[0] * (query.shape[0] // QB)
+
+    @pl.loop(0, query.shape[0] // ROW_TILE)
+    def _(tile):
+        products = jnp.dot(
+            normed[aligned(tile * ROW_TILE, ROW_TILE), :], weight, preferred_element_type=F32
+        )
+        for row in range(0, ROW_TILE, QB):
+            angles = rope_angles(first + tile * (ROW_TILE // QB) + row // QB, base, blocks)
+            for lane in range(0, query.shape[1], LANES):
+                turned = rope_lanes(products[row : row + QB, lane : lane + LANES], angles)
+                query[aligned(tile * ROW_TILE + row), lane : lane + LANES] = (
+                    turned.astype(BF16) * HEAD ** (-0.5)
+                )
+
+
+def key_value_kernel(orders, sp_step, *refs):
+    pieces, (normed, pool, base, blocks) = refs[:2], refs[2:6]
+    key_value, first_out, second_out, weight = refs[6:]
+    sp = here()[0]
+    odd = sp % 2
+    depth = pieces[0].shape[1]
+    for flip, piece in enumerate(pieces):
+        for slot, masks in enumerate(zip(*(slot_masks(order) for order in orders))):
+            even_mask, odd_mask = (mask // sp_step for mask in masks)
+            picked = jnp.where(odd == flip, even_mask, odd_mask)
+            place = lax.bitwise_xor(sp, lax.bitwise_xor(picked, flip))
+            weight[aligned(place * depth, depth), :] = piece[slot]
+    right = weight[...]
+    rows = key_value.shape[0]
+
+    @pl.loop(0, rows // ROW_TILE)
+    def _(tile):
+        place = aligned(tile * ROW_TILE, ROW_TILE)
+        products = jnp.dot(normed[place, :], right, preferred_element_type=F32)
+        lane = lax.broadcasted_iota(jnp.int32, (QB, LANES), 1)
+        for row in range(0, ROW_TILE, QB):
+            block = tile * (ROW_TILE // QB) + row // QB
+            angles = rope_angles(sp * (rows // QB) + block, base, blocks)
+            plain = products[row : row + QB, :]
+            result = jnp.where(lane < HEAD, rope_lanes(plain, angles), plain).astype(BF16)
+            key_value[aligned(block * QB), :] = result
+
+    groups = pool.shape[1] // LANES
+    edge = (first_out.shape[0] - WINDOW) // groups
+    for parity, (head, tail) in enumerate(((second_out, first_out), (first_out, second_out))):
+
+        @pl.when(odd == parity)
+        def _(head=head, tail=tail):
+            head[:WINDOW, :] = key_value[:WINDOW, :]
+            tail[:WINDOW, :] = key_value[rows - WINDOW :, :]
+            for group in range(groups):
+                lanes = slice(group * LANES, (group + 1) * LANES)
+                place = slice(WINDOW + group * edge, WINDOW + (group + 1) * edge)
+                head[place, :] = pool[:edge, lanes]
+                tail[place, :] = pool[rows - edge :, lanes]
+
+
+def split_halves(rows):
+    wide = rows.astype(F32)
+    first = lax.broadcasted_iota(jnp.int32, wide.shape, 1) < HEAD
+    turned = pltpu.roll(wide, HEAD, 1)
+    return jnp.where(first, wide, turned).astype(BF16), jnp.where(first, turned, wide).astype(BF16)
+
+
+def attend_block(queries, keys, values, low_ok, high_ok, sink):
+    first = lax.broadcasted_iota(jnp.int32, (QB, LANES), 1) < HEAD
+    zero = jnp.zeros((QB, LANES), BF16)
+    split = []
+    for start in range(0, queries.shape[1], LANES):
+        pair = queries[:, start : start + LANES]
+        split += [jnp.where(first, pair, zero), jnp.where(first, zero, pair)]
+    scores = lax.dot_general(
+        jnp.concatenate(split, axis=0),
+        keys,
+        (((1,), (1,)), ((), ())),
+        preferred_element_type=F32,
+    )
+    masked, weights = [], []
+    for head in range(len(split)):
+        part = scores[head * QB : (head + 1) * QB, :]
+        parts = (
+            jnp.where(low_ok, part[:, :WINDOW], NEG_BIG),
+            part[:, WINDOW : WINDOW + QB],
+            jnp.where(high_ok, part[:, WINDOW + QB :], NEG_BIG),
+        )
+        top = jnp.maximum(jnp.maximum(parts[0], parts[1]), parts[2])
+        masked.append((parts, jnp.maximum(jnp.max(top, axis=-1, keepdims=True), sink[head])))
+    for head, (parts, top) in enumerate(masked):
+        expo = [jnp.exp(part - top) for part in parts]
+        total = jnp.sum(expo[0] + expo[1] + expo[2], axis=-1, keepdims=True)
+        inverse = 1.0 / (total + jnp.exp(sink[head] - top))
+        weights.append(jnp.concatenate([(part * inverse).astype(BF16) for part in expo], axis=1))
+    result = jnp.dot(jnp.concatenate(weights, axis=0), values, preferred_element_type=F32)
+    heads = [result[head * QB : (head + 1) * QB, :] for head in range(len(split))]
+    pairs = [jnp.where(first, *pair).astype(BF16) for pair in zip(heads[::2], heads[1::2])]
+    return jnp.concatenate(pairs, axis=1)
+
+
+def inside_window():
+    row = lax.broadcasted_iota(jnp.int32, (QB, WINDOW), 0)
+    column = lax.broadcasted_iota(jnp.int32, (QB, WINDOW), 1)
+    return column >= row, column <= row
+
+
+def inner_kernel(sink, query, key_value, given, kept, keys, values):
+    blocks = query.shape[0] // QB
+
+    @pl.loop(0, blocks)
+    def _(block):
+        place = aligned(block * QB)
+        keys[place, :], values[place, :] = split_halves(key_value[place, :])
+
+    low_ok, high_ok = inside_window()
+    count, firsts = inner_blocks(blocks)
+
+    @pl.loop(0, count)
+    def _(step):
+        for first, out in zip(firsts, (given, kept)):
+            block = first + step
+            span = aligned((block - 1) * QB, QB + 2 * WINDOW)
+            out[aligned(step * QB), :] = attend_block(
+                query[aligned(block * QB), :], keys[span, :], values[span, :], low_ok, high_ok, sink
+            )
+
+
+def outer_kernel(sp_count, sink, query, key_value, pool, scale, first, second, *outs):
+    sp, tp = here()
+    even = sp % 2 == 0
+    rows, channels = pool.shape
+    heads_width = query.shape[1]
+    last = rows // QB - 1
+    groups = channels // LANES
+    edge = (first.shape[0] - WINDOW) // groups
+    low_inside, high_inside = inside_window()
+    bands = [band(group, groups, edge) for group in range(groups)]
+    for step, out in enumerate(outs):
+        at_front = lax.bitwise_xor(tp, step) == 1
+        block = jnp.where(at_front, 0, last)
+        coming = jnp.where(even == at_front, second[...], first[...])
+        ahead, behind = key_value[: 2 * QB, :], key_value[rows - 2 * QB :, :]
+        thirds = (
+            jnp.where(at_front, coming[:WINDOW, :], behind[:QB, :]),
+            jnp.where(at_front, ahead[:QB, :], behind[QB:, :]),
+            jnp.where(at_front, ahead[QB:, :], coming[:WINDOW, :]),
+        )
+        keys, values = split_halves(jnp.concatenate(thirds, axis=0))
+        low_ok = low_inside & jnp.logical_not(at_front & (sp == 0))
+        high_ok = high_inside & (at_front | (sp != sp_count - 1))
+        out[:, :heads_width] = attend_block(
+            query[aligned(block * QB), :], keys, values, low_ok, high_ok, sink
+        )
+        position = sp * rows + block * QB + lax.broadcasted_iota(jnp.int32, (QB, 1), 0)
+        for group, (reach, inside) in enumerate(bands):
+            lanes = slice(group * LANES, (group + 1) * LANES)
+            place = slice(WINDOW + group * edge, WINDOW + (group + 1) * edge)
+            near, far = pool[: QB + edge, lanes], pool[rows - QB - edge :, lanes]
+            front = jnp.concatenate([coming[place, :], near], axis=0)
+            back = jnp.concatenate([far, coming[place, :]], axis=0)
+            sums = jnp.dot(inside, jnp.where(at_front, front, back), preferred_element_type=F32)
+            counted = jnp.minimum(position + reach, sp_count * rows) - jnp.maximum(
+                position - reach, 0
+            )
+            mean = sums * (1.0 / counted.astype(F32))
+            own = pool[aligned(block * QB), lanes].astype(F32)
+            start = heads_width + group * LANES
+            out[:, start : start + LANES] = ((mean - own) * scale[:, lanes]).astype(BF16)
+
+
+def join_kernel(*refs):
+    parts, joined = refs[:6], refs[6]
+    tp = here()[1]
+    inner, width = parts[0].shape
+    count = joined.shape[0] - inner
+    inner_rows = aligned((1 - tp) * count, inner)
+    edge_rows = aligned(tp * inner, count)
+    for side, (attended, pooled, edges) in enumerate((parts[:3], parts[3:])):
+        owner = lax.bitwise_xor(tp, side)
+        for half, part in enumerate((attended, pooled)):
+            columns = pl.ds(pl.multiple_of((half * 2 + owner) * width, LANES), width)
+            joined[inner_rows, columns] = part[...]
+            joined[edge_rows, columns] = edges[:, half * width : (half + 1) * width]
+
+
+def output_kernel(pieces, joined_parts, *refs):
+    count = len(pieces)
+    sources, refs = refs[:count], refs[count:]
+    if joined_parts:
+        parts, (out, joined, staged, sems) = refs[:6], refs[6:]
+        join_kernel(*parts, joined)
+    else:
+        joined, _, out, staged, sems = refs
+    sp, tp = here()
+    depth, lanes = sources[0].shape[1], sources[0].shape[2]
+    pairs = sources[0].shape[0] // 4
+    stores = []
+
+    def store(number, column):
+        start = pl.multiple_of(column * lanes, LANES)
+        return pltpu.make_async_copy(
+            staged.at[number], out.at[:, pl.ds(start, lanes)], sems.at[number]
+        )
+
+    for index, (source, (flip, tables)) in enumerate(zip(sources, pieces)):
+        kind = lax.bitwise_xor(sp % 2, flip)
+
+        def entry(column, field, tables=tables, kind=kind):
+            picked = jnp.int32(0)
+            for place, values in enumerate(zip(*tables)):
+                value = jnp.where(kind == 0, values[0][field], values[1][field])
+                picked = jnp.where(column == place, value, picked)
+            return picked
+
+        @pl.loop(0, pairs)
+        def _(pair, index=index, source=source, entry=entry, flip=flip):
+            total = None
+            for side in range(2):
+                start = pl.multiple_of(lax.bitwise_xor(tp, side) * depth, LANES)
+                right = jnp.concatenate(
+                    [source[entry(2 * pair + half, 1 + side)] for half in range(2)], axis=1
+                )
+                product = jnp.dot(
+                    joined[:, pl.ds(start, depth)], right, preferred_element_type=F32
+                )
+                total = product if total is None else total + product
+            for half in range(2):
+                number = index * 2 * pairs + 2 * pair + half
+                staged[number] = total[:, half * lanes : (half + 1) * lanes].astype(BF16)
+                delta = lax.bitwise_xor(entry(2 * pair + half, 0), flip)
+                store(number, lax.bitwise_xor(sp, delta)).start()
+
+        stores += [index * 2 * pairs + number for number in range(2 * pairs)]
+    for number in stores:
+        store(number, 0).wait()
+
+
+def exchange_orders(sp_count, tp_count):
+    sp_bits = [tp_count << bit for bit in range(1, sp_count.bit_length() - 1)][::-1]
+    tp_bits = [1 << bit for bit in range(tp_count.bit_length() - 1)]
+    mixed = sp_bits[:1] + tp_bits + sp_bits[1:]
+    return (sp_bits[-1:] + sp_bits[:-1], sp_bits), (mixed, mixed[-1:] + mixed[:-1])
+
+
+def slot_masks(bits):
+    masks = [0]
+    for bit in bits:
+        masks = masks + [mask ^ bit for mask in masks]
+    return masks
+
+
+def output_tables(orders, late, tp_count):
+    tables = []
+    for order in orders:
+        found = {}
+        for slot, mask in enumerate(slot_masks(order[:-1])):
+            delta, step = divmod(mask ^ (order[-1] * late), tp_count)
+            found.setdefault(delta, {})[step] = slot
+        tables.append([[delta, *(slots[t] for t in range(tp_count))] for delta, slots in found.items()])
+    return tables
+
+
+def doubled(block, orders, sp_count, tp_count, together):
+    even, odd = orders
+    devices = range(sp_count * tp_count)
+
+    def send(array, masks):
+        pairs = [(i, i ^ masks[(i // tp_count) & 1]) for i in devices]
+        return lax.ppermute(array, ("sp", "tp"), pairs)
+
+    held = block[None]
+    for masks in zip(even[:-1], odd[:-1]):
+        held = jnp.concatenate([held, send(held, masks)], axis=0)
+    core = (tp_count, tp_count)
+    came = send(held, (even[-1], odd[-1]))
+    if together:
+        held = jnp.concatenate([held, came], axis=0)
+        return held, send(held, core)
+    return held, came, send(held, core), send(came, core)
+
+
+def rope_tables(length):
+    half = HEAD // 2
+    inverse = np.float32(10000.0) ** (-np.arange(half, dtype=np.float32) / np.float32(half))
+    inverse = np.tile(inverse.astype(np.float64), LANES // half)
+    tables = []
+    for positions in (np.arange(QB), np.arange(0, length, QB)):
+        angles = positions[:, None] * inverse[None, :]
+        tables.append(np.stack([np.cos(angles), np.sin(angles)]).astype(np.float32))
+    return tables
+
+
+def call(kernel, operands, outs, scratch, flops, scalar=0, space=pltpu.VMEM, **more):
+    specs = [pl.BlockSpec(memory_space=pltpu.SMEM)] * scalar
+    specs += [whole()] * (len(operands) - scalar)
+    shapes = [jax.ShapeDtypeStruct(shape, dtype) for shape, dtype in outs]
+    return pl.pallas_call(
+        kernel,
+        in_specs=more.pop("in_specs", specs),
+        out_specs=[pl.BlockSpec(memory_space=space)] * len(shapes),
+        out_shape=shapes,
+        scratch_shapes=scratch,
+        compiler_params=pltpu.CompilerParams(vmem_limit_bytes=GRANT),
+        cost_estimate=pl.CostEstimate(flops=flops, bytes_accessed=0, transcendentals=0),
+        **more,
+    )(*operands)
+
+
+def fast_body(tokens, norm_gain, w_query, w_key, w_value, w_pool_in, sink_logit, pool_scale, w_out):
+    sp_count, tp_count = lax.axis_size("sp"), lax.axis_size("tp")
+    rows, width = tokens.shape
+    heads_width, channels = w_query.shape[1], w_pool_in.shape[1]
+    kv_orders, out_orders = exchange_orders(sp_count, tp_count)
+
+    key_head = lax.axis_index("tp") * (heads_width // HEAD) // (QH // KVH)
+    kv_block = jnp.concatenate(
+        [lax.dynamic_slice_in_dim(w, key_head * HEAD, HEAD, 1) for w in (w_key, w_value)], axis=1
+    )
+    kv_pieces = doubled(kv_block, kv_orders, sp_count, tp_count, True)
+    out_pieces = doubled(w_out, out_orders, sp_count, tp_count, False)
+
+    base, blocks = (jnp.array(table) for table in rope_tables(rows * sp_count))
+    edge = 2 * (POOL_SPANS[-1] // 2)
+    inner = rows // 2 - QB
+    scale = pool_scale[None, :]
+
+    loaded = (tokens, norm_gain[None, :], w_query, w_pool_in, base, blocks)
+    loaded = [pltpu.with_memory_space_constraint(part, pltpu.HBM) for part in loaded]
+    normed, w_query, w_pool_in, base, blocks = call(
+        norm_kernel,
+        loaded,
+        [(tokens.shape, BF16)] + [(part.shape, part.dtype) for part in loaded[2:]],
+        [
+            pltpu.VMEM(tokens.shape, BF16),
+            pltpu.VMEM((1, width), F32),
+            pltpu.SemaphoreType.DMA((5 + rows // ROW_TILE,)),
+        ],
+        2 * rows * width * heads_width,
+        in_specs=[pl.BlockSpec(memory_space=pltpu.HBM)] * 6,
+    )
+    pool, pooled_given, pooled = call(
+        functools.partial(pool_kernel, edge),
+        (normed, w_pool_in, scale),
+        [((rows, channels), BF16)] + [((inner, channels), BF16)] * 2,
+        [],
+        2 * rows * width * channels,
+    )
+    (query,) = call(
+        query_kernel,
+        (normed, w_query, base, blocks),
+        [((rows, heads_width), BF16)],
+        [],
+        2 * rows * width * heads_width,
+    )
+    payload = (WINDOW + edge * (channels // LANES), LANES)
+    key_value, first, second = call(
+        functools.partial(key_value_kernel, kv_orders, tp_count),
+        (*kv_pieces, normed, pool, base, blocks),
+        [((rows, LANES), BF16), (payload, BF16), (payload, BF16)],
+        [pltpu.VMEM((width, LANES), BF16)],
+        2 * rows * width * LANES,
+    )
+
+    across = [(i, i ^ 1) for i in range(sp_count)]
+    between = [(i, i + 1) for i in range(1, sp_count - 1, 2)]
+    first = lax.ppermute(first, "sp", across)
+    second = lax.ppermute(second, "sp", between + [(b, a) for a, b in between])
+
+    flops = 4 * rows * 3 * WINDOW * LANES * (heads_width // HEAD)
+    given, attended = call(
+        inner_kernel,
+        (sink_logit, query, key_value),
+        [((inner, heads_width), BF16)] * 2,
+        [pltpu.VMEM((rows, LANES), BF16)] * 2,
+        flops,
+        scalar=1,
+    )
+    edge_given, edges = call(
+        functools.partial(outer_kernel, sp_count),
+        (sink_logit, query, key_value, pool, scale, first, second),
+        [((QB, heads_width + channels), BF16)] * 2,
+        [],
+        flops // 3,
+        scalar=1,
+    )
+    other = [(0, 1), (1, 0)]
+    pooled_came = lax.ppermute(pooled_given, "tp", other)
+    attended_came = lax.ppermute(given, "tp", other)
+    edges_came = lax.ppermute(edge_given, "tp", other)
+
+    columns = w_out.shape[1] * sp_count
+    tables = [
+        (flip, output_tables(out_orders, late, tp_count)) for flip in range(2) for late in range(2)
+    ]
+    parts = (attended, pooled, edges, attended_came, pooled_came, edges_came)
+    held, came, early, late = out_pieces
+    flops = rows * columns * w_out.shape[0]
+    staged = (sp_count // 4, rows // 2, w_out.shape[1])
+    shape = (rows // 2, columns)
+    in_hbm, in_vmem = pl.BlockSpec(memory_space=pltpu.HBM), whole()
+    out, joined = pl.pallas_call(
+        functools.partial(output_kernel, [tables[0], tables[2], tables[1]], True),
+        in_specs=[in_vmem] * 9,
+        out_specs=[in_hbm, in_vmem],
+        out_shape=[
+            jax.ShapeDtypeStruct(shape, BF16),
+            jax.ShapeDtypeStruct((rows // 2, 2 * w_out.shape[0]), BF16),
+        ],
+        scratch_shapes=[
+            pltpu.VMEM((3 * staged[0],) + staged[1:], BF16),
+            pltpu.SemaphoreType.DMA((3 * staged[0],)),
+        ],
+        compiler_params=pltpu.CompilerParams(vmem_limit_bytes=GRANT),
+        cost_estimate=pl.CostEstimate(flops=flops, bytes_accessed=0, transcendentals=0),
+        name="output",
+    )(held, early, came, *parts)
+    return pl.pallas_call(
+        functools.partial(output_kernel, [tables[3]], False),
+        in_specs=[in_vmem, in_vmem, in_hbm],
+        out_specs=in_hbm,
+        out_shape=jax.ShapeDtypeStruct(shape, BF16),
+        input_output_aliases={2: 0},
+        scratch_shapes=[pltpu.VMEM(staged, BF16), pltpu.SemaphoreType.DMA((staged[0],))],
+        compiler_params=pltpu.CompilerParams(vmem_limit_bytes=GRANT),
+        cost_estimate=pl.CostEstimate(flops=flops // 3, bytes_accessed=0, transcendentals=0),
+        name="finish",
+    )(late, joined, out)
+
+
+def tiled(rows, w_query, w_pool_in, w_out):
+    sp_count, tp_count = lax.axis_size("sp"), lax.axis_size("tp")
+    return (
+        sp_count & (sp_count - 1) == 0
+        and sp_count >= 8
+        and tp_count == 2
+        and rows % (2 * ROW_TILE) == 0
+        and 2 * w_query.shape[1] == QH * HEAD
+        and w_query.shape[1] == w_pool_in.shape[1]
+        and w_pool_in.shape[1] % LANES == 0
+        and w_out.shape[1] % LANES == 0
+    )
+
+
+def body(*args):
+    tokens, w_query, w_pool_in, w_out = args[0], args[2], args[5], args[8]
+    if tiled(tokens.shape[0], w_query, w_pool_in, w_out):
+        return fast_body(*args)
+    return plain_body(*args)
+
+
 def solution(mesh):
     in_specs = (
         P("sp", None),

time: 168 us -> 89.1 us (0.53)
  the two profiles are of different devices: /device:TPU:0 before, /device:TPU:25 now
where the time goes in v3:
time: 89.1 us; the launch traced here: 88.8 us
  waiting for transfers between devices  38.4 us (43%)
  Pallas kernels  23.8 us (27%)
  starting transfers between devices  22.6 us (25%)
  other arithmetic  3.03 us (3%)
    ppermute x10, waiting for transfers between devices, send(): return lax.ppermute(array, ('sp', 'tp'), pairs)  32.3 us
    pallas_call x6, Pallas kernels, call(): pl.pallas_call(kernel, in_specs=more.pop('in_specs', specs), out_specs=[p...  18.4 us
    ppermute x10, starting transfers between devices, send(): return lax.ppermute(array, ('sp', 'tp'), pairs)  16.1 us
    ppermute x1, waiting for transfers between devices, fast_body(): edges_came = lax.ppermute(edge_given, 'tp', other)  6.02 us
    pallas_call x1, Pallas kernels, fast_body(): pl.pallas_call(functools.partial(output_kernel, [tables[0], tables[2], ta...  3.75 us
    ppermute x1, starting transfers between devices, fast_body(): second = lax.ppermute(second, 'sp', between + [(b, a) for a, b in between])  3.23 us
    concatenate x5, other arithmetic, doubled(): held = jnp.concatenate([held, send(held, masks)], axis=0)  2.92 us
  transfers between devices with their start and end apart: 15, of which 6 were waited for; matrix products, arithmetic and copies ran while one was open for 1% of the time, Pallas kernels for 25%

profile of v3, /device:TPU:25, one launch (start us, length us, event | category | flops | bytes accessed | tf_op | source)
XLA Modules:
  0.0 88.8 jit_solution(8040575139571871039)
XLA Ops:
  0.0 1.2 %collective-permute-start = (bf16[1,512,128]{2,1,0:T(8,128)(2,1)}, bf16[1,512,128]{2,1,0:T(8,128)(2,1)S(1)}, u32[]{:S(2)}, u32[]{:S(2)}) collective-permute-start(bf16[1,512,128]{2,1,0:T(8,128)(2,1)} %bitcast.7), channel_id=1, source_target_pairs={{0,16},{1,17},{2,6},{3,7},{4,20},{5,21},{6,2},{7,3},{8,24},{9,25},... | collective-permute-start | bytes 393224 | tf_op jit(solution)/shard_map/ppermute | solution.py:521
  1.2 2.8 %collective-permute-done = bf16[1,512,128]{2,1,0:T(8,128)(2,1)S(1)} collective-permute-done((bf16[1,512,128]{2,1,0:T(8,128)(2,1)}, bf16[1,512,128]{2,1,0:T(8,128)(2,1)S(1)}, u32[]{:S(2)}, u32[]{:S(2)}) %collective-permute-start) | collective-permute-done | bytes 131104 | tf_op jit(solution)/shard_map/ppermute | solution.py:521
  4.0 0.9 %pad_maximum_fusion.2 = bf16[2,512,128]{2,1,0:T(8,128)(2,1)S(1)} fusion(bf16[1,512,128]{2,1,0:T(8,128)(2,1)S(1)} %collective-permute-done, bf16[1,512,128]{2,1,0:T(8,128)(2,1)} %bitcast.8), kind=kLoop, calls=%fused_computation.2 | loop fusion | flops 131072 | bytes 524288 | tf_op jit(solution)/shard_map/concatenate | solution.py:525
  5.0 0.1 collective-permute-start.1
  5.1 8.8 %collective-permute-done.1 = bf16[2,512,128]{2,1,0:T(8,128)(2,1)S(1)} collective-permute-done((bf16[2,512,128]{2,1,0:T(8,128)(2,1)S(1)}, bf16[2,512,128]{2,1,0:T(8,128)(2,1)S(1)}, u32[]{:S(2)}, u32[]{:S(2)}) %collective-permute-start.1) | collective-permute-done | bytes 262176 | tf_op jit(solution)/shard_map/ppermute | solution.py:521
  13.8 1.0 %pad_maximum_fusion.1 = bf16[4,512,128]{2,1,0:T(8,128)(2,1)S(1)} fusion(bf16[2,512,128]{2,1,0:T(8,128)(2,1)S(1)} %collective-permute-done.1, bf16[1,512,128]{2,1,0:T(8,128)(2,1)S(1)} %collective-permute-done, bf16[1,512,128]{2,1,0:T(8,128)(2,1)} %bitcast.9), kind=kLoop, calls=%fused_computation.1 | loop fusion | flops 524288 | bytes 1048576 | tf_op jit(solution)/shard_map/concatenate | solution.py:525
  14.8 1.3 %collective-permute-start.2 = (bf16[4,512,128]{2,1,0:T(8,128)(2,1)S(1)}, bf16[4,512,128]{2,1,0:T(8,128)(2,1)S(1)}, u32[]{:S(2)}, u32[]{:S(2)}) collective-permute-start(bf16[4,512,128]{2,1,0:T(8,128)(2,1)S(1)} %pad_maximum_fusion.1), channel_id=1, source_target_pairs={{0,8},{1,9},{2,3},{3,2},{4,12},{5,13},{6,7},{7,6},{8,0},{9,1},{10,... | collective-permute-start | bytes 1572872 | tf_op jit(solution)/shard_map/ppermute | solution.py:521
  16.1 7.1 %collective-permute-done.2 = bf16[4,512,128]{2,1,0:T(8,128)(2,1)S(1)} collective-permute-done((bf16[4,512,128]{2,1,0:T(8,128)(2,1)S(1)}, bf16[4,512,128]{2,1,0:T(8,128)(2,1)S(1)}, u32[]{:S(2)}, u32[]{:S(2)}) %collective-permute-start.2) | collective-permute-done | bytes 524320 | tf_op jit(solution)/shard_map/ppermute | solution.py:521
  23.2 1.0 %pad_maximum_fusion.refs_0_ = bf16[8,512,128]{2,1,0:T(8,128)(2,1)S(1)} fusion(bf16[4,512,128]{2,1,0:T(8,128)(2,1)S(1)} %collective-permute-done.2, bf16[2,512,128]{2,1,0:T(8,128)(2,1)S(1)} %collective-permute-done.1, bf16[1,512,128]{2,1,0:T(8,128)(2,1)S(1)} %collective-permute-done, bf16[1,512,128]{2,1,0:T(8,128)(2,1)} %bitcast.10), kind=kLoop, calls=%fused_computation | loop fusion | flops 1572864 | bytes 2097152 | tf_op jit(solution)/shard_map/concatenate | solution.py:525
  24.2 0.0 copy-start
  24.2 0.1 collective-permute-start.3
  24.3 0.9 constant_dynamic-slice_fusion
  25.2 0.1 maximum_bitcast_fusion
  25.3 0.3 collective-permute-start.6
  25.6 10.8 %collective-permute-done.6 = bf16[1,128,128]{2,1,0:T(8,128)(2,1)S(1)} collective-permute-done((bf16[1,128,128]{2,1,0:T(8,128)(2,1)S(1)}, bf16[1,128,128]{2,1,0:T(8,128)(2,1)S(1)}, u32[]{:S(2)}, u32[]{:S(2)}) %collective-permute-start.6) | collective-permute-done | bytes 32800 | tf_op jit(solution)/shard_map/ppermute | solution.py:521
  36.4 1.5 %collective-permute-start.7 = (bf16[2,128,128]{2,1,0:T(8,128)(2,1)S(1)}, bf16[2,128,128]{2,1,0:T(8,128)(2,1)S(1)}, u32[]{:S(2)}, u32[]{:S(2)}) collective-permute-start(bf16[2,128,128]{2,1,0:T(8,128)(2,1)S(1)} %pad_maximum_fusion.5), channel_id=1, source_target_pairs={{0,16},{1,17},{2,10},{3,11},{4,20},{5,21},{6,14},{7,15},{8,24},{9,... | collective-permute-start | bytes 196616 | tf_op jit(solution)/shard_map/ppermute | solution.py:521
  37.9 4.1 %collective-permute-start.5 = (bf16[8,512,128]{2,1,0:T(8,128)(2,1)S(1)}, bf16[8,512,128]{2,1,0:T(8,128)(2,1)S(1)}, u32[]{:S(2)}, u32[]{:S(2)}) collective-permute-start(bf16[8,512,128]{2,1,0:T(8,128)(2,1)S(1)} %pad_maximum_fusion.refs_0_), channel_id=1, source_target_pairs={{0,2},{1,3},{2,0},{3,1},{4,6},{5,7},{6,4},{7,5},{8,10},{9,11},{10,... | collective-permute-start | bytes 3145736 | tf_op jit(solution)/shard_map/ppermute | solution.py:521
  42.0 0.0 collective-permute-done.3.refs_2_
  42.0 0.1 collective-permute-start.4
  42.1 0.0 collective-permute-done.7
  42.1 1.3 %collective-permute-start.8 = (bf16[4,128,128]{2,1,0:T(8,128)(2,1)S(1)}, bf16[4,128,128]{2,1,0:T(8,128)(2,1)S(1)}, u32[]{:S(2)}, u32[]{:S(2)}) collective-permute-start(bf16[4,128,128]{2,1,0:T(8,128)(2,1)S(1)} %pad_maximum_fusion.4), channel_id=1, source_target_pairs={{0,8},{1,9},{2,6},{3,7},{4,12},{5,13},{6,2},{7,3},{8,0},{9,1},{10,... | collective-permute-start | bytes 393224 | tf_op jit(solution)/shard_map/ppermute | solution.py:521
  43.4 2.9 %collective-permute-done.8 = bf16[4,128,128]{2,1,0:T(8,128)(2,1)S(1)} collective-permute-done((bf16[4,128,128]{2,1,0:T(8,128)(2,1)S(1)}, bf16[4,128,128]{2,1,0:T(8,128)(2,1)S(1)}, u32[]{:S(2)}, u32[]{:S(2)}) %collective-permute-start.8) | collective-permute-done | bytes 131104 | tf_op jit(solution)/shard_map/ppermute | solution.py:521
  46.3 6.1 %collective-permute-start.9 = (bf16[8,128,128]{2,1,0:T(8,128)(2,1)S(1)}, bf16[8,128,128]{2,1,0:T(8,128)(2,1)S(1)}, u32[]{:S(2)}, u32[]{:S(2)}) collective-permute-start(bf16[8,128,128]{2,1,0:T(8,128)(2,1)S(1)} %pad_maximum_fusion.3.refs_0_), channel_id=1, source_target_pairs={{0,2},{1,3},{2,0},{3,1},{4,6},{5,7},{6,4},{7,5},{8,10},{9,11},{10,... | collective-permute-start | bytes 786440 | tf_op jit(solution)/shard_map/ppermute | solution.py:521
  52.4 3.8 %shard_map.109 = (bf16[1024,2048]{1,0:T(8,128)(2,1)S(1)}, bf16[2048,256]{1,0:T(8,128)(2,1)S(1)}, bf16[2048,256]{1,0:T(8,128)(2,1)S(1)}, f32[2,128,128]{2,1,0:T(8,128)S(1)}, f32[2,128,128]{2,1,0:T(8,128)S(1)}) custom-call(bf16[1024,2048]{1,0:T(8,128)(2,1)} %refs_0_.1, f32[1,2048]{1,0:T(1,128)} %bitcast.11, bf16[2048,256]{1,0:T(8,128)(2,1)} %refs_2_.1, ...), custom_call_target="tpu_custom_call" | custom-call | flops 1073741824 | tf_op jit(solution)/shard_map/pallas_call | solution.py:549
  56.2 0.0 copy-done
  56.2 3.0 %shard_map.111 = (bf16[1024,256]{1,0:T(8,128)(2,1)S(1)}, bf16[384,256]{1,0:T(8,128)(2,1)S(1)}, bf16[384,256]{1,0:T(8,128)(2,1)S(1)}) custom-call(bf16[1024,2048]{1,0:T(8,128)(2,1)S(1)} %get-tuple-element.22.normed.refs_2_, bf16[2048,256]{1,0:T(8,128)(2,1)S(1)} %get-tuple-element.26.w_pool, f32[1,256]{1,0:T(1,128)S(1)} %bitcast.5), custom_call_target="tpu_custom_call" | custom-call | flops 1073741824 | tf_op jit(solution)/shard_map/pallas_call | solution.py:549
  59.2 1.3 %collective-permute-start.13 = (bf16[384,256]{1,0:T(8,128)(2,1)S(1)}, bf16[384,256]{1,0:T(8,128)(2,1)S(1)}, u32[]{:S(2)}, u32[]{:S(2)}) collective-permute-start(bf16[384,256]{1,0:T(8,128)(2,1)S(1)} %get-tuple-element.35), channel_id=1, source_target_pairs={{0,1},{1,0},{2,3},{3,2},{4,5},{5,4},{6,7},{7,6},{8,9},{9,8},{10,11... | collective-permute-start | bytes 589832 | tf_op jit(solution)/shard_map/ppermute | solution.py:639
  60.5 2.5 %shard_map.110.query = bf16[1024,256]{1,0:T(8,128)(2,1)S(1)} custom-call(bf16[1024,2048]{1,0:T(8,128)(2,1)S(1)} %get-tuple-element.22.normed.refs_2_, bf16[2048,256]{1,0:T(8,128)(2,1)S(1)} %get-tuple-element.23.w_query, f32[2,128,128]{2,1,0:T(8,128)S(1)} %get-tuple-element.24.base.refs_4_, f32[2,128,128]{2,1,0:T(8,128)S(1)} %get-tuple-element.25.blocks.refs_5_), custom_call_target="tpu_custom_call" | custom-call | flops 1073741824 | tf_op jit(solution)/shard_map/pallas_call | solution.py:549
  63.0 0.0 copy-start.1
  63.0 0.0 collective-permute-done.9.refs_1_
  63.0 2.1 %shard_map.112 = (bf16[1024,128]{1,0:T(8,128)(2,1)S(1)}, bf16[160,128]{1,0:T(8,128)(2,1)S(1)}, bf16[160,128]{1,0:T(8,128)(2,1)S(1)}) custom-call(bf16[8,128,128]{2,1,0:T(8,128)(2,1)S(1)} %pad_maximum_fusion.3.refs_0_, bf16[8,128,128]{2,1,0:T(8,128)(2,1)S(1)} %collective-permute-done.9.refs_1_, bf16[1024,2048]{1,0:T(8,128)(2,1)S(1)} %get-tuple-element.22.normed.refs_2_, ...), custom_call_target="tpu_custom_call" | custom-call | flops 536870912 | tf_op jit(solution)/shard_map/pallas_call | solution.py:549
  65.1 0.4 collective-permute-start.10
  65.5 3.2 %collective-permute-start.11 = (bf16[160,128]{1,0:T(8,128)(2,1)S(1)}, bf16[160,128]{1,0:T(8,128)(2,1)S(1)}, u32[]{:S(2)}, u32[]{:S(2)}) collective-permute-start(bf16[160,128]{1,0:T(8,128)(2,1)S(1)} %get-tuple-element.32), channel_id=1, source_target_pairs={{2,4},{6,8},{10,12},{14,16},{18,20},{22,24},{26,28},{4,2},{8,6},{1... | collective-permute-start | bytes 122888 | tf_op jit(solution)/shard_map/ppermute | solution.py:619
  68.8 0.0 copy-done.1
  68.8 5.0 %shard_map.113 = (bf16[384,256]{1,0:T(8,128)(2,1)S(1)}, bf16[384,256]{1,0:T(8,128)(2,1)S(1)}) custom-call(f32[4]{0:T(128)S(1)} %copy-done.1, bf16[1024,256]{1,0:T(8,128)(2,1)S(1)} %shard_map.110.query, bf16[1024,128]{1,0:T(8,128)(2,1)S(1)} %get-tuple-element.28.key_value), custom_call_target="tpu_custom_call" | custom-call | flops 805306368 | tf_op jit(solution)/shard_map/pallas_call | solution.py:549
  73.8 0.0 collective-permute-done.10.first
  73.8 0.3 collective-permute-start.12
  74.1 0.0 collective-permute-done.11.second
  74.1 2.0 %shard_map.114 = (bf16[128,512]{1,0:T(8,128)(2,1)S(1)}, bf16[128,512]{1,0:T(8,128)(2,1)S(1)}) custom-call(f32[4]{0:T(128)S(1)} %copy-done.1, bf16[1024,256]{1,0:T(8,128)(2,1)S(1)} %shard_map.110.query, bf16[1024,128]{1,0:T(8,128)(2,1)S(1)} %get-tuple-element.28.key_value, bf16[1024,256]{1,0:T(8,128)(2,1)S(1)} %get-tuple-element.27.refs_3_.pool, ...), custom_call_target="tpu_custom_call" | custom-call | flops 268435456 | tf_op jit(solution)/shard_map/pallas_call | solution.py:549
  76.1 1.3 %collective-permute-start.14 = (bf16[128,512]{1,0:T(8,128)(2,1)S(1)}, bf16[128,512]{1,0:T(8,128)(2,1)S(1)}, u32[]{:S(2)}, u32[]{:S(2)}) collective-permute-start(bf16[128,512]{1,0:T(8,128)(2,1)S(1)} %get-tuple-element.36), channel_id=1, source_target_pairs={{0,1},{1,0},{2,3},{3,2},{4,5},{5,4},{6,7},{7,6},{8,9},{9,8},{10,11... | collective-permute-start | bytes 393224 | tf_op jit(solution)/shard_map/ppermute | solution.py:641
  77.3 0.0 collective-permute-done.13.refs_7_
  77.3 6.0 %collective-permute-done.14.refs_8_ = bf16[128,512]{1,0:T(8,128)(2,1)S(1)} collective-permute-done((bf16[128,512]{1,0:T(8,128)(2,1)S(1)}, bf16[128,512]{1,0:T(8,128)(2,1)S(1)}, u32[]{:S(2)}, u32[]{:S(2)}) %collective-permute-start.14) | collective-permute-done | bytes 131104 | tf_op jit(solution)/shard_map/ppermute | solution.py:641
  83.4 0.0 collective-permute-done.12.refs_6_
  83.4 0.0 collective-permute-done.5.refs_1_
  83.4 3.8 %output.1 = (bf16[512,2048]{1,0:T(8,128)(2,1)}, bf16[512,1024]{1,0:T(8,128)(2,1)S(1)}) custom-call(bf16[8,512,128]{2,1,0:T(8,128)(2,1)S(1)} %pad_maximum_fusion.refs_0_, bf16[8,512,128]{2,1,0:T(8,128)(2,1)S(1)} %collective-permute-done.5.refs_1_, bf16[8,512,128]{2,1,0:T(8,128)(2,1)S(1)} %collective-permute-done.3.refs_2_, ...), custom_call_target="tpu_custom_call" | custom-call | flops 1073741824 | tf_op jit(solution)/shard_map/output/pallas_call | solution.py:653
  87.1 0.0 collective-permute-done.4.refs_0_
  87.1 1.7 %finish.1 = bf16[512,2048]{1,0:T(8,128)(2,1)} custom-call(bf16[8,512,128]{2,1,0:T(8,128)(2,1)S(1)} %collective-permute-done.4.refs_0_, bf16[512,1024]{1,0:T(8,128)(2,1)S(1)} %get-tuple-element.37.refs_1_, bf16[512,2048]{1,0:T(8,128)(2,1)} %get-tuple-element.38.refs_2_), custom_call_target="tpu_custom_call", output_to_operand_aliasing={{}: (2, {})} | custom-call | flops 357913952 | tf_op jit(solution)/shard_map/finish/pallas_call | solution.py:669
  (3 shorter events, 0.1 us)
Async XLA Ops:
  0.0 4.0 %collective-permute-start = (bf16[1,512,128]{2,1,0:T(8,128)(2,1)}, bf16[1,512,128]{2,1,0:T(8,128)(2,1)S(1)}, u32[]{:S(2)}, u32[]{:S(2)}) collective-permute-start(bf16[1,512,128]{2,1,0:T(8,128)(2,1)} %bitcast.7), channel_id=1, source_target_pairs={{0,16},{1,17},{2,6},{3,7},{4,20},{5,21},{6,2},{7,3},{8,24},{9,25},... | collective-permute-start | bytes 393224 | tf_op jit(solution)/shard_map/ppermute | solution.py:521
  5.0 8.9 %collective-permute-start.1 = (bf16[2,512,128]{2,1,0:T(8,128)(2,1)S(1)}, bf16[2,512,128]{2,1,0:T(8,128)(2,1)S(1)}, u32[]{:S(2)}, u32[]{:S(2)}) collective-permute-start(bf16[2,512,128]{2,1,0:T(8,128)(2,1)S(1)} %pad_maximum_fusion.2), channel_id=1, source_target_pairs={{0,1},{1,0},{2,18},{3,19},{4,5},{5,4},{6,22},{7,23},{8,9},{9,8},{1... | collective-permute-start | bytes 786440 | tf_op jit(solution)/shard_map/ppermute | solution.py:521
  14.8 8.4 %collective-permute-start.2 = (bf16[4,512,128]{2,1,0:T(8,128)(2,1)S(1)}, bf16[4,512,128]{2,1,0:T(8,128)(2,1)S(1)}, u32[]{:S(2)}, u32[]{:S(2)}) collective-permute-start(bf16[4,512,128]{2,1,0:T(8,128)(2,1)S(1)} %pad_maximum_fusion.1), channel_id=1, source_target_pairs={{0,8},{1,9},{2,3},{3,2},{4,12},{5,13},{6,7},{7,6},{8,0},{9,1},{10,... | collective-permute-start | bytes 1572872 | tf_op jit(solution)/shard_map/ppermute | solution.py:521
  24.2 32.0 %copy-start = (f32[256]{0:T(256)S(1)}, f32[256]{0:T(256)}, u32[]{:S(2)}) copy-start(f32[256]{0:T(256)} %param.18) | copy-start | bytes 3076
  24.2 17.8 %collective-permute-start.3 = (bf16[8,512,128]{2,1,0:T(8,128)(2,1)S(1)}, bf16[8,512,128]{2,1,0:T(8,128)(2,1)S(1)}, u32[]{:S(2)}, u32[]{:S(2)}) collective-permute-start(bf16[8,512,128]{2,1,0:T(8,128)(2,1)S(1)} %pad_maximum_fusion.refs_0_), channel_id=1, source_target_pairs={{0,4},{1,5},{2,10},{3,11},{4,0},{5,1},{6,14},{7,15},{8,12},{9,13},... | collective-permute-start | bytes 3145736 | tf_op jit(solution)/shard_map/ppermute | solution.py:521
  25.3 11.1 %collective-permute-start.6 = (bf16[1,128,128]{2,1,0:T(8,128)(2,1)S(1)}, bf16[1,128,128]{2,1,0:T(8,128)(2,1)S(1)}, u32[]{:S(2)}, u32[]{:S(2)}) collective-permute-start(bf16[1,128,128]{2,1,0:T(8,128)(2,1)S(1)} %maximum_bitcast_fusion), channel_id=1, source_target_pairs={{0,4},{1,5},{2,18},{3,19},{4,0},{5,1},{6,22},{7,23},{8,12},{9,13},... | collective-permute-start | bytes 98312 | tf_op jit(solution)/shard_map/ppermute | solution.py:521
  36.4 5.7 %collective-permute-start.7 = (bf16[2,128,128]{2,1,0:T(8,128)(2,1)S(1)}, bf16[2,128,128]{2,1,0:T(8,128)(2,1)S(1)}, u32[]{:S(2)}, u32[]{:S(2)}) collective-permute-start(bf16[2,128,128]{2,1,0:T(8,128)(2,1)S(1)} %pad_maximum_fusion.5), channel_id=1, source_target_pairs={{0,16},{1,17},{2,10},{3,11},{4,20},{5,21},{6,14},{7,15},{8,24},{9,... | collective-permute-start | bytes 196616 | tf_op jit(solution)/shard_map/ppermute | solution.py:521
  37.9 45.5 %collective-permute-start.5 = (bf16[8,512,128]{2,1,0:T(8,128)(2,1)S(1)}, bf16[8,512,128]{2,1,0:T(8,128)(2,1)S(1)}, u32[]{:S(2)}, u32[]{:S(2)}) collective-permute-start(bf16[8,512,128]{2,1,0:T(8,128)(2,1)S(1)} %pad_maximum_fusion.refs_0_), channel_id=1, source_target_pairs={{0,2},{1,3},{2,0},{3,1},{4,6},{5,7},{6,4},{7,5},{8,10},{9,11},{10,... | collective-permute-start | bytes 3145736 | tf_op jit(solution)/shard_map/ppermute | solution.py:521
  42.0 45.1 %collective-permute-start.4 = (bf16[8,512,128]{2,1,0:T(8,128)(2,1)S(1)}, bf16[8,512,128]{2,1,0:T(8,128)(2,1)S(1)}, u32[]{:S(2)}, u32[]{:S(2)}) collective-permute-start(bf16[8,512,128]{2,1,0:T(8,128)(2,1)S(1)} %collective-permute-done.3.refs_2_), channel_id=1, source_target_pairs={{0,2},{1,3},{2,0},{3,1},{4,6},{5,7},{6,4},{7,5},{8,10},{9,11},{10,... | collective-permute-start | bytes 3145736 | tf_op jit(solution)/shard_map/ppermute | solution.py:521
  42.1 4.2 %collective-permute-start.8 = (bf16[4,128,128]{2,1,0:T(8,128)(2,1)S(1)}, bf16[4,128,128]{2,1,0:T(8,128)(2,1)S(1)}, u32[]{:S(2)}, u32[]{:S(2)}) collective-permute-start(bf16[4,128,128]{2,1,0:T(8,128)(2,1)S(1)} %pad_maximum_fusion.4), channel_id=1, source_target_pairs={{0,8},{1,9},{2,6},{3,7},{4,12},{5,13},{6,2},{7,3},{8,0},{9,1},{10,... | collective-permute-start | bytes 393224 | tf_op jit(solution)/shard_map/ppermute | solution.py:521
  46.3 16.7 %collective-permute-start.9 = (bf16[8,128,128]{2,1,0:T(8,128)(2,1)S(1)}, bf16[8,128,128]{2,1,0:T(8,128)(2,1)S(1)}, u32[]{:S(2)}, u32[]{:S(2)}) collective-permute-start(bf16[8,128,128]{2,1,0:T(8,128)(2,1)S(1)} %pad_maximum_fusion.3.refs_0_), channel_id=1, source_target_pairs={{0,2},{1,3},{2,0},{3,1},{4,6},{5,7},{6,4},{7,5},{8,10},{9,11},{10,... | collective-permute-start | bytes 786440 | tf_op jit(solution)/shard_map/ppermute | solution.py:521
  59.2 18.1 %collective-permute-start.13 = (bf16[384,256]{1,0:T(8,128)(2,1)S(1)}, bf16[384,256]{1,0:T(8,128)(2,1)S(1)}, u32[]{:S(2)}, u32[]{:S(2)}) collective-permute-start(bf16[384,256]{1,0:T(8,128)(2,1)S(1)} %get-tuple-element.35), channel_id=1, source_target_pairs={{0,1},{1,0},{2,3},{3,2},{4,5},{5,4},{6,7},{7,6},{8,9},{9,8},{10,11... | collective-permute-start | bytes 589832 | tf_op jit(solution)/shard_map/ppermute | solution.py:639
  63.0 5.8 %copy-start.1 = (f32[4]{0:T(128)S(1)}, f32[4]{0:T(128)}, u32[]{:S(2)}) copy-start(f32[4]{0:T(128)} %sink.3) | copy-start | bytes 52
  65.1 8.6 %collective-permute-start.10 = (bf16[160,128]{1,0:T(8,128)(2,1)S(1)}, bf16[160,128]{1,0:T(8,128)(2,1)S(1)}, u32[]{:S(2)}, u32[]{:S(2)}) collective-permute-start(bf16[160,128]{1,0:T(8,128)(2,1)S(1)} %get-tuple-element.31), channel_id=1, source_target_pairs={{0,2},{2,0},{4,6},{6,4},{8,10},{10,8},{12,14},{14,12},{16,18},{18,... | collective-permute-start | bytes 122888 | tf_op jit(solution)/shard_map/ppermute | solution.py:618
  65.5 8.6 %collective-permute-start.11 = (bf16[160,128]{1,0:T(8,128)(2,1)S(1)}, bf16[160,128]{1,0:T(8,128)(2,1)S(1)}, u32[]{:S(2)}, u32[]{:S(2)}) collective-permute-start(bf16[160,128]{1,0:T(8,128)(2,1)S(1)} %get-tuple-element.32), channel_id=1, source_target_pairs={{2,4},{6,8},{10,12},{14,16},{18,20},{22,24},{26,28},{4,2},{8,6},{1... | collective-permute-start | bytes 122888 | tf_op jit(solution)/shard_map/ppermute | solution.py:619
  73.8 9.6 %collective-permute-start.12 = (bf16[384,256]{1,0:T(8,128)(2,1)S(1)}, bf16[384,256]{1,0:T(8,128)(2,1)S(1)}, u32[]{:S(2)}, u32[]{:S(2)}) collective-permute-start(bf16[384,256]{1,0:T(8,128)(2,1)S(1)} %get-tuple-element.34), channel_id=1, source_target_pairs={{0,1},{1,0},{2,3},{3,2},{4,5},{5,4},{6,7},{7,6},{8,9},{9,8},{10,11... | collective-permute-start | bytes 589832 | tf_op jit(solution)/shard_map/ppermute | solution.py:640
  76.1 7.3 %collective-permute-start.14 = (bf16[128,512]{1,0:T(8,128)(2,1)S(1)}, bf16[128,512]{1,0:T(8,128)(2,1)S(1)}, u32[]{:S(2)}, u32[]{:S(2)}) collective-permute-start(bf16[128,512]{1,0:T(8,128)(2,1)S(1)} %get-tuple-element.36), channel_id=1, source_target_pairs={{0,1},{1,0},{2,3},{3,2},{4,5},{5,4},{6,7},{7,6},{8,9},{9,8},{10,11... | collective-permute-start | bytes 393224 | tf_op jit(solution)/shard_map/ppermute | solution.py:641
